TPU v7x, 512 devices: a whole 4x8x8 slice. The times are simulated.
512 devices in a mesh: ep: 128 (over z, y, core), tp: 4 (over x).
Axes of the slice: x: 4, y: 8, z: 8, core: 2. Of those that a mesh axis runs over, the one named last changes fastest.
Arguments:
- tokens: bfloat16 [16384, 1024], P('ep'), may hold values from -6 to 6
- cotangent: bfloat16 [16384, 1024], P('ep'), may hold values from -1.5 to 1.5
- routing: int32 [16384, 2], P('ep'), may hold values from 0 to 31, all different within a row; in each aligned block of 128 rows (0 to 127, 128 to 255, ...) at most 12 rows name the same one
- gates: bfloat16 [16384, 2], P('ep'), may hold values from 0.099609375 to 0.8984375
- gate_proj: bfloat16 [128, 1024, 1024], P('ep', None, 'tp'), may hold values from -0.1875 to 0.1875
- up_proj: bfloat16 [128, 1024, 1024], P('ep', None, 'tp'), may hold values from -0.1875 to 0.1875
- down_proj: bfloat16 [128, 1024, 1024], P('ep', 'tp'), may hold values from -0.09375 to 0.09375
Outputs:
- token_grad: bfloat16 [16384, 1024], P('ep')
- gate_grad: float32 [16384, 2], P('ep')
- gate_proj_grad: bfloat16 [128, 1024, 1024], P('ep', None, 'tp')
- up_proj_grad: bfloat16 [128, 1024, 1024], P('ep', None, 'tp')
- down_proj_grad: bfloat16 [128, 1024, 1024], P('ep', 'tp')
- input_row_norms: float32 [32, 2, 1024], replicated
- hidden_row_norms: float32 [128, 1024], P('ep', 'tp')
Inputs may be any that keep to these rules, and one draw needn't show every extreme that they name: `routing`: the two experts of a token differ. Among the 128 tokens of one ep index no expert is chosen more than 12 times, and on some ep index some expert is chosen exactly 12 times.
All inputs are finite; a program needn't handle non-finite values.
Results may differ from a plain program's by a relative error of at most 0.012.
Values may be sent and summed in bfloat16 or wider, within the bound.
No kernel may reach another device: no remote copies, remote signals or barrier semaphores. Data moves between devices by JAX's collectives and lax.ppermute only.
A program may use at most 128 MiB of HBM per device.

v0:
```python
import jax
import jax.numpy as jnp
import numpy as np
from jax import lax
from jax.experimental import pallas as pl
from jax.experimental.pallas import tpu as pltpu
from jax.sharding import Mesh
from jax.sharding import PartitionSpec as P

EP = ("z", "yh", "yp", "c")
HOMES = ("z", "yh")
GROUP = ("yp", "tp")
BF = jnp.bfloat16
F32 = jnp.float32
T, D, H = 128, 1024, 256
EXPERTS, SLOTS, SRC = 32, 12, 32
ROWS = SRC * SLOTS
CH = 192
ALL = 2 * ROWS
SENT = 2 * ROWS + SRC
TURNS = (0, 3, 1, 2)
NN = (((1,), (0,)), ((), ()))
NT = (((1,), (1,)), ((), ()))
TN = (((0,), (0,)), ((), ()))


def dot(a, b, dims=NN):
    return lax.dot_general(a, b, dims, preferred_element_type=F32)


def iota(shape, dim):
    return lax.broadcasted_iota(jnp.int32, shape, dim)


def call(kernel, outs, scalars, *args):
    specs = [pl.BlockSpec(memory_space=pltpu.SMEM)] if scalars is not None else []
    args = ([scalars] if scalars is not None else []) + list(args)
    specs = specs + [pl.BlockSpec(memory_space=pltpu.VMEM) for _ in range(len(args) - len(specs))]
    return kernel(outs, specs)(*args)


def kernel_of(body, name, scratch=(), flops=2**27):
    def build(outs, specs):
        return pl.pallas_call(
            body,
            out_shape=outs,
            in_specs=specs,
            out_specs=jax.tree.map(lambda _: pl.BlockSpec(memory_space=pltpu.VMEM), outs),
            scratch_shapes=list(scratch),
            compiler_params=pltpu.CompilerParams(vmem_limit_bytes=56 * 1024 * 1024),
            cost_estimate=pl.CostEstimate(flops=flops, transcendentals=0, bytes_accessed=2**20),
            name=name,
        )

    return build


def shape(dims, dtype=BF):
    return jax.ShapeDtypeStruct(dims, dtype)


def tables():
    o = np.arange(192)
    regroup = (o % 48 // 12 * 48 + o // 48 * 12 + o % 12)[:, None] == np.arange(192)[None, :]
    r = np.arange(CH)
    lane = (r % SLOTS)[:, None] == np.arange(128)[None, :]
    source = np.arange(16)[:, None] == (r // SLOTS)[None, :]
    j = np.arange(256)
    src, row = j // 32, j % 32
    at = np.where(row < 24, row // 12 * 96 + src * 12 + row % 12, 200 + row - 25)
    at = np.where(row == 24, 192 + src, at)
    back = (at[:, None] == np.arange(208)[None, :]) & (row < 29)[:, None]
    return tuple(jnp.asarray(a.astype(np.float32), BF) for a in (regroup, lane, source, back))


def dispatch_body(at, rt, gt, tok, cot, out):
    x = at[0]
    r0, r1 = rt[0:1, :], rt[1:2, :]
    g0, g1 = gt[0:1, :].astype(F32), gt[1:2, :].astype(F32)
    e = iota((EXPERTS, T), 0)
    m0, m1 = (e == r0).astype(F32), (e == r1).astype(F32)
    earlier = (iota((T, T), 0) < iota((T, T), 1)).astype(F32).astype(BF)
    before = dot((m0 + m1).astype(BF), earlier)
    base0 = r0 * 48 + jnp.sum(m0 * before, axis=0, keepdims=True).astype(jnp.int32)
    base1 = r1 * 48 + jnp.sum(m1 * before, axis=0, keepdims=True).astype(jnp.int32)

    def step(i, carry):
        row = iota((192, T), 0) + i * 192
        total = jnp.zeros((192, 128), F32)
        for half in range(2):
            cols = pl.ds(pl.multiple_of((x * 2 + half) * 128, 128), 128)
            for kind in range(2):
                off = kind * 24 + half * 12
                hit0, hit1 = row == base0 + off, row == base1 + off
                if kind == 0:
                    pick = jnp.where(hit0 | hit1, 1.0, 0.0)
                    total += dot(pick.astype(BF), tok[:, cols])
                else:
                    pick = jnp.where(hit0, g0, jnp.where(hit1, g1, 0.0))
                    total += dot(pick.astype(BF), cot[:, cols])
        out[pl.ds(pl.multiple_of(i * 192, 192), 192), :] = total.astype(BF)
        return carry

    lax.fori_loop(0, 8, step, 0)


def regroup_body(order, rows, out):
    for b in range(8):
        moved = dot(order[...], rows[b * 192 : (b + 1) * 192, :]).astype(BF)
        for k in range(4):
            out[k * ROWS + b * 48 : k * ROWS + (b + 1) * 48, :] = moved[k * 48 : (k + 1) * 48]


def places(at):
    return [pl.ds(pl.multiple_of(lax.rem(at[0] + turn, 4) * H, H), H) for turn in TURNS]


def rows_of(pieces, kind, first, count):
    cols = []
    for piece in pieces:
        for half in range(2):
            start = (kind * 2 + half) * ROWS + first
            cols.append(piece[pl.ds(start, count), :])
    return jnp.concatenate(cols, axis=1)


def expert_body(at, lane, source, *refs):
    pieces, (wg, wgo, wu, wuo, wd, wdo) = refs[:8], refs[8:14]
    out, scaled_o, ggp_o, gup_o = refs[14:18]
    pg, pu, pd = refs[18:21]
    half = at[1]
    for t, here in enumerate(places(at)):
        there = slice(t * H, (t + 1) * H)
        for mat, mine, other in ((pg, wg, wgo), (pu, wu, wuo)):
            mat[there, :H] = mine[here, :]
            mat[there, H:] = other[here, :]
        pd[:H, there] = wd[:, here]
        pd[H:, there] = wdo[:, here]
    for group in range(2):
        parity = half if group == 0 else 1 - half

        def step(i, carry, group=group, parity=parity):
            first = pl.multiple_of(i * CH, CH)
            kept = pl.ds(pl.multiple_of(group * ROWS + i * CH, CH), CH)
            rows_x = rows_of(pieces[group::2], 0, first, CH)
            rows_y = rows_of(pieces[group::2], 1, first, CH)
            pre_gate = dot(rows_x, pg[...])
            pre_up = dot(rows_x, pu[...])
            back = dot(rows_y, pd[...], NT)
            s = jax.nn.sigmoid(pre_gate)
            act = pre_gate * s
            prod = act * pre_up
            scaled_o[kept, :] = prod.astype(BF)
            ggp = (back * pre_up * s * (1.0 + pre_gate * (1.0 - s))).astype(BF)
            gup = (back * act).astype(BF)
            ggp_o[kept, :] = ggp
            gup_o[kept, :] = gup
            part = jnp.sum(back * prod, axis=1, keepdims=True)
            spread = (part * lane[...].astype(F32)).astype(BF)
            gates = dot(source[...], spread).astype(BF)
            grad = dot(ggp[:, :H], wg[...], NT) + dot(ggp[:, H:], wgo[...], NT)
            grad += dot(gup[:, :H], wu[...], NT) + dot(gup[:, H:], wuo[...], NT)
            grad = grad.astype(BF)
            for x in range(4):
                there = parity * 4 + x
                for b in range(2):
                    cols = slice((x * 2 + b) * 128, (x * 2 + b + 1) * 128)
                    out[there, pl.ds(b * ROWS + first, CH), :] = grad[:, cols]
                out[there, pl.ds(pl.multiple_of(ALL + i * 16, 16), 16), :] = gates
            return carry

        lax.fori_loop(0, ROWS // CH, step, 0)


def weights_body(at, *refs):
    pieces, (scaled, ggp, gup) = refs[:8], refs[8:11]
    g_own, u_own, d_own, far = refs[11:15]
    for t, here in enumerate(places(at)):
        both = [[rows_of((pieces[2 * t + n],), kind, 0, ROWS) for n in range(2)] for kind in range(2)]
        rows_x, rows_y = (jnp.concatenate(b, axis=0) for b in both)
        for n, own, left in ((0, g_own, ggp), (1, u_own, gup)):
            grad = dot(rows_x, left[...], TN)
            own[here, :] = grad[:, :H]
            far[n, here, :] = grad[:, H:].astype(BF)
        down = dot(scaled[...], rows_y, TN)
        d_own[:, here] = down[:H]
        far[2, here, :] = down[H:].astype(BF)


def sums_body(g_own, u_own, d_own, far, g_out, u_out, d_out, in_sq, hid_sq):
    ones = jnp.ones((8, H), BF)
    in_sq[...] = jnp.zeros((16, 8, 128), F32)
    for k, (own, out) in enumerate(((g_own, g_out), (u_own, u_out))):
        grad = own[...] + far[k].astype(F32)
        out[...] = grad.astype(BF)
        squares = dot(ones, (grad * grad).astype(BF), NT)
        for b in range(8):
            row = k * 2 + b % 2
            for copy in range(4):
                in_sq[copy * 4 + b // 2, row : row + 1, :] = squares[0:1, b * 128 : (b + 1) * 128]
    total = jnp.zeros((8, H), F32)
    for b in range(4):
        cols = slice(b * H, (b + 1) * H)
        grad = d_own[:, cols] + far[2, cols, :].astype(F32)
        d_out[:, cols] = grad.astype(BF)
        total += dot(ones, (grad * grad).astype(BF), NT)
    hid_sq[...] = total[0:1]


def back_body(order, parts, squares, out):
    norms = jnp.sum(squares[...], axis=0)

    def total(first, count):
        rows = slice(first, first + count)
        added = parts[0, rows, :].astype(F32)
        for k in range(1, 8):
            added += parts[k, rows, :].astype(F32)
        return added

    gates = total(ALL, SRC)
    for b in range(4):
        filled = [total(b * 96, 96), total(ROWS + b * 96, 96), gates[b * 8 : (b + 1) * 8], norms]
        filled = jnp.concatenate(filled, axis=0).astype(BF)
        out[b * 256 : (b + 1) * 256, :] = dot(order[...], filled).astype(BF)


def combine_body(rt, gt, got, out, gate):
    diagonal = iota((T, T), 0) == iota((T, T), 1)

    def column(row):
        return jnp.sum(jnp.where(diagonal, row, 0.0), axis=1, keepdims=True)

    r0, r1 = (column(rt[k : k + 1, :].astype(F32)).astype(jnp.int32) for k in range(2))
    gates = [column(gt[k : k + 1, :].astype(F32)) for k in range(2)]
    e = iota((T, 128), 1)
    m0, m1 = (e == r0).astype(F32), (e == r1).astype(F32)
    earlier = (iota((T, T), 1) < iota((T, T), 0)).astype(F32).astype(BF)
    before = dot(earlier, (m0 + m1).astype(BF))
    rank0 = jnp.sum(m0 * before, axis=1, keepdims=True).astype(jnp.int32)
    rank1 = jnp.sum(m1 * before, axis=1, keepdims=True).astype(jnp.int32)
    row = iota((T, 1024), 1)
    rows = got[...]
    for half in range(2):
        hit0 = row == r0 * 32 + rank0 + half * 12
        hit1 = row == r1 * 32 + rank1 + half * 12
        pick = jnp.where(hit0 | hit1, 1.0, 0.0).astype(BF)
        out[half * T : (half + 1) * T, :] = dot(pick, rows).astype(BF)
    for k, (r, rank) in enumerate(((r0, rank0), (r1, rank1))):
        both = dot(jnp.where(row == r * 32 + 24, 1.0, 0.0).astype(BF), rows)
        total = jnp.sum(jnp.where(e == rank, both, 0.0), axis=1, keepdims=True)
        share = jnp.where(diagonal, total / gates[k], 0.0)
        gate[k : k + 1, :] = jnp.sum(share, axis=0, keepdims=True)
    n = iota((T, 1024), 0)
    hit = row == (n & 31) * 32 + 25 + ((n >> 5) & 1) * 2 + (n >> 6)
    out[2 * T :, :] = dot(jnp.where(hit, 1.0, 0.0).astype(BF), rows).astype(BF)


def final_body(got, token, norms):
    for x in range(4):
        for half in range(2):
            cols = slice((x * 2 + half) * 128, (x * 2 + half + 1) * 128)
            token[:, cols] = got[x * 384 + half * T : x * 384 + (half + 1) * T, :]
            first = x * 384 + 2 * T + half * 64
            for kind in range(2):
                rows = got[first + kind * 32 : first + kind * 32 + 32, :]
                norms[:, kind, cols] = rows.astype(F32)


SWAP = [(0, 1), (1, 0)]


def turned(x, by):
    return lax.ppermute(x, "tp", [(i, (i + by) % 4) for i in range(4)])


def body(tokens, cotangent, routing, gates, gate_proj, up_proj, down_proj):
    regroup, lane, source, back = tables()
    at = jnp.stack([lax.axis_index("tp"), lax.axis_index("yp")]).astype(jnp.int32)
    weights = (gate_proj[0], up_proj[0], down_proj[0])
    sent = call(
        kernel_of(dispatch_body, "dispatch"), shape((1536, 128)), at,
        routing.T, gates.T, tokens, cotangent,
    )
    others = [lax.ppermute(w, "c", SWAP) for w in weights]
    moved = lax.all_to_all(sent.reshape(SRC, 48, 128), HOMES, 0, 0, tiled=True)
    mine = call(
        kernel_of(regroup_body, "regroup"), shape((1536, 128)), None,
        regroup, moved.reshape(1536, 128),
    )
    mine2 = turned(mine, 2)
    near = lax.ppermute(mine, "yp", SWAP)
    mine1, mine3 = turned(mine, 1), turned(mine, -1)
    near2 = lax.ppermute(mine2, "yp", SWAP)
    near1, near3 = turned(near, 1), turned(near, -1)
    pieces = (mine, near, mine1, near1, mine3, near3, mine2, near2)
    ordered = [w for pair in zip(weights, others) for w in pair]
    hidden = shape((ALL, 2 * H))
    rows, scaled, ggp, gup = call(
        kernel_of(
            expert_body, "expert",
            [pltpu.VMEM((D, 2 * H), BF), pltpu.VMEM((D, 2 * H), BF), pltpu.VMEM((2 * H, D), BF)],
            flops=2**32,
        ),
        (shape((8, SENT, 128)), hidden, hidden, hidden), at,
        lane, source, *pieces, *ordered,
    )
    parts = lax.all_to_all(rows, GROUP, 0, 0, tiled=True)
    g_own, u_own, d_own, far = call(
        kernel_of(weights_body, "weights", flops=2**31),
        (shape((D, H), F32), shape((D, H), F32), shape((H, D), F32), shape((3, D, H))),
        at, *pieces, scaled, ggp, gup,
    )
    far = lax.ppermute(far, "c", SWAP)
    gate_grad, up_grad, down_grad, squares, hid_sq = call(
        kernel_of(sums_body, "sums", flops=2**29),
        (
            shape((D, H)), shape((D, H)), shape((H, D)),
            shape((16, 8, 128), F32), shape((1, H), F32),
        ),
        None, g_own, u_own, d_own, far,
    )
    squares, parts = lax.optimization_barrier((squares, parts))
    squares = lax.all_to_all(squares, ("c",) + GROUP, 0, 0, tiled=True)
    answer = call(kernel_of(back_body, "back"), shape((1024, 128)), None, back, parts, squares)
    got = lax.all_to_all(answer.reshape(SRC, 32, 128), HOMES, 0, 0, tiled=True)
    own, gate = call(
        kernel_of(combine_body, "combine"), (shape((384, 128)), shape((2, T), F32)), None,
        routing.T, gates.T, got.reshape(1024, 128),
    )
    every = lax.all_gather(own, "tp", axis=0, tiled=True)
    token, norms = call(
        kernel_of(final_body, "final"), (shape((T, D)), shape((EXPERTS, 2, D), F32)), None, every
    )
    return (
        token,
        gate.T,
        gate_grad[None],
        up_grad[None],
        down_grad[None],
        norms,
        hid_sq,
    )


def solution(mesh):
    devices = mesh.devices.reshape(8, 4, 2, 2, mesh.shape["tp"])
    split = Mesh(devices, ("z", "yh", "yp", "c", "tp"))
    placed = (
        P(EP, None), P(EP, None), P(EP, None), P(EP, None),
        P(EP, None, "tp"), P(EP, None, "tp"), P(EP, "tp", None),
    )
    return jax.shard_map(
        body,
        mesh=split,
        in_specs=placed,
        out_specs=(
            P(EP, None), P(EP, None), P(EP, None, "tp"), P(EP, None, "tp"), P(EP, "tp", None),
            P(), P(EP, "tp"),
        ),
        check_vma=False,
    )
```

profile of v0, /device:TPU:16, one launch (start us, length us, event | category | flops | bytes accessed | tf_op | source)
XLA Modules:
  0.0 160.1 jit_solution(12256977527579733272)
XLA Ops:
  0.6 0.0 copy-start.3
  0.6 0.0 copy-start.4
  0.7 0.0 copy-start.5
  0.7 0.6 pad_add_fusion.at
  1.3 3.6 %dispatch.1 = bf16[1536,128]{1,0:T(8,128)(2,1)} custom-call(s32[2]{0:T(128)} %pad_add_fusion.at, s32[2,128]{1,0:T(2,128)} %bitcast.19, bf16[2,128]{1,0:T(2,128)(2,1)} %bitcast.21, bf16[128,1024]{1,0:T(8,128)(2,1)} %tok.1, bf16[128,1024]{1,0:T(8,128)(2,1)} %cot.1), custom_call_target="tpu_custom_call" | custom-call | flops 134217728 | bytes 1048576 | tf_op jit(solution)/shard_map/dispatch/pallas_call | solution.py:39
  4.9 16.1 %all-to-all-start = ((bf16[32,48,128]{2,1,0:T(8,128)(2,1)}), bf16[32,48,128]{2,1,0:T(8,128)(2,1)S(1)}, u32[]{:S(2)}, u32[]{:S(2)}) async-start(bf16[32,48,128]{2,1,0:T(8,128)(2,1)} %bitcast.16), calls=%async_computation | async-start | bytes 786432 | tf_op jit(solution)/shard_map/all_to_all | solution.py:285
  21.0 0.0 copy-done.3
  21.0 1.9 %collective-permute-start.7 = (bf16[1024,256]{1,0:T(8,128)(2,1)S(1)}, bf16[1024,256]{1,0:T(8,128)(2,1)S(1)}, u32[]{:S(2)}, u32[]{:S(2)}) collective-permute-start(bf16[1024,256]{1,0:T(8,128)(2,1)S(1)} %bitcast.24), channel_id=1, source_target_pairs={{0,4},{4,0},{1,5},{5,1},{2,6},{6,2},{3,7},{7,3},{8,12},{12,8},{9,1... | collective-permute-start | bytes 1572872 | tf_op jit(solution)/shard_map/ppermute | solution.py:284
  22.9 2.4 %collective-permute-start.8 = (bf16[1024,256]{1,0:T(8,128)(2,1)S(1)}, bf16[1024,256]{1,0:T(8,128)(2,1)S(1)}, u32[]{:S(2)}, u32[]{:S(2)}) collective-permute-start(bf16[1024,256]{1,0:T(8,128)(2,1)S(1)} %bitcast.26), channel_id=1, source_target_pairs={{0,4},{4,0},{1,5},{5,1},{2,6},{6,2},{3,7},{7,3},{8,12},{12,8},{9,1... | collective-permute-start | bytes 1572872 | tf_op jit(solution)/shard_map/ppermute | solution.py:284
  25.3 1.9 %collective-permute-start.9 = (bf16[256,1024]{1,0:T(8,128)(2,1)S(1)}, bf16[256,1024]{1,0:T(8,128)(2,1)S(1)}, u32[]{:S(2)}, u32[]{:S(2)}) collective-permute-start(bf16[256,1024]{1,0:T(8,128)(2,1)S(1)} %bitcast.28), channel_id=1, source_target_pairs={{0,4},{4,0},{1,5},{5,1},{2,6},{6,2},{3,7},{7,3},{8,12},{12,8},{9,1... | collective-permute-start | bytes 1572872 | tf_op jit(solution)/shard_map/ppermute | solution.py:284
  27.3 10.5 %all-to-all-done = bf16[32,48,128]{2,1,0:T(8,128)(2,1)S(1)} async-done(((bf16[32,48,128]{2,1,0:T(8,128)(2,1)}), bf16[32,48,128]{2,1,0:T(8,128)(2,1)S(1)}, u32[]{:S(2)}, u32[]{:S(2)}) %all-to-all-start) | async-done | bytes 393248 | tf_op jit(solution)/shard_map/all_to_all | solution.py:285
  37.7 0.7 copy-done.1
  38.5 2.2 %regroup.1.refs_0_ = bf16[1536,128]{1,0:T(8,128)(2,1)} custom-call(bf16[192,192]{1,0:T(8,128)(2,1)} %constant.17.clone.order, bf16[1536,128]{1,0:T(8,128)(2,1)} %bitcast.15), custom_call_target="tpu_custom_call" | custom-call | flops 134217728 | bytes 1048576 | tf_op jit(solution)/shard_map/regroup/pallas_call | solution.py:39
  40.6 4.9 %collective-permute-start.5 = (bf16[1536,128]{1,0:T(8,128)(2,1)}, bf16[1536,128]{1,0:T(8,128)(2,1)S(1)}, u32[]{:S(2)}, u32[]{:S(2)}) collective-permute-start(bf16[1536,128]{1,0:T(8,128)(2,1)} %regroup.1.refs_0_), channel_id=1, source_target_pairs={{0,2},{1,3},{2,0},{3,1},{4,6},{5,7},{6,4},{7,5},{8,10},{9,11},{10,... | collective-permute-start | bytes 1179656 | tf_op jit(solution)/shard_map/ppermute | solution.py:273
  45.6 1.9 %collective-permute-start = (bf16[1536,128]{1,0:T(8,128)(2,1)}, bf16[1536,128]{1,0:T(8,128)(2,1)S(1)}, u32[]{:S(2)}, u32[]{:S(2)}) collective-permute-start(bf16[1536,128]{1,0:T(8,128)(2,1)} %regroup.1.refs_0_), channel_id=1, source_target_pairs={{0,8},{8,0},{1,9},{9,1},{2,10},{10,2},{3,11},{11,3},{4,12},{12,4},... | collective-permute-start | bytes 1179656 | tf_op jit(solution)/shard_map/ppermute | solution.py:291
  47.5 0.0 collective-permute-done.7.refs_9_
  47.5 0.0 copy-start.6
  47.5 3.1 %collective-permute-start.3 = (bf16[1536,128]{1,0:T(8,128)(2,1)}, bf16[1536,128]{1,0:T(8,128)(2,1)S(1)}, u32[]{:S(2)}, u32[]{:S(2)}) collective-permute-start(bf16[1536,128]{1,0:T(8,128)(2,1)} %regroup.1.refs_0_), channel_id=1, source_target_pairs={{0,3},{1,0},{2,1},{3,2},{4,7},{5,4},{6,5},{7,6},{8,11},{9,8},{10,9... | collective-permute-start | bytes 1179656 | tf_op jit(solution)/shard_map/ppermute | solution.py:273
  50.6 0.0 collective-permute-done.8.refs_11_
  50.6 0.0 copy-start.7
  50.6 2.8 %collective-permute-start.1 = (bf16[1536,128]{1,0:T(8,128)(2,1)}, bf16[1536,128]{1,0:T(8,128)(2,1)S(1)}, u32[]{:S(2)}, u32[]{:S(2)}) collective-permute-start(bf16[1536,128]{1,0:T(8,128)(2,1)} %regroup.1.refs_0_), channel_id=1, source_target_pairs={{0,1},{1,2},{2,3},{3,0},{4,5},{5,6},{6,7},{7,4},{8,9},{9,10},{10,1... | collective-permute-start | bytes 1179656 | tf_op jit(solution)/shard_map/ppermute | solution.py:273
  53.4 2.0 %collective-permute-done.5.refs_6_ = bf16[1536,128]{1,0:T(8,128)(2,1)S(1)} collective-permute-done((bf16[1536,128]{1,0:T(8,128)(2,1)}, bf16[1536,128]{1,0:T(8,128)(2,1)S(1)}, u32[]{:S(2)}, u32[]{:S(2)}) %collective-permute-start.5) | collective-permute-done | bytes 393248 | tf_op jit(solution)/shard_map/ppermute | solution.py:273
  55.4 1.9 %collective-permute-start.6 = (bf16[1536,128]{1,0:T(8,128)(2,1)S(1)}, bf16[1536,128]{1,0:T(8,128)(2,1)S(1)}, u32[]{:S(2)}, u32[]{:S(2)}) collective-permute-start(bf16[1536,128]{1,0:T(8,128)(2,1)S(1)} %collective-permute-done.5.refs_6_), channel_id=1, source_target_pairs={{0,8},{8,0},{1,9},{9,1},{2,10},{10,2},{3,11},{11,3},{4,12},{12,4},... | collective-permute-start | bytes 1179656 | tf_op jit(solution)/shard_map/ppermute | solution.py:293
  57.4 0.6 collective-permute-done.refs_1_
  58.0 4.9 %collective-permute-start.4 = (bf16[1536,128]{1,0:T(8,128)(2,1)S(1)}, bf16[1536,128]{1,0:T(8,128)(2,1)S(1)}, u32[]{:S(2)}, u32[]{:S(2)}) collective-permute-start(bf16[1536,128]{1,0:T(8,128)(2,1)S(1)} %collective-permute-done.refs_1_), channel_id=1, source_target_pairs={{0,3},{1,0},{2,1},{3,2},{4,7},{5,4},{6,5},{7,6},{8,11},{9,8},{10,9... | collective-permute-start | bytes 1179656 | tf_op jit(solution)/shard_map/ppermute | solution.py:273
  62.9 0.0 collective-permute-done.9.refs_13_
  62.9 0.0 copy-start.8
  62.9 1.9 %collective-permute-start.2 = (bf16[1536,128]{1,0:T(8,128)(2,1)S(1)}, bf16[1536,128]{1,0:T(8,128)(2,1)S(1)}, u32[]{:S(2)}, u32[]{:S(2)}) collective-permute-start(bf16[1536,128]{1,0:T(8,128)(2,1)S(1)} %collective-permute-done.refs_1_), channel_id=1, source_target_pairs={{0,1},{1,2},{2,3},{3,0},{4,5},{5,6},{6,7},{7,4},{8,9},{9,10},{10,1... | collective-permute-start | bytes 1179656 | tf_op jit(solution)/shard_map/ppermute | solution.py:273
  64.8 0.0 collective-permute-done.3.refs_4_
  64.9 0.0 collective-permute-done.1.refs_2_
  64.9 1.4 collective-permute-done.6.refs_7_
  66.3 5.4 %collective-permute-done.4.refs_5_ = bf16[1536,128]{1,0:T(8,128)(2,1)S(1)} collective-permute-done((bf16[1536,128]{1,0:T(8,128)(2,1)S(1)}, bf16[1536,128]{1,0:T(8,128)(2,1)S(1)}, u32[]{:S(2)}, u32[]{:S(2)}) %collective-permute-start.4) | collective-permute-done | bytes 393248 | tf_op jit(solution)/shard_map/ppermute | solution.py:273
  71.7 2.1 %collective-permute-done.2.refs_3_ = bf16[1536,128]{1,0:T(8,128)(2,1)S(1)} collective-permute-done((bf16[1536,128]{1,0:T(8,128)(2,1)S(1)}, bf16[1536,128]{1,0:T(8,128)(2,1)S(1)}, u32[]{:S(2)}, u32[]{:S(2)}) %collective-permute-start.2) | collective-permute-done | bytes 393248 | tf_op jit(solution)/shard_map/ppermute | solution.py:273
  73.9 0.8 copy-done.15
  74.6 11.5 %expert.1 = (bf16[8,800,128]{2,1,0:T(8,128)(2,1)}, bf16[768,512]{1,0:T(8,128)(2,1)}, bf16[768,512]{1,0:T(8,128)(2,1)}, bf16[768,512]{1,0:T(8,128)(2,1)}) custom-call(s32[2]{0:T(128)} %pad_add_fusion.at, bf16[192,128]{1,0:T(8,128)(2,1)} %constant.18.clone.lane, bf16[16,192]{1,0:T(8,128)(2,1)} %constant.19.clone.source, bf16[1536,128]{1,0:T(8,128)(2,1)} %regroup.1.refs_0_, ...), custom_call_target="tpu_custom_call" | custom-call | flops 4294967296 | bytes 1048576 | tf_op jit(solution)/shard_map/expert/pallas_call | solution.py:39
  86.2 3.6 %all-to-all-start.1 = ((bf16[8,800,128]{2,1,0:T(8,128)(2,1)}), bf16[8,800,128]{2,1,0:T(8,128)(2,1)S(1)}, u32[]{:S(2)}, u32[]{:S(2)}) async-start(bf16[8,800,128]{2,1,0:T(8,128)(2,1)} %get-tuple-element.34), calls=%async_computation.1 | async-start | bytes 3276800 | tf_op jit(solution)/shard_map/all_to_all | solution.py:307
  89.8 7.0 %weights.1 = (f32[1024,256]{1,0:T(8,128)}, f32[1024,256]{1,0:T(8,128)}, f32[256,1024]{1,0:T(8,128)}, bf16[3,1024,256]{2,1,0:T(8,128)(2,1)}) custom-call(s32[2]{0:T(128)} %pad_add_fusion.at, bf16[1536,128]{1,0:T(8,128)(2,1)} %regroup.1.refs_0_, bf16[1536,128]{1,0:T(8,128)(2,1)} %copy-done.10, bf16[1536,128]{1,0:T(8,128)(2,1)} %copy-done.12, ...), custom_call_target="tpu_custom_call" | custom-call | flops 2147483648 | bytes 1048576 | tf_op jit(solution)/shard_map/weights/pallas_call | solution.py:39
  96.7 1.9 %collective-permute-start.10 = (bf16[3,1024,256]{2,1,0:T(8,128)(2,1)}, bf16[3,1024,256]{2,1,0:T(8,128)(2,1)S(1)}, u32[]{:S(2)}, u32[]{:S(2)}) collective-permute-start(bf16[3,1024,256]{2,1,0:T(8,128)(2,1)} %get-tuple-element.32), channel_id=1, source_target_pairs={{0,4},{4,0},{1,5},{5,1},{2,6},{6,2},{3,7},{7,3},{8,12},{12,8},{9,1... | collective-permute-start | bytes 4718600 | tf_op jit(solution)/shard_map/ppermute | solution.py:313
  98.7 3.6 %collective-permute-done.10.far = bf16[3,1024,256]{2,1,0:T(8,128)(2,1)S(1)} collective-permute-done((bf16[3,1024,256]{2,1,0:T(8,128)(2,1)}, bf16[3,1024,256]{2,1,0:T(8,128)(2,1)S(1)}, u32[]{:S(2)}, u32[]{:S(2)}) %collective-permute-start.10) | collective-permute-done | bytes 1572896 | tf_op jit(solution)/shard_map/ppermute | solution.py:313
  102.2 1.1 copy-done.2
  103.4 3.8 %sums.1 = (bf16[1024,256]{1,0:T(8,128)(2,1)}, bf16[1024,256]{1,0:T(8,128)(2,1)}, bf16[256,1024]{1,0:T(8,128)(2,1)}, f32[16,8,128]{2,1,0:T(8,128)}, f32[1,256]{1,0:T(1,128)}) custom-call(f32[1024,256]{1,0:T(8,128)} %get-tuple-element.29.g_own, f32[1024,256]{1,0:T(8,128)} %get-tuple-element.30.u_own, f32[256,1024]{1,0:T(8,128)} %get-tuple-element.31.d_own, ...), custom_call_target="tpu_custom_call" | custom-call | flops 536870912 | bytes 1048576 | tf_op jit(solution)/shard_map/sums/pallas_call | solution.py:39
  107.2 1.2 all-to-all-done.1.parts
  108.4 10.8 %all_to_all.20.squares = f32[16,8,128]{2,1,0:T(8,128)} all-to-all(f32[16,8,128]{2,1,0:T(8,128)} %get-tuple-element.36), channel_id=1, replica_groups=mesh['z'=8,'yh'=4,'yp'=2,'c'=2,'tp'=4] {'c','yp','tp'}, dimensions={0} | all-to-all | bytes 131072 | tf_op jit(solution)/shard_map/all_to_all | solution.py:323
  119.2 2.6 %back.1 = bf16[1024,128]{1,0:T(8,128)(2,1)} custom-call(bf16[256,208]{1,0:T(8,128)(2,1)} %constant.20.clone.order, bf16[8,800,128]{2,1,0:T(8,128)(2,1)} %copy-done, f32[16,8,128]{2,1,0:T(8,128)} %all_to_all.20.squares), custom_call_target="tpu_custom_call" | custom-call | flops 134217728 | bytes 1048576 | tf_op jit(solution)/shard_map/back/pallas_call | solution.py:39
  121.8 20.4 %all_to_all.21 = bf16[32,32,128]{2,1,0:T(8,128)(2,1)} all-to-all(bf16[32,32,128]{2,1,0:T(8,128)(2,1)} %bitcast.17), channel_id=1, replica_groups=mesh['z'=8,'yh'=4,'yp'=2,'c'=2,'tp'=4] {'z','yh'}, dimensions={0} | all-to-all | bytes 524288 | tf_op jit(solution)/shard_map/all_to_all | solution.py:325
  142.2 2.5 %combine.1 = (bf16[384,128]{1,0:T(8,128)(2,1)}, f32[2,128]{1,0:T(2,128)}) custom-call(s32[2,128]{1,0:T(2,128)} %bitcast.20, bf16[2,128]{1,0:T(2,128)(2,1)} %bitcast.22, bf16[1024,128]{1,0:T(8,128)(2,1)} %bitcast.18), custom_call_target="tpu_custom_call" | custom-call | flops 134217728 | bytes 1048576 | tf_op jit(solution)/shard_map/combine/pallas_call | solution.py:39
  144.7 13.5 %all_gather.3.got = bf16[1536,128]{1,0:T(8,128)(2,1)} all-gather(bf16[384,128]{1,0:T(8,128)(2,1)} %get-tuple-element.37), channel_id=1, replica_groups=mesh['z'=8,'yh'=4,'yp'=2,'c'=2,'tp'=4] {'tp'}, dimensions={0}, use_global_device_ids=true | all-gather | bytes 491520 | tf_op jit(solution)/shard_map/all_gather | solution.py:330
  158.2 1.9 %final.1 = (bf16[128,1024]{1,0:T(8,128)(2,1)}, f32[32,2,1024]{2,1,0:T(2,128)}) custom-call(bf16[1536,128]{1,0:T(8,128)(2,1)} %all_gather.3.got), custom_call_target="tpu_custom_call" | custom-call | flops 134217728 | bytes 1048576 | tf_op jit(solution)/shard_map/final/pallas_call | solution.py:39
  (22 shorter events, 0.0 us)
Async XLA Ops:
  0.6 20.3 %copy-start.3 = (bf16[1,1024,256]{2,1,0:T(8,128)(2,1)S(1)}, bf16[1,1024,256]{2,1,0:T(8,128)(2,1)}, u32[]{:S(2)}) copy-start(bf16[1,1024,256]{2,1,0:T(8,128)(2,1)} %param.15) | copy-start | bytes 1572868
  0.6 22.3 %copy-start.4 = (bf16[1,1024,256]{2,1,0:T(8,128)(2,1)S(1)}, bf16[1,1024,256]{2,1,0:T(8,128)(2,1)}, u32[]{:S(2)}) copy-start(bf16[1,1024,256]{2,1,0:T(8,128)(2,1)} %param.16) | copy-start | bytes 1572868
  0.7 24.7 %copy-start.5 = (bf16[1,256,1024]{2,1,0:T(8,128)(2,1)S(1)}, bf16[1,256,1024]{2,1,0:T(8,128)(2,1)}, u32[]{:S(2)}) copy-start(bf16[1,256,1024]{2,1,0:T(8,128)(2,1)} %param.17) | copy-start | bytes 1572868
  4.9 32.8 %all-to-all-start = ((bf16[32,48,128]{2,1,0:T(8,128)(2,1)}), bf16[32,48,128]{2,1,0:T(8,128)(2,1)S(1)}, u32[]{:S(2)}, u32[]{:S(2)}) async-start(bf16[32,48,128]{2,1,0:T(8,128)(2,1)} %bitcast.16), calls=%async_computation | async-start | bytes 786432 | tf_op jit(solution)/shard_map/all_to_all | solution.py:285
  21.0 26.5 %collective-permute-start.7 = (bf16[1024,256]{1,0:T(8,128)(2,1)S(1)}, bf16[1024,256]{1,0:T(8,128)(2,1)S(1)}, u32[]{:S(2)}, u32[]{:S(2)}) collective-permute-start(bf16[1024,256]{1,0:T(8,128)(2,1)S(1)} %bitcast.24), channel_id=1, source_target_pairs={{0,4},{4,0},{1,5},{5,1},{2,6},{6,2},{3,7},{7,3},{8,12},{12,8},{9,1... | collective-permute-start | bytes 1572872 | tf_op jit(solution)/shard_map/ppermute | solution.py:284
  22.9 27.7 %collective-permute-start.8 = (bf16[1024,256]{1,0:T(8,128)(2,1)S(1)}, bf16[1024,256]{1,0:T(8,128)(2,1)S(1)}, u32[]{:S(2)}, u32[]{:S(2)}) collective-permute-start(bf16[1024,256]{1,0:T(8,128)(2,1)S(1)} %bitcast.26), channel_id=1, source_target_pairs={{0,4},{4,0},{1,5},{5,1},{2,6},{6,2},{3,7},{7,3},{8,12},{12,8},{9,1... | collective-permute-start | bytes 1572872 | tf_op jit(solution)/shard_map/ppermute | solution.py:284
  25.3 37.5 %collective-permute-start.9 = (bf16[256,1024]{1,0:T(8,128)(2,1)S(1)}, bf16[256,1024]{1,0:T(8,128)(2,1)S(1)}, u32[]{:S(2)}, u32[]{:S(2)}) collective-permute-start(bf16[256,1024]{1,0:T(8,128)(2,1)S(1)} %bitcast.28), channel_id=1, source_target_pairs={{0,4},{4,0},{1,5},{5,1},{2,6},{6,2},{3,7},{7,3},{8,12},{12,8},{9,1... | collective-permute-start | bytes 1572872 | tf_op jit(solution)/shard_map/ppermute | solution.py:284
  37.7 0.7 copy-start.1
  40.6 14.8 %collective-permute-start.5 = (bf16[1536,128]{1,0:T(8,128)(2,1)}, bf16[1536,128]{1,0:T(8,128)(2,1)S(1)}, u32[]{:S(2)}, u32[]{:S(2)}) collective-permute-start(bf16[1536,128]{1,0:T(8,128)(2,1)} %regroup.1.refs_0_), channel_id=1, source_target_pairs={{0,2},{1,3},{2,0},{3,1},{4,6},{5,7},{6,4},{7,5},{8,10},{9,11},{10,... | collective-permute-start | bytes 1179656 | tf_op jit(solution)/shard_map/ppermute | solution.py:273
  45.6 12.4 %collective-permute-start = (bf16[1536,128]{1,0:T(8,128)(2,1)}, bf16[1536,128]{1,0:T(8,128)(2,1)S(1)}, u32[]{:S(2)}, u32[]{:S(2)}) collective-permute-start(bf16[1536,128]{1,0:T(8,128)(2,1)} %regroup.1.refs_0_), channel_id=1, source_target_pairs={{0,8},{8,0},{1,9},{9,1},{2,10},{10,2},{3,11},{11,3},{4,12},{12,4},... | collective-permute-start | bytes 1179656 | tf_op jit(solution)/shard_map/ppermute | solution.py:291
  47.5 26.3 %copy-start.6 = (bf16[1024,256]{1,0:T(8,128)(2,1)}, bf16[1024,256]{1,0:T(8,128)(2,1)S(1)}, u32[]{:S(2)}) copy-start(bf16[1024,256]{1,0:T(8,128)(2,1)S(1)} %collective-permute-done.7.refs_9_) | copy-start | bytes 1572868
  47.5 17.3 %collective-permute-start.3 = (bf16[1536,128]{1,0:T(8,128)(2,1)}, bf16[1536,128]{1,0:T(8,128)(2,1)S(1)}, u32[]{:S(2)}, u32[]{:S(2)}) collective-permute-start(bf16[1536,128]{1,0:T(8,128)(2,1)} %regroup.1.refs_0_), channel_id=1, source_target_pairs={{0,3},{1,0},{2,1},{3,2},{4,7},{5,4},{6,5},{7,6},{8,11},{9,8},{10,9... | collective-permute-start | bytes 1179656 | tf_op jit(solution)/shard_map/ppermute | solution.py:273
  50.6 23.2 %copy-start.7 = (bf16[1024,256]{1,0:T(8,128)(2,1)}, bf16[1024,256]{1,0:T(8,128)(2,1)S(1)}, u32[]{:S(2)}) copy-start(bf16[1024,256]{1,0:T(8,128)(2,1)S(1)} %collective-permute-done.8.refs_11_) | copy-start | bytes 1572868
  50.6 14.2 %collective-permute-start.1 = (bf16[1536,128]{1,0:T(8,128)(2,1)}, bf16[1536,128]{1,0:T(8,128)(2,1)S(1)}, u32[]{:S(2)}, u32[]{:S(2)}) collective-permute-start(bf16[1536,128]{1,0:T(8,128)(2,1)} %regroup.1.refs_0_), channel_id=1, source_target_pairs={{0,1},{1,2},{2,3},{3,0},{4,5},{5,6},{6,7},{7,4},{8,9},{9,10},{10,1... | collective-permute-start | bytes 1179656 | tf_op jit(solution)/shard_map/ppermute | solution.py:273
  55.4 18.4 %copy-start.9 = (bf16[1536,128]{1,0:T(8,128)(2,1)}, bf16[1536,128]{1,0:T(8,128)(2,1)S(1)}, u32[]{:S(2)}) copy-start(bf16[1536,128]{1,0:T(8,128)(2,1)S(1)} %collective-permute-done.5.refs_6_) | copy-start | bytes 1179652
  55.4 10.8 %collective-permute-start.6 = (bf16[1536,128]{1,0:T(8,128)(2,1)S(1)}, bf16[1536,128]{1,0:T(8,128)(2,1)S(1)}, u32[]{:S(2)}, u32[]{:S(2)}) collective-permute-start(bf16[1536,128]{1,0:T(8,128)(2,1)S(1)} %collective-permute-done.5.refs_6_), channel_id=1, source_target_pairs={{0,8},{8,0},{1,9},{9,1},{2,10},{10,2},{3,11},{11,3},{4,12},{12,4},... | collective-permute-start | bytes 1179656 | tf_op jit(solution)/shard_map/ppermute | solution.py:293
  58.0 15.9 %copy-start.10 = (bf16[1536,128]{1,0:T(8,128)(2,1)}, bf16[1536,128]{1,0:T(8,128)(2,1)S(1)}, u32[]{:S(2)}) copy-start(bf16[1536,128]{1,0:T(8,128)(2,1)S(1)} %collective-permute-done.refs_1_) | copy-start | bytes 1179652
  58.0 13.7 %collective-permute-start.4 = (bf16[1536,128]{1,0:T(8,128)(2,1)S(1)}, bf16[1536,128]{1,0:T(8,128)(2,1)S(1)}, u32[]{:S(2)}, u32[]{:S(2)}) collective-permute-start(bf16[1536,128]{1,0:T(8,128)(2,1)S(1)} %collective-permute-done.refs_1_), channel_id=1, source_target_pairs={{0,3},{1,0},{2,1},{3,2},{4,7},{5,4},{6,5},{7,6},{8,11},{9,8},{10,9... | collective-permute-start | bytes 1179656 | tf_op jit(solution)/shard_map/ppermute | solution.py:273
  62.9 10.9 %copy-start.8 = (bf16[256,1024]{1,0:T(8,128)(2,1)}, bf16[256,1024]{1,0:T(8,128)(2,1)S(1)}, u32[]{:S(2)}) copy-start(bf16[256,1024]{1,0:T(8,128)(2,1)S(1)} %collective-permute-done.9.refs_13_) | copy-start | bytes 1572868
  62.9 10.9 %collective-permute-start.2 = (bf16[1536,128]{1,0:T(8,128)(2,1)S(1)}, bf16[1536,128]{1,0:T(8,128)(2,1)S(1)}, u32[]{:S(2)}, u32[]{:S(2)}) collective-permute-start(bf16[1536,128]{1,0:T(8,128)(2,1)S(1)} %collective-permute-done.refs_1_), channel_id=1, source_target_pairs={{0,1},{1,2},{2,3},{3,0},{4,5},{5,6},{6,7},{7,4},{8,9},{9,10},{10,1... | collective-permute-start | bytes 1179656 | tf_op jit(solution)/shard_map/ppermute | solution.py:273
  64.9 9.0 %copy-start.11 = (bf16[1536,128]{1,0:T(8,128)(2,1)}, bf16[1536,128]{1,0:T(8,128)(2,1)S(1)}, u32[]{:S(2)}) copy-start(bf16[1536,128]{1,0:T(8,128)(2,1)S(1)} %collective-permute-done.3.refs_4_) | copy-start | bytes 1179652
  64.9 9.0 %copy-start.12 = (bf16[1536,128]{1,0:T(8,128)(2,1)}, bf16[1536,128]{1,0:T(8,128)(2,1)S(1)}, u32[]{:S(2)}) copy-start(bf16[1536,128]{1,0:T(8,128)(2,1)S(1)} %collective-permute-done.1.refs_2_) | copy-start | bytes 1179652
  66.3 7.6 %copy-start.13 = (bf16[1536,128]{1,0:T(8,128)(2,1)}, bf16[1536,128]{1,0:T(8,128)(2,1)S(1)}, u32[]{:S(2)}) copy-start(bf16[1536,128]{1,0:T(8,128)(2,1)S(1)} %collective-permute-done.6.refs_7_) | copy-start | bytes 1179652
  71.7 2.2 %copy-start.14 = (bf16[1536,128]{1,0:T(8,128)(2,1)}, bf16[1536,128]{1,0:T(8,128)(2,1)S(1)}, u32[]{:S(2)}) copy-start(bf16[1536,128]{1,0:T(8,128)(2,1)S(1)} %collective-permute-done.4.refs_5_) | copy-start | bytes 1179652
  73.9 0.8 copy-start.15
  86.2 22.2 %all-to-all-start.1 = ((bf16[8,800,128]{2,1,0:T(8,128)(2,1)}), bf16[8,800,128]{2,1,0:T(8,128)(2,1)S(1)}, u32[]{:S(2)}, u32[]{:S(2)}) async-start(bf16[8,800,128]{2,1,0:T(8,128)(2,1)} %get-tuple-element.34), calls=%async_computation.1 | async-start | bytes 3276800 | tf_op jit(solution)/shard_map/all_to_all | solution.py:307
  96.7 5.5 %collective-permute-start.10 = (bf16[3,1024,256]{2,1,0:T(8,128)(2,1)}, bf16[3,1024,256]{2,1,0:T(8,128)(2,1)S(1)}, u32[]{:S(2)}, u32[]{:S(2)}) collective-permute-start(bf16[3,1024,256]{2,1,0:T(8,128)(2,1)} %get-tuple-element.32), channel_id=1, source_target_pairs={{0,4},{4,0},{1,5},{5,1},{2,6},{6,2},{3,7},{7,3},{8,12},{12,8},{9,1... | collective-permute-start | bytes 4718600 | tf_op jit(solution)/shard_map/ppermute | solution.py:313
  102.2 1.1 copy-start.2
  108.4 10.8 %copy-start = (bf16[8,800,128]{2,1,0:T(8,128)(2,1)}, bf16[8,800,128]{2,1,0:T(8,128)(2,1)S(1)}, u32[]{:S(2)}) copy-start(bf16[8,800,128]{2,1,0:T(8,128)(2,1)S(1)} %all-to-all-done.1.parts) | copy-start | bytes 4915204
where the time goes:
time: 161 us; the launch traced here: 160 us
  starting transfers between devices  49.3 us (31%)
  blocking collectives  44.7 us (28%)
  Pallas kernels  35.1 us (22%)
  waiting for transfers between devices  26.8 us (17%)
  local copies, waits for them, and re-layouts  2.72 us (2%)
    pallas_call x8, Pallas kernels, call(): return kernel(outs, specs)(*args)  35.1 us
    all_to_all x1, blocking collectives, body(): got = lax.all_to_all(answer.reshape(SRC, 32, 128), HOMES, 0, 0, tiled=True)  20.4 us
    ppermute x5, starting transfers between devices, turned(): return lax.ppermute(x, 'tp', [(i, (i + by) % 4) for i in range(4)])  17.6 us
    all_to_all x1, starting transfers between devices, body(): moved = lax.all_to_all(sent.reshape(SRC, 48, 128), HOMES, 0, 0, tiled=True)  16.1 us
    all_gather x1, blocking collectives, body(): every = lax.all_gather(own, 'tp', axis=0, tiled=True)  13.5 us
    all_to_all x1, blocking collectives, body(): squares = lax.all_to_all(squares, ('c',) + GROUP, 0, 0, tiled=True)  10.8 us
    all_to_all x1, waiting for transfers between devices, body(): moved = lax.all_to_all(sent.reshape(SRC, 48, 128), HOMES, 0, 0, tiled=True)  10.5 us
    ppermute x5, waiting for transfers between devices, turned(): return lax.ppermute(x, 'tp', [(i, (i + by) % 4) for i in range(4)])  9.54 us
  transfers between devices with their start and end apart: 13, of which 8 were waited for; matrix products, arithmetic and copies ran while one was open for 0% of the time, Pallas kernels for 8%

commit v1 on v0

--- a/solution.py
+++ b/solution.py
@@ -18,6 +18,7 @@
 CH = 192
 ALL = 2 * ROWS
 SENT = 2 * ROWS + SRC
+VM = (8, 8, 8)
 TURNS = (0, 3, 1, 2)
 NN = (((1,), (0,)), ((), ()))
 NT = (((1,), (1,)), ((), ()))
@@ -32,22 +33,18 @@
     return lax.broadcasted_iota(jnp.int32, shape, dim)
 
 
-def call(kernel, outs, scalars, *args):
-    specs = [pl.BlockSpec(memory_space=pltpu.SMEM)] if scalars is not None else []
-    args = ([scalars] if scalars is not None else []) + list(args)
-    specs = specs + [pl.BlockSpec(memory_space=pltpu.VMEM) for _ in range(len(args) - len(specs))]
-    return kernel(outs, specs)(*args)
-
-
-def kernel_of(body, name, scratch=(), flops=2**27):
+def call(kernel, outs, *args):
+    return kernel(outs, [pl.BlockSpec(memory_space=pltpu.VMEM) for _ in args])(*args)
+
+
+def kernel_of(body, name, flops=2**27, vmem=4):
     def build(outs, specs):
         return pl.pallas_call(
             body,
             out_shape=outs,
             in_specs=specs,
             out_specs=jax.tree.map(lambda _: pl.BlockSpec(memory_space=pltpu.VMEM), outs),
-            scratch_shapes=list(scratch),
-            compiler_params=pltpu.CompilerParams(vmem_limit_bytes=56 * 1024 * 1024),
+            compiler_params=pltpu.CompilerParams(vmem_limit_bytes=vmem * 1024 * 1024),
             cost_estimate=pl.CostEstimate(flops=flops, transcendentals=0, bytes_accessed=2**20),
             name=name,
         )
@@ -73,8 +70,8 @@
     return tuple(jnp.asarray(a.astype(np.float32), BF) for a in (regroup, lane, source, back))
 
 
-def dispatch_body(at, rt, gt, tok, cot, out):
-    x = at[0]
+def dispatch_body(rt, gt, tok, cot, out):
+    x = lax.axis_index("tp")
     r0, r1 = rt[0:1, :], rt[1:2, :]
     g0, g1 = gt[0:1, :].astype(F32), gt[1:2, :].astype(F32)
     e = iota((EXPERTS, T), 0)
@@ -111,8 +108,23 @@
             out[k * ROWS + b * 48 : k * ROWS + (b + 1) * 48, :] = moved[k * 48 : (k + 1) * 48]
 
 
-def places(at):
-    return [pl.ds(pl.multiple_of(lax.rem(at[0] + turn, 4) * H, H), H) for turn in TURNS]
+def blocks():
+    x = lax.axis_index("tp")
+    return [lax.rem(x + turn, 4) for turn in TURNS]
+
+
+def places():
+    return [pl.ds(pl.multiple_of(b * H, H), H) for b in blocks()]
+
+
+def prepare_body(wg, wgo, wu, wuo, wd, wdo, pg, pu, pd):
+    for t, here in enumerate(places()):
+        there = slice(t * H, (t + 1) * H)
+        for mat, mine, other in ((pg, wg, wgo), (pu, wu, wuo)):
+            mat[there, :H] = mine[here, :]
+            mat[there, H:] = other[here, :]
+        pd[:H, there] = wd[:, here]
+        pd[H:, there] = wdo[:, here]
 
 
 def rows_of(pieces, kind, first, count):
@@ -124,65 +136,62 @@
     return jnp.concatenate(cols, axis=1)
 
 
-def expert_body(at, lane, source, *refs):
-    pieces, (wg, wgo, wu, wuo, wd, wdo) = refs[:8], refs[8:14]
-    out, scaled_o, ggp_o, gup_o = refs[14:18]
-    pg, pu, pd = refs[18:21]
-    half = at[1]
-    for t, here in enumerate(places(at)):
-        there = slice(t * H, (t + 1) * H)
-        for mat, mine, other in ((pg, wg, wgo), (pu, wu, wuo)):
-            mat[there, :H] = mine[here, :]
-            mat[there, H:] = other[here, :]
-        pd[:H, there] = wd[:, here]
-        pd[H:, there] = wdo[:, here]
-    for group in range(2):
-        parity = half if group == 0 else 1 - half
-
-        def step(i, carry, group=group, parity=parity):
-            first = pl.multiple_of(i * CH, CH)
-            kept = pl.ds(pl.multiple_of(group * ROWS + i * CH, CH), CH)
-            rows_x = rows_of(pieces[group::2], 0, first, CH)
-            rows_y = rows_of(pieces[group::2], 1, first, CH)
-            pre_gate = dot(rows_x, pg[...])
-            pre_up = dot(rows_x, pu[...])
-            back = dot(rows_y, pd[...], NT)
-            s = jax.nn.sigmoid(pre_gate)
-            act = pre_gate * s
-            prod = act * pre_up
-            scaled_o[kept, :] = prod.astype(BF)
-            ggp = (back * pre_up * s * (1.0 + pre_gate * (1.0 - s))).astype(BF)
-            gup = (back * act).astype(BF)
-            ggp_o[kept, :] = ggp
-            gup_o[kept, :] = gup
-            part = jnp.sum(back * prod, axis=1, keepdims=True)
-            spread = (part * lane[...].astype(F32)).astype(BF)
-            gates = dot(source[...], spread).astype(BF)
-            grad = dot(ggp[:, :H], wg[...], NT) + dot(ggp[:, H:], wgo[...], NT)
-            grad += dot(gup[:, :H], wu[...], NT) + dot(gup[:, H:], wuo[...], NT)
-            grad = grad.astype(BF)
-            for x in range(4):
-                there = parity * 4 + x
-                for b in range(2):
-                    cols = slice((x * 2 + b) * 128, (x * 2 + b + 1) * 128)
-                    out[there, pl.ds(b * ROWS + first, CH), :] = grad[:, cols]
-                out[there, pl.ds(pl.multiple_of(ALL + i * 16, 16), 16), :] = gates
-            return carry
-
-        lax.fori_loop(0, ROWS // CH, step, 0)
-
-
-def weights_body(at, *refs):
-    pieces, (scaled, ggp, gup) = refs[:8], refs[8:11]
-    g_own, u_own, d_own, far = refs[11:15]
-    for t, here in enumerate(places(at)):
-        both = [[rows_of((pieces[2 * t + n],), kind, 0, ROWS) for n in range(2)] for kind in range(2)]
-        rows_x, rows_y = (jnp.concatenate(b, axis=0) for b in both)
-        for n, own, left in ((0, g_own, ggp), (1, u_own, gup)):
-            grad = dot(rows_x, left[...], TN)
+def expert_rows(pieces, lane, source, pg, pu, pd, out, group, scaled_o, ggp_o, gup_o):
+    def step(i, carry):
+        first = pl.multiple_of(i * CH, CH)
+        kept = pl.ds(first, CH)
+        rows_x = rows_of(pieces, 0, first, CH)
+        rows_y = rows_of(pieces, 1, first, CH)
+        pre_gate = dot(rows_x, pg[...])
+        pre_up = dot(rows_x, pu[...])
+        back = dot(rows_y, pd[...], NT)
+        s = jax.nn.sigmoid(pre_gate)
+        act = pre_gate * s
+        prod = act * pre_up
+        scaled_o[kept, :] = prod.astype(BF)
+        ggp = (back * pre_up * s * (1.0 + pre_gate * (1.0 - s))).astype(BF)
+        gup = (back * act).astype(BF)
+        ggp_o[kept, :] = ggp
+        gup_o[kept, :] = gup
+        part = jnp.sum(back * prod, axis=1, keepdims=True)
+        spread = (part * lane[...].astype(F32)).astype(BF)
+        gates = dot(source[...], spread).astype(BF)
+        grad = (dot(ggp, pg[...], NT) + dot(gup, pu[...], NT)).astype(BF)
+        for t, x in enumerate(blocks()):
+            for b in range(2):
+                cols = slice((t * 2 + b) * 128, (t * 2 + b + 1) * 128)
+                out[group * 4 + x, pl.ds(b * ROWS + first, CH), :] = grad[:, cols]
+            out[group * 4 + x, pl.ds(pl.multiple_of(ALL + i * 16, 16), 16), :] = gates
+        return carry
+
+    lax.fori_loop(0, ROWS // CH, step, 0)
+
+
+def first_body(lane, source, *refs):
+    pieces, (pg, pu, pd), (out, *hidden) = refs[:4], refs[4:7], refs[7:]
+    expert_rows(pieces, lane, source, pg, pu, pd, out, 0, *hidden)
+
+
+def second_body(lane, source, early, *refs):
+    pieces, (pg, pu, pd), (out, *hidden) = refs[:4], refs[4:7], refs[7:]
+    half = lax.axis_index("yp")
+    for x in range(4):
+        out[half * 4 + x] = early[x]
+    expert_rows(pieces, lane, source, pg, pu, pd, out, 1 - half, *hidden)
+
+
+def weights_body(*refs):
+    pieces = refs[:4], refs[4:8]
+    hidden = refs[8:11], refs[11:14]
+    g_own, u_own, d_own, far = refs[14:18]
+    for t, here in enumerate(places()):
+        rows_x = [rows_of((p[t],), 0, 0, ROWS) for p in pieces]
+        rows_y = [rows_of((p[t],), 1, 0, ROWS) for p in pieces]
+        for n, own in ((0, g_own), (1, u_own)):
+            grad = sum(dot(rows_x[k], hidden[k][1 + n][...], TN) for k in range(2))
             own[here, :] = grad[:, :H]
             far[n, here, :] = grad[:, H:].astype(BF)
-        down = dot(scaled[...], rows_y, TN)
+        down = sum(dot(hidden[k][0][...], rows_y[k], TN) for k in range(2))
         d_own[:, here] = down[:H]
         far[2, here, :] = down[H:].astype(BF)
 
@@ -227,6 +236,10 @@
 def combine_body(rt, gt, got, out, gate):
     diagonal = iota((T, T), 0) == iota((T, T), 1)
 
+    def put(where, value):
+        for x in range(4):
+            out[x, where, :] = value.astype(BF)
+
     def column(row):
         return jnp.sum(jnp.where(diagonal, row, 0.0), axis=1, keepdims=True)
 
@@ -244,7 +257,7 @@
         hit0 = row == r0 * 32 + rank0 + half * 12
         hit1 = row == r1 * 32 + rank1 + half * 12
         pick = jnp.where(hit0 | hit1, 1.0, 0.0).astype(BF)
-        out[half * T : (half + 1) * T, :] = dot(pick, rows).astype(BF)
+        put(slice(half * T, (half + 1) * T), dot(pick, rows))
     for k, (r, rank) in enumerate(((r0, rank0), (r1, rank1))):
         both = dot(jnp.where(row == r * 32 + 24, 1.0, 0.0).astype(BF), rows)
         total = jnp.sum(jnp.where(e == rank, both, 0.0), axis=1, keepdims=True)
@@ -252,17 +265,17 @@
         gate[k : k + 1, :] = jnp.sum(share, axis=0, keepdims=True)
     n = iota((T, 1024), 0)
     hit = row == (n & 31) * 32 + 25 + ((n >> 5) & 1) * 2 + (n >> 6)
-    out[2 * T :, :] = dot(jnp.where(hit, 1.0, 0.0).astype(BF), rows).astype(BF)
+    put(slice(2 * T, 3 * T), dot(jnp.where(hit, 1.0, 0.0).astype(BF), rows))
 
 
 def final_body(got, token, norms):
     for x in range(4):
         for half in range(2):
             cols = slice((x * 2 + half) * 128, (x * 2 + half + 1) * 128)
-            token[:, cols] = got[x * 384 + half * T : x * 384 + (half + 1) * T, :]
-            first = x * 384 + 2 * T + half * 64
+            token[:, cols] = got[x, half * T : (half + 1) * T, :]
+            first = 2 * T + half * 64
             for kind in range(2):
-                rows = got[first + kind * 32 : first + kind * 32 + 32, :]
+                rows = got[x, first + kind * 32 : first + kind * 32 + 32, :]
                 norms[:, kind, cols] = rows.astype(F32)
 
 
@@ -275,61 +288,62 @@
 
 def body(tokens, cotangent, routing, gates, gate_proj, up_proj, down_proj):
     regroup, lane, source, back = tables()
-    at = jnp.stack([lax.axis_index("tp"), lax.axis_index("yp")]).astype(jnp.int32)
     weights = (gate_proj[0], up_proj[0], down_proj[0])
     sent = call(
-        kernel_of(dispatch_body, "dispatch"), shape((1536, 128)), at,
+        kernel_of(dispatch_body, "dispatch"), shape((1536, 128)),
         routing.T, gates.T, tokens, cotangent,
     )
     others = [lax.ppermute(w, "c", SWAP) for w in weights]
     moved = lax.all_to_all(sent.reshape(SRC, 48, 128), HOMES, 0, 0, tiled=True)
     mine = call(
-        kernel_of(regroup_body, "regroup"), shape((1536, 128)), None,
-        regroup, moved.reshape(1536, 128),
+        kernel_of(regroup_body, "regroup"), shape((1536, 128)), regroup, moved.reshape(1536, 128)
     )
     mine2 = turned(mine, 2)
     near = lax.ppermute(mine, "yp", SWAP)
     mine1, mine3 = turned(mine, 1), turned(mine, -1)
     near2 = lax.ppermute(mine2, "yp", SWAP)
     near1, near3 = turned(near, 1), turned(near, -1)
-    pieces = (mine, near, mine1, near1, mine3, near3, mine2, near2)
-    ordered = [w for pair in zip(weights, others) for w in pair]
-    hidden = shape((ALL, 2 * H))
-    rows, scaled, ggp, gup = call(
-        kernel_of(
-            expert_body, "expert",
-            [pltpu.VMEM((D, 2 * H), BF), pltpu.VMEM((D, 2 * H), BF), pltpu.VMEM((2 * H, D), BF)],
-            flops=2**32,
-        ),
-        (shape((8, SENT, 128)), hidden, hidden, hidden), at,
-        lane, source, *pieces, *ordered,
+    pieces, nears = (mine, mine1, mine3, mine2), (near, near1, near3, near2)
+    ordered = call(
+        kernel_of(prepare_body, "prepare"),
+        (shape((D, 2 * H)), shape((D, 2 * H)), shape((2 * H, D))),
+        *(w for pair in zip(weights, others) for w in pair),
+    )
+    hidden = shape((ROWS, 2 * H))
+    early, *hidden1 = call(
+        kernel_of(first_body, "first", flops=2**31, vmem=VM[0]),
+        (shape((4, SENT, 128)), hidden, hidden, hidden), lane, source, *pieces, *ordered,
+    )
+    rows, *hidden2 = call(
+        kernel_of(second_body, "second", flops=2**31, vmem=VM[0]),
+        (shape((8, SENT, 128)), hidden, hidden, hidden), lane, source, early, *nears, *ordered,
     )
     parts = lax.all_to_all(rows, GROUP, 0, 0, tiled=True)
     g_own, u_own, d_own, far = call(
-        kernel_of(weights_body, "weights", flops=2**31),
+        kernel_of(weights_body, "weights", flops=2**31, vmem=VM[1]),
         (shape((D, H), F32), shape((D, H), F32), shape((H, D), F32), shape((3, D, H))),
-        at, *pieces, scaled, ggp, gup,
+        *pieces, *nears, *hidden1, *hidden2,
     )
     far = lax.ppermute(far, "c", SWAP)
     gate_grad, up_grad, down_grad, squares, hid_sq = call(
-        kernel_of(sums_body, "sums", flops=2**29),
+        kernel_of(sums_body, "sums", flops=2**29, vmem=VM[2]),
         (
             shape((D, H)), shape((D, H)), shape((H, D)),
             shape((16, 8, 128), F32), shape((1, H), F32),
         ),
-        None, g_own, u_own, d_own, far,
+        g_own, u_own, d_own, far,
     )
     squares, parts = lax.optimization_barrier((squares, parts))
     squares = lax.all_to_all(squares, ("c",) + GROUP, 0, 0, tiled=True)
-    answer = call(kernel_of(back_body, "back"), shape((1024, 128)), None, back, parts, squares)
+    answer = call(kernel_of(back_body, "back"), shape((1024, 128)), back, parts, squares)
     got = lax.all_to_all(answer.reshape(SRC, 32, 128), HOMES, 0, 0, tiled=True)
     own, gate = call(
-        kernel_of(combine_body, "combine"), (shape((384, 128)), shape((2, T), F32)), None,
+        kernel_of(combine_body, "combine"), (shape((4, 384, 128)), shape((2, T), F32)),
         routing.T, gates.T, got.reshape(1024, 128),
     )
-    every = lax.all_gather(own, "tp", axis=0, tiled=True)
+    every = lax.all_to_all(own, "tp", 0, 0, tiled=True)
     token, norms = call(
-        kernel_of(final_body, "final"), (shape((T, D)), shape((EXPERTS, 2, D), F32)), None, every
+        kernel_of(final_body, "final"), (shape((T, D)), shape((EXPERTS, 2, D), F32)), every
     )
     return (
         token,

time: 161 us -> 152 us (0.944)
  local copies, waits for them, and re-layouts: 2.72 us -> 18.8 us
  Pallas kernels: 35.1 us -> 19.3 us
  waiting for transfers between devices: 26.8 us -> 18.5 us
  blocking collectives: 44.7 us -> 40.5 us
  starting transfers between devices: 49.3 us -> 52.6 us
    unnamed x32 -> x82, local copies, waits for them, and re-layouts: 2.72 us -> 18.8 us
    pallas_call x8 -> x10, Pallas kernels: 35.1 us -> 19.3 us  [call(): kernel(outs, [pl.BlockSpec(memory_space=pltpu.VMEM) for _ in args])(*args)]
    all_gather x1 -> x0, blocking collectives: 13.5 us -> none  [body(): every = lax.all_gather(own, 'tp', axis=0, tiled=True)]
    all_to_all x0 -> x1, blocking collectives: none -> 10.5 us  [body(): every = lax.all_to_all(own, 'tp', 0, 0, tiled=True)]
    ppermute x5, waiting for transfers between devices: 9.54 us -> 3.68 us  [turned(): return lax.ppermute(x, 'tp', [(i, (i + by) % 4) for i in range(4)])]
    ppermute x1, starting transfers between devices: 1.91 us -> 3.92 us  [body(): near2 = lax.ppermute(mine2, 'yp', SWAP)]
    all_to_all x1, starting transfers between devices: 3.6 us -> 5.47 us  [body(): parts = lax.all_to_all(rows, GROUP, 0, 0, tiled=True)]
  transfers between devices with their start and end apart: 13 -> 13, of which waited for: 8 -> 5; matrix products, arithmetic and copies ran while one was open for 0% -> 0% of each run, Pallas kernels for 8% -> 6%
where the time goes in v1:
time: 152 us; the launch traced here: 151 us
  starting transfers between devices  52.6 us (35%)
  blocking collectives  40.5 us (27%)
  Pallas kernels  19.3 us (13%)
  local copies, waits for them, and re-layouts  18.8 us (12%)
  waiting for transfers between devices  18.5 us (12%)
    pallas_call x10, Pallas kernels, call(): kernel(outs, [pl.BlockSpec(memory_space=pltpu.VMEM) for _ in args])(*args)  19.3 us
    all_to_all x1, blocking collectives, body(): got = lax.all_to_all(answer.reshape(SRC, 32, 128), HOMES, 0, 0, tiled=True)  19.1 us
    unnamed x82, local copies, waits for them, and re-layouts  18.8 us
    ppermute x5, starting transfers between devices, turned(): return lax.ppermute(x, 'tp', [(i, (i + by) % 4) for i in range(4)])  17 us
    all_to_all x1, starting transfers between devices, body(): moved = lax.all_to_all(sent.reshape(SRC, 48, 128), HOMES, 0, 0, tiled=True)  16.1 us
    all_to_all x1, blocking collectives, body(): squares = lax.all_to_all(squares, ('c',) + GROUP, 0, 0, tiled=True)  10.9 us
    all_to_all x1, blocking collectives, body(): every = lax.all_to_all(own, 'tp', 0, 0, tiled=True)  10.5 us
    all_to_all x1, waiting for transfers between devices, body(): moved = lax.all_to_all(sent.reshape(SRC, 48, 128), HOMES, 0, 0, tiled=True)  10.5 us
  transfers between devices with their start and end apart: 13, of which 5 were waited for; matrix products, arithmetic and copies ran while one was open for 0% of the time, Pallas kernels for 6%

profile of v1, /device:TPU:16, one launch (start us, length us, event | category | flops | bytes accessed | tf_op | source)
XLA Modules:
  0.0 150.8 jit_solution(2598348032464449926)
XLA Ops:
  0.7 1.1 copy-done.5
  1.7 0.9 copy-done.6
  2.7 0.7 copy-done.9
  4.0 2.6 %dispatch.1 = bf16[1536,128]{1,0:T(8,128)(2,1)} custom-call(s32[2,128]{1,0:T(2,128)S(1)} %bitcast.22, bf16[2,128]{1,0:T(2,128)(2,1)S(1)} %bitcast.24, bf16[128,1024]{1,0:T(8,128)(2,1)S(1)} %copy-done.5, bf16[128,1024]{1,0:T(8,128)(2,1)S(1)} %copy-done.6), custom_call_target="tpu_custom_call" | custom-call | flops 134217728 | bytes 1048576 | tf_op jit(solution)/shard_map/dispatch/pallas_call | solution.py:37
  6.6 16.1 %all-to-all-start = ((bf16[32,48,128]{2,1,0:T(8,128)(2,1)}), bf16[32,48,128]{2,1,0:T(8,128)(2,1)S(1)}, u32[]{:S(2)}, u32[]{:S(2)}) async-start(bf16[32,48,128]{2,1,0:T(8,128)(2,1)} %bitcast.2), calls=%async_computation | async-start | bytes 786432 | tf_op jit(solution)/shard_map/all_to_all | solution.py:297
  22.7 1.9 %collective-permute-start.7 = (bf16[1024,256]{1,0:T(8,128)(2,1)S(1)}, bf16[1024,256]{1,0:T(8,128)(2,1)S(1)}, u32[]{:S(2)}, u32[]{:S(2)}) collective-permute-start(bf16[1024,256]{1,0:T(8,128)(2,1)S(1)} %bitcast.15), channel_id=1, source_target_pairs={{0,4},{4,0},{1,5},{5,1},{2,6},{6,2},{3,7},{7,3},{8,12},{12,8},{9,1... | collective-permute-start | bytes 1572872 | tf_op jit(solution)/shard_map/ppermute | solution.py:296
  24.6 2.4 %collective-permute-start.8 = (bf16[1024,256]{1,0:T(8,128)(2,1)S(1)}, bf16[1024,256]{1,0:T(8,128)(2,1)S(1)}, u32[]{:S(2)}, u32[]{:S(2)}) collective-permute-start(bf16[1024,256]{1,0:T(8,128)(2,1)S(1)} %bitcast.17), channel_id=1, source_target_pairs={{0,4},{4,0},{1,5},{5,1},{2,6},{6,2},{3,7},{7,3},{8,12},{12,8},{9,1... | collective-permute-start | bytes 1572872 | tf_op jit(solution)/shard_map/ppermute | solution.py:296
  27.0 1.9 %collective-permute-start.9 = (bf16[256,1024]{1,0:T(8,128)(2,1)S(1)}, bf16[256,1024]{1,0:T(8,128)(2,1)S(1)}, u32[]{:S(2)}, u32[]{:S(2)}) collective-permute-start(bf16[256,1024]{1,0:T(8,128)(2,1)S(1)} %bitcast.19), channel_id=1, source_target_pairs={{0,4},{4,0},{1,5},{5,1},{2,6},{6,2},{3,7},{7,3},{8,12},{12,8},{9,1... | collective-permute-start | bytes 1572872 | tf_op jit(solution)/shard_map/ppermute | solution.py:296
  28.9 10.5 %all-to-all-done = bf16[32,48,128]{2,1,0:T(8,128)(2,1)S(1)} async-done(((bf16[32,48,128]{2,1,0:T(8,128)(2,1)}), bf16[32,48,128]{2,1,0:T(8,128)(2,1)S(1)}, u32[]{:S(2)}, u32[]{:S(2)}) %all-to-all-start) | async-done | bytes 393248 | tf_op jit(solution)/shard_map/all_to_all | solution.py:297
  39.4 0.9 copy-done.8
  40.7 2.1 %collective-permute-start.3 = (bf16[1536,128]{1,0:T(8,128)(2,1)S(1)}, bf16[1536,128]{1,0:T(8,128)(2,1)S(1)}, u32[]{:S(2)}, u32[]{:S(2)}) collective-permute-start(bf16[1536,128]{1,0:T(8,128)(2,1)S(1)} %regroup.1.refs_0_), channel_id=1, source_target_pairs={{0,8},{8,0},{1,9},{9,1},{2,10},{10,2},{3,11},{11,3},{4,12},{12,4},... | collective-permute-start | bytes 1179656 | tf_op jit(solution)/shard_map/ppermute | solution.py:302
  42.8 4.9 %collective-permute-start.2 = (bf16[1536,128]{1,0:T(8,128)(2,1)S(1)}, bf16[1536,128]{1,0:T(8,128)(2,1)S(1)}, u32[]{:S(2)}, u32[]{:S(2)}) collective-permute-start(bf16[1536,128]{1,0:T(8,128)(2,1)S(1)} %regroup.1.refs_0_), channel_id=1, source_target_pairs={{0,2},{1,3},{2,0},{3,1},{4,6},{5,7},{6,4},{7,5},{8,10},{9,11},{10,... | collective-permute-start | bytes 1179656 | tf_op jit(solution)/shard_map/ppermute | solution.py:286
  47.7 3.1 %collective-permute-start.1 = (bf16[1536,128]{1,0:T(8,128)(2,1)S(1)}, bf16[1536,128]{1,0:T(8,128)(2,1)S(1)}, u32[]{:S(2)}, u32[]{:S(2)}) collective-permute-start(bf16[1536,128]{1,0:T(8,128)(2,1)S(1)} %regroup.1.refs_0_), channel_id=1, source_target_pairs={{0,3},{1,0},{2,1},{3,2},{4,7},{5,4},{6,5},{7,6},{8,11},{9,8},{10,9... | collective-permute-start | bytes 1179656 | tf_op jit(solution)/shard_map/ppermute | solution.py:286
  50.8 2.8 %collective-permute-start = (bf16[1536,128]{1,0:T(8,128)(2,1)S(1)}, bf16[1536,128]{1,0:T(8,128)(2,1)S(1)}, u32[]{:S(2)}, u32[]{:S(2)}) collective-permute-start(bf16[1536,128]{1,0:T(8,128)(2,1)S(1)} %regroup.1.refs_0_), channel_id=1, source_target_pairs={{0,1},{1,2},{2,3},{3,0},{4,5},{5,6},{6,7},{7,4},{8,9},{9,10},{10,1... | collective-permute-start | bytes 1179656 | tf_op jit(solution)/shard_map/ppermute | solution.py:286
  53.6 4.3 %collective-permute-start.5 = (bf16[1536,128]{1,0:T(8,128)(2,1)S(1)}, bf16[1536,128]{1,0:T(8,128)(2,1)S(1)}, u32[]{:S(2)}, u32[]{:S(2)}) collective-permute-start(bf16[1536,128]{1,0:T(8,128)(2,1)S(1)} %collective-permute-done.3.refs_0_.refs_4_), channel_id=1, source_target_pairs={{0,3},{1,0},{2,1},{3,2},{4,7},{5,4},{6,5},{7,6},{8,11},{9,8},{10,9... | collective-permute-start | bytes 1179656 | tf_op jit(solution)/shard_map/ppermute | solution.py:286
  57.9 1.9 %collective-permute-start.4 = (bf16[1536,128]{1,0:T(8,128)(2,1)S(1)}, bf16[1536,128]{1,0:T(8,128)(2,1)S(1)}, u32[]{:S(2)}, u32[]{:S(2)}) collective-permute-start(bf16[1536,128]{1,0:T(8,128)(2,1)S(1)} %collective-permute-done.3.refs_0_.refs_4_), channel_id=1, source_target_pairs={{0,1},{1,2},{2,3},{3,0},{4,5},{5,6},{6,7},{7,4},{8,9},{9,10},{10,1... | collective-permute-start | bytes 1179656 | tf_op jit(solution)/shard_map/ppermute | solution.py:286
  59.8 3.9 %collective-permute-start.6 = (bf16[1536,128]{1,0:T(8,128)(2,1)S(1)}, bf16[1536,128]{1,0:T(8,128)(2,1)S(1)}, u32[]{:S(2)}, u32[]{:S(2)}) collective-permute-start(bf16[1536,128]{1,0:T(8,128)(2,1)S(1)} %collective-permute-done.2.refs_3_), channel_id=1, source_target_pairs={{0,8},{8,0},{1,9},{9,1},{2,10},{10,2},{3,11},{11,3},{4,12},{12,4},... | collective-permute-start | bytes 1179656 | tf_op jit(solution)/shard_map/ppermute | solution.py:304
  64.1 2.6 %collective-permute-done.1.refs_2_ = bf16[1536,128]{1,0:T(8,128)(2,1)S(1)} collective-permute-done((bf16[1536,128]{1,0:T(8,128)(2,1)S(1)}, bf16[1536,128]{1,0:T(8,128)(2,1)S(1)}, u32[]{:S(2)}, u32[]{:S(2)}) %collective-permute-start.1) | collective-permute-done | bytes 393248 | tf_op jit(solution)/shard_map/ppermute | solution.py:286
  66.7 3.5 %first.1 = (bf16[4,800,128]{2,1,0:T(8,128)(2,1)S(1)}, bf16[384,512]{1,0:T(8,128)(2,1)S(1)}, bf16[384,512]{1,0:T(8,128)(2,1)S(1)}, bf16[384,512]{1,0:T(8,128)(2,1)S(1)}) custom-call(bf16[192,128]{1,0:T(8,128)(2,1)S(1)} %copy-done.27, bf16[16,192]{1,0:T(8,128)(2,1)S(1)} %copy-done.28, bf16[1536,128]{1,0:T(8,128)(2,1)S(1)} %regroup.1.refs_0_, ...), custom_call_target="tpu_custom_call" | custom-call | flops 2147483648 | bytes 1048576 | tf_op jit(solution)/shard_map/first/pallas_call | solution.py:37
  70.3 0.7 copy-done.35
  71.0 0.8 copy-done.37
  71.8 0.8 copy-done.39
  72.6 1.0 collective-permute-done.5.refs_2_.refs_6_
  73.6 4.8 %second.1 = (bf16[8,800,128]{2,1,0:T(8,128)(2,1)}, bf16[384,512]{1,0:T(8,128)(2,1)S(1)}, bf16[384,512]{1,0:T(8,128)(2,1)S(1)}, bf16[384,512]{1,0:T(8,128)(2,1)S(1)}) custom-call(bf16[192,128]{1,0:T(8,128)(2,1)S(1)} %copy-done.27, bf16[16,192]{1,0:T(8,128)(2,1)S(1)} %copy-done.28, bf16[4,800,128]{2,1,0:T(8,128)(2,1)S(1)} %get-tuple-element.39.early, ...), custom_call_target="tpu_custom_call" | custom-call | flops 2147483648 | bytes 1048576 | tf_op jit(solution)/shard_map/second/pallas_call | solution.py:37
  78.4 0.8 copy-done.29
  79.2 0.8 copy-done.31
  79.9 0.8 copy-done.33
  80.7 5.5 %all-to-all-start.1 = ((bf16[8,800,128]{2,1,0:T(8,128)(2,1)}), bf16[8,800,128]{2,1,0:T(8,128)(2,1)S(1)}, u32[]{:S(2)}, u32[]{:S(2)}) async-start(bf16[8,800,128]{2,1,0:T(8,128)(2,1)} %get-tuple-element.48), calls=%async_computation.1 | async-start | bytes 3276800 | tf_op jit(solution)/shard_map/all_to_all | solution.py:321
  86.2 1.0 copy-done.20
  87.2 1.0 copy-done.22
  88.2 1.0 copy-done.24
  89.2 1.0 copy-done.26
  90.2 1.0 copy-done.30
  91.2 1.0 copy-done.32
  92.2 1.0 copy-done.34
  93.2 1.0 copy-done.36
  94.2 1.0 copy-done.38
  95.2 1.0 copy-done.40
  96.2 3.4 %weights.1 = (f32[1024,256]{1,0:T(8,128)S(1)}, f32[1024,256]{1,0:T(8,128)S(1)}, f32[256,1024]{1,0:T(8,128)S(1)}, bf16[3,1024,256]{2,1,0:T(8,128)(2,1)S(1)}) custom-call(bf16[1536,128]{1,0:T(8,128)(2,1)S(1)} %copy-done.4, bf16[1536,128]{1,0:T(8,128)(2,1)S(1)} %copy-done.20, bf16[1536,128]{1,0:T(8,128)(2,1)S(1)} %copy-done.18, ...), custom_call_target="tpu_custom_call" | custom-call | flops 2147483648 | bytes 1048576 | tf_op jit(solution)/shard_map/weights/pallas_call | solution.py:37
  99.6 1.9 %collective-permute-start.10 = (bf16[3,1024,256]{2,1,0:T(8,128)(2,1)S(1)}, bf16[3,1024,256]{2,1,0:T(8,128)(2,1)S(1)}, u32[]{:S(2)}, u32[]{:S(2)}) collective-permute-start(bf16[3,1024,256]{2,1,0:T(8,128)(2,1)S(1)} %get-tuple-element.46), channel_id=1, source_target_pairs={{0,4},{4,0},{1,5},{5,1},{2,6},{6,2},{3,7},{7,3},{8,12},{12,8},{9,1... | collective-permute-start | bytes 4718600 | tf_op jit(solution)/shard_map/ppermute | solution.py:327
  101.6 3.4 %collective-permute-done.10.far = bf16[3,1024,256]{2,1,0:T(8,128)(2,1)S(1)} collective-permute-done((bf16[3,1024,256]{2,1,0:T(8,128)(2,1)S(1)}, bf16[3,1024,256]{2,1,0:T(8,128)(2,1)S(1)}, u32[]{:S(2)}, u32[]{:S(2)}) %collective-permute-start.10) | collective-permute-done | bytes 1572896 | tf_op jit(solution)/shard_map/ppermute | solution.py:327
  104.9 1.5 %sums.1 = (bf16[1024,256]{1,0:T(8,128)(2,1)}, bf16[1024,256]{1,0:T(8,128)(2,1)}, bf16[256,1024]{1,0:T(8,128)(2,1)}, f32[16,8,128]{2,1,0:T(8,128)S(1)}, f32[1,256]{1,0:T(1,128)}) custom-call(f32[1024,256]{1,0:T(8,128)S(1)} %get-tuple-element.43.g_own, f32[1024,256]{1,0:T(8,128)S(1)} %get-tuple-element.44.u_own, f32[256,1024]{1,0:T(8,128)S(1)} %get-tuple-element.45.d_own, ...), custom_call_target="tpu_custom_call" | custom-call | flops 536870912 | bytes 1048576 | tf_op jit(solution)/shard_map/sums/pallas_call | solution.py:37
  106.5 1.0 all-to-all-done.1.parts
  107.5 10.9 %all_to_all.25.squares = f32[16,8,128]{2,1,0:T(8,128)S(1)} all-to-all(f32[16,8,128]{2,1,0:T(8,128)S(1)} %get-tuple-element.50), channel_id=1, replica_groups=mesh['z'=8,'yh'=4,'yp'=2,'c'=2,'tp'=4] {'c','yp','tp'}, dimensions={0} | all-to-all | bytes 131072 | tf_op jit(solution)/shard_map/all_to_all | solution.py:337
  118.8 19.1 %all_to_all.26 = bf16[32,32,128]{2,1,0:T(8,128)(2,1)S(1)} all-to-all(bf16[32,32,128]{2,1,0:T(8,128)(2,1)S(1)} %bitcast.14), channel_id=1, replica_groups=mesh['z'=8,'yh'=4,'yp'=2,'c'=2,'tp'=4] {'z','yh'}, dimensions={0} | all-to-all | bytes 524288 | tf_op jit(solution)/shard_map/all_to_all | solution.py:339
  137.9 1.5 combine.1
  139.4 10.5 %all_to_all.27.got = bf16[4,384,128]{2,1,0:T(8,128)(2,1)S(1)} all-to-all(bf16[4,384,128]{2,1,0:T(8,128)(2,1)S(1)} %get-tuple-element.51), channel_id=1, replica_groups=mesh['z'=8,'yh'=4,'yp'=2,'c'=2,'tp'=4] {'tp'}, dimensions={0} | all-to-all | bytes 786432 | tf_op jit(solution)/shard_map/all_to_all | solution.py:344
  149.9 0.9 final.1
  (73 shorter events, 1.9 us)
Async XLA Ops:
  0.6 22.0 %copy-start = (bf16[1,1024,256]{2,1,0:T(8,128)(2,1)S(1)}, bf16[1,1024,256]{2,1,0:T(8,128)(2,1)}, u32[]{:S(2)}) copy-start(bf16[1,1024,256]{2,1,0:T(8,128)(2,1)} %param.15) | copy-start | bytes 1572868
  0.6 23.9 %copy-start.1 = (bf16[1,1024,256]{2,1,0:T(8,128)(2,1)S(1)}, bf16[1,1024,256]{2,1,0:T(8,128)(2,1)}, u32[]{:S(2)}) copy-start(bf16[1,1024,256]{2,1,0:T(8,128)(2,1)} %param.16) | copy-start | bytes 1572868
  0.7 26.4 %copy-start.2 = (bf16[1,256,1024]{2,1,0:T(8,128)(2,1)S(1)}, bf16[1,256,1024]{2,1,0:T(8,128)(2,1)}, u32[]{:S(2)}) copy-start(bf16[1,256,1024]{2,1,0:T(8,128)(2,1)} %param.17) | copy-start | bytes 1572868
  0.7 1.1 copy-start.5
  1.7 0.9 copy-start.6
  6.6 32.8 %all-to-all-start = ((bf16[32,48,128]{2,1,0:T(8,128)(2,1)}), bf16[32,48,128]{2,1,0:T(8,128)(2,1)S(1)}, u32[]{:S(2)}, u32[]{:S(2)}) async-start(bf16[32,48,128]{2,1,0:T(8,128)(2,1)} %bitcast.2), calls=%async_computation | async-start | bytes 786432 | tf_op jit(solution)/shard_map/all_to_all | solution.py:297
  22.7 25.1 %collective-permute-start.7 = (bf16[1024,256]{1,0:T(8,128)(2,1)S(1)}, bf16[1024,256]{1,0:T(8,128)(2,1)S(1)}, u32[]{:S(2)}, u32[]{:S(2)}) collective-permute-start(bf16[1024,256]{1,0:T(8,128)(2,1)S(1)} %bitcast.15), channel_id=1, source_target_pairs={{0,4},{4,0},{1,5},{5,1},{2,6},{6,2},{3,7},{7,3},{8,12},{12,8},{9,1... | collective-permute-start | bytes 1572872 | tf_op jit(solution)/shard_map/ppermute | solution.py:296
  24.6 26.2 %collective-permute-start.8 = (bf16[1024,256]{1,0:T(8,128)(2,1)S(1)}, bf16[1024,256]{1,0:T(8,128)(2,1)S(1)}, u32[]{:S(2)}, u32[]{:S(2)}) collective-permute-start(bf16[1024,256]{1,0:T(8,128)(2,1)S(1)} %bitcast.17), channel_id=1, source_target_pairs={{0,4},{4,0},{1,5},{5,1},{2,6},{6,2},{3,7},{7,3},{8,12},{12,8},{9,1... | collective-permute-start | bytes 1572872 | tf_op jit(solution)/shard_map/ppermute | solution.py:296
  27.0 30.9 %collective-permute-start.9 = (bf16[256,1024]{1,0:T(8,128)(2,1)S(1)}, bf16[256,1024]{1,0:T(8,128)(2,1)S(1)}, u32[]{:S(2)}, u32[]{:S(2)}) collective-permute-start(bf16[256,1024]{1,0:T(8,128)(2,1)S(1)} %bitcast.19), channel_id=1, source_target_pairs={{0,4},{4,0},{1,5},{5,1},{2,6},{6,2},{3,7},{7,3},{8,12},{12,8},{9,1... | collective-permute-start | bytes 1572872 | tf_op jit(solution)/shard_map/ppermute | solution.py:296
  39.4 0.9 copy-start.8
  40.7 29.6 %copy-start.3 = (bf16[1536,128]{1,0:T(8,128)(2,1)}, bf16[1536,128]{1,0:T(8,128)(2,1)S(1)}, u32[]{:S(2)}) copy-start(bf16[1536,128]{1,0:T(8,128)(2,1)S(1)} %regroup.1.refs_0_) | copy-start | bytes 1179652
  40.7 26.0 %copy-start.27 = (bf16[192,128]{1,0:T(8,128)(2,1)S(1)}, bf16[192,128]{1,0:T(8,128)(2,1)}, u32[]{:S(2)}) copy-start(bf16[192,128]{1,0:T(8,128)(2,1)} %constant.9.clone.lane) | copy-start | bytes 147460
  40.7 26.0 %copy-start.28 = (bf16[16,192]{1,0:T(8,128)(2,1)S(1)}, bf16[16,192]{1,0:T(8,128)(2,1)}, u32[]{:S(2)}) copy-start(bf16[16,192]{1,0:T(8,128)(2,1)} %constant.10.clone.source) | copy-start | bytes 18436
  40.7 12.9 %collective-permute-start.3 = (bf16[1536,128]{1,0:T(8,128)(2,1)S(1)}, bf16[1536,128]{1,0:T(8,128)(2,1)S(1)}, u32[]{:S(2)}, u32[]{:S(2)}) collective-permute-start(bf16[1536,128]{1,0:T(8,128)(2,1)S(1)} %regroup.1.refs_0_), channel_id=1, source_target_pairs={{0,8},{8,0},{1,9},{9,1},{2,10},{10,2},{3,11},{11,3},{4,12},{12,4},... | collective-permute-start | bytes 1179656 | tf_op jit(solution)/shard_map/ppermute | solution.py:302
  42.8 17.0 %collective-permute-start.2 = (bf16[1536,128]{1,0:T(8,128)(2,1)S(1)}, bf16[1536,128]{1,0:T(8,128)(2,1)S(1)}, u32[]{:S(2)}, u32[]{:S(2)}) collective-permute-start(bf16[1536,128]{1,0:T(8,128)(2,1)S(1)} %regroup.1.refs_0_), channel_id=1, source_target_pairs={{0,2},{1,3},{2,0},{3,1},{4,6},{5,7},{6,4},{7,5},{8,10},{9,11},{10,... | collective-permute-start | bytes 1179656 | tf_op jit(solution)/shard_map/ppermute | solution.py:286
  47.7 19.0 %collective-permute-start.1 = (bf16[1536,128]{1,0:T(8,128)(2,1)S(1)}, bf16[1536,128]{1,0:T(8,128)(2,1)S(1)}, u32[]{:S(2)}, u32[]{:S(2)}) collective-permute-start(bf16[1536,128]{1,0:T(8,128)(2,1)S(1)} %regroup.1.refs_0_), channel_id=1, source_target_pairs={{0,3},{1,0},{2,1},{3,2},{4,7},{5,4},{6,5},{7,6},{8,11},{9,8},{10,9... | collective-permute-start | bytes 1179656 | tf_op jit(solution)/shard_map/ppermute | solution.py:286
  50.8 15.9 %collective-permute-start = (bf16[1536,128]{1,0:T(8,128)(2,1)S(1)}, bf16[1536,128]{1,0:T(8,128)(2,1)S(1)}, u32[]{:S(2)}, u32[]{:S(2)}) collective-permute-start(bf16[1536,128]{1,0:T(8,128)(2,1)S(1)} %regroup.1.refs_0_), channel_id=1, source_target_pairs={{0,1},{1,2},{2,3},{3,0},{4,5},{5,6},{6,7},{7,4},{8,9},{9,10},{10,1... | collective-permute-start | bytes 1179656 | tf_op jit(solution)/shard_map/ppermute | solution.py:286
  53.6 20.0 %copy-start.13 = (bf16[1536,128]{1,0:T(8,128)(2,1)}, bf16[1536,128]{1,0:T(8,128)(2,1)S(1)}, u32[]{:S(2)}) copy-start(bf16[1536,128]{1,0:T(8,128)(2,1)S(1)} %collective-permute-done.3.refs_0_.refs_4_) | copy-start | bytes 1179652
  53.6 20.0 %collective-permute-start.5 = (bf16[1536,128]{1,0:T(8,128)(2,1)S(1)}, bf16[1536,128]{1,0:T(8,128)(2,1)S(1)}, u32[]{:S(2)}, u32[]{:S(2)}) collective-permute-start(bf16[1536,128]{1,0:T(8,128)(2,1)S(1)} %collective-permute-done.3.refs_0_.refs_4_), channel_id=1, source_target_pairs={{0,3},{1,0},{2,1},{3,2},{4,7},{5,4},{6,5},{7,6},{8,11},{9,8},{10,9... | collective-permute-start | bytes 1179656 | tf_op jit(solution)/shard_map/ppermute | solution.py:286
  57.9 15.7 %collective-permute-start.4 = (bf16[1536,128]{1,0:T(8,128)(2,1)S(1)}, bf16[1536,128]{1,0:T(8,128)(2,1)S(1)}, u32[]{:S(2)}, u32[]{:S(2)}) collective-permute-start(bf16[1536,128]{1,0:T(8,128)(2,1)S(1)} %collective-permute-done.3.refs_0_.refs_4_), channel_id=1, source_target_pairs={{0,1},{1,2},{2,3},{3,0},{4,5},{5,6},{6,7},{7,4},{8,9},{9,10},{10,1... | collective-permute-start | bytes 1179656 | tf_op jit(solution)/shard_map/ppermute | solution.py:286
  59.8 10.4 %copy-start.15 = (bf16[1536,128]{1,0:T(8,128)(2,1)}, bf16[1536,128]{1,0:T(8,128)(2,1)S(1)}, u32[]{:S(2)}) copy-start(bf16[1536,128]{1,0:T(8,128)(2,1)S(1)} %collective-permute-done.2.refs_3_) | copy-start | bytes 1179652
  59.8 13.8 %collective-permute-start.6 = (bf16[1536,128]{1,0:T(8,128)(2,1)S(1)}, bf16[1536,128]{1,0:T(8,128)(2,1)S(1)}, u32[]{:S(2)}, u32[]{:S(2)}) collective-permute-start(bf16[1536,128]{1,0:T(8,128)(2,1)S(1)} %collective-permute-done.2.refs_3_), channel_id=1, source_target_pairs={{0,8},{8,0},{1,9},{9,1},{2,10},{10,2},{3,11},{11,3},{4,12},{12,4},... | collective-permute-start | bytes 1179656 | tf_op jit(solution)/shard_map/ppermute | solution.py:304
  66.7 3.6 %copy-start.17 = (bf16[1536,128]{1,0:T(8,128)(2,1)}, bf16[1536,128]{1,0:T(8,128)(2,1)S(1)}, u32[]{:S(2)}) copy-start(bf16[1536,128]{1,0:T(8,128)(2,1)S(1)} %collective-permute-done.1.refs_2_) | copy-start | bytes 1179652
  66.7 3.6 %copy-start.19 = (bf16[1536,128]{1,0:T(8,128)(2,1)}, bf16[1536,128]{1,0:T(8,128)(2,1)S(1)}, u32[]{:S(2)}) copy-start(bf16[1536,128]{1,0:T(8,128)(2,1)S(1)} %collective-permute-done.refs_1_) | copy-start | bytes 1179652
  71.8 0.8 copy-start.39
  73.6 4.8 %copy-start.21 = (bf16[1536,128]{1,0:T(8,128)(2,1)}, bf16[1536,128]{1,0:T(8,128)(2,1)S(1)}, u32[]{:S(2)}) copy-start(bf16[1536,128]{1,0:T(8,128)(2,1)S(1)} %collective-permute-done.5.refs_2_.refs_6_) | copy-start | bytes 1179652
  73.6 4.8 %copy-start.23 = (bf16[1536,128]{1,0:T(8,128)(2,1)}, bf16[1536,128]{1,0:T(8,128)(2,1)S(1)}, u32[]{:S(2)}) copy-start(bf16[1536,128]{1,0:T(8,128)(2,1)S(1)} %collective-permute-done.4.refs_1_.refs_5_) | copy-start | bytes 1179652
  73.6 4.8 %copy-start.25 = (bf16[1536,128]{1,0:T(8,128)(2,1)}, bf16[1536,128]{1,0:T(8,128)(2,1)S(1)}, u32[]{:S(2)}) copy-start(bf16[1536,128]{1,0:T(8,128)(2,1)S(1)} %collective-permute-done.6.refs_3_.refs_7_) | copy-start | bytes 1179652
  79.2 0.8 copy-start.31
  80.7 5.5 %copy-start.4 = (bf16[1536,128]{1,0:T(8,128)(2,1)S(1)}, bf16[1536,128]{1,0:T(8,128)(2,1)}, u32[]{:S(2)}) copy-start(bf16[1536,128]{1,0:T(8,128)(2,1)} %copy-done.3) | copy-start | bytes 1179652
  80.7 5.5 %copy-start.14 = (bf16[1536,128]{1,0:T(8,128)(2,1)S(1)}, bf16[1536,128]{1,0:T(8,128)(2,1)}, u32[]{:S(2)}) copy-start(bf16[1536,128]{1,0:T(8,128)(2,1)} %copy-done.13) | copy-start | bytes 1179652
  80.7 5.5 %copy-start.16 = (bf16[1536,128]{1,0:T(8,128)(2,1)S(1)}, bf16[1536,128]{1,0:T(8,128)(2,1)}, u32[]{:S(2)}) copy-start(bf16[1536,128]{1,0:T(8,128)(2,1)} %copy-done.15) | copy-start | bytes 1179652
  80.7 5.5 %copy-start.18 = (bf16[1536,128]{1,0:T(8,128)(2,1)S(1)}, bf16[1536,128]{1,0:T(8,128)(2,1)}, u32[]{:S(2)}) copy-start(bf16[1536,128]{1,0:T(8,128)(2,1)} %copy-done.17) | copy-start | bytes 1179652
  80.7 26.7 %all-to-all-start.1 = ((bf16[8,800,128]{2,1,0:T(8,128)(2,1)}), bf16[8,800,128]{2,1,0:T(8,128)(2,1)S(1)}, u32[]{:S(2)}, u32[]{:S(2)}) async-start(bf16[8,800,128]{2,1,0:T(8,128)(2,1)} %get-tuple-element.48), calls=%async_computation.1 | async-start | bytes 3276800 | tf_op jit(solution)/shard_map/all_to_all | solution.py:321
  86.2 1.0 copy-start.20
  87.2 1.0 copy-start.22
  88.2 1.0 copy-start.24
  89.2 1.0 copy-start.26
  90.2 1.0 copy-start.30
  91.2 1.0 copy-start.32
  92.2 1.0 copy-start.34
  93.2 1.0 copy-start.36
  94.2 1.0 copy-start.38
  95.2 1.0 copy-start.40
  99.6 5.3 %collective-permute-start.10 = (bf16[3,1024,256]{2,1,0:T(8,128)(2,1)S(1)}, bf16[3,1024,256]{2,1,0:T(8,128)(2,1)S(1)}, u32[]{:S(2)}, u32[]{:S(2)}) collective-permute-start(bf16[3,1024,256]{2,1,0:T(8,128)(2,1)S(1)} %get-tuple-element.46), channel_id=1, source_target_pairs={{0,4},{4,0},{1,5},{5,1},{2,6},{6,2},{3,7},{7,3},{8,12},{12,8},{9,1... | collective-permute-start | bytes 4718600 | tf_op jit(solution)/shard_map/ppermute | solution.py:327
  104.9 13.5 %copy-start.7 = (bf16[256,208]{1,0:T(8,128)(2,1)S(1)}, bf16[256,208]{1,0:T(8,128)(2,1)}, u32[]{:S(2)}) copy-start(bf16[256,208]{1,0:T(8,128)(2,1)} %constant.11.clone.order) | copy-start | bytes 319492
  106.5 31.4 %copy-start.10 = (s32[128,2]{0,1:T(2,128)S(1)}, s32[128,2]{0,1:T(2,128)}, u32[]{:S(2)}) copy-start(s32[128,2]{0,1:T(2,128)} %param.13) | copy-start | bytes 3076
  106.5 31.4 %copy-start.12 = (bf16[128,2]{0,1:T(2,128)(2,1)S(1)}, bf16[128,2]{0,1:T(2,128)(2,1)}, u32[]{:S(2)}) copy-start(bf16[128,2]{0,1:T(2,128)(2,1)} %param.14) | copy-start | bytes 1540
  (6 other events, 4.4 us)

commit v2 on v1

--- a/solution.py
+++ b/solution.py
@@ -16,9 +16,7 @@
 EXPERTS, SLOTS, SRC = 32, 12, 32
 ROWS = SRC * SLOTS
 CH = 192
-ALL = 2 * ROWS
-SENT = 2 * ROWS + SRC
-VM = (8, 8, 8)
+PART = 2 * CH + 16
 TURNS = (0, 3, 1, 2)
 NN = (((1,), (0,)), ((), ()))
 NT = (((1,), (1,)), ((), ()))
@@ -33,45 +31,48 @@
     return lax.broadcasted_iota(jnp.int32, shape, dim)
 
 
-def call(kernel, outs, *args):
-    return kernel(outs, [pl.BlockSpec(memory_space=pltpu.VMEM) for _ in args])(*args)
-
-
-def kernel_of(body, name, flops=2**27, vmem=4):
-    def build(outs, specs):
-        return pl.pallas_call(
-            body,
-            out_shape=outs,
-            in_specs=specs,
-            out_specs=jax.tree.map(lambda _: pl.BlockSpec(memory_space=pltpu.VMEM), outs),
-            compiler_params=pltpu.CompilerParams(vmem_limit_bytes=vmem * 1024 * 1024),
-            cost_estimate=pl.CostEstimate(flops=flops, transcendentals=0, bytes_accessed=2**20),
-            name=name,
-        )
-
-    return build
+def kernel(body, name, outs, *args, flops=2**27, vmem=4, spaces=None, out_spaces=None, scratch=(), alias=None):
+    vm = pltpu.VMEM
+    one = not isinstance(outs, tuple)
+    out_spaces = out_spaces or [vm] * (1 if one else len(outs))
+    out_specs = tuple(pl.BlockSpec(memory_space=m) for m in out_spaces)
+    return pl.pallas_call(
+        body,
+        out_shape=outs,
+        in_specs=[pl.BlockSpec(memory_space=m) for m in (spaces or [vm] * len(args))],
+        out_specs=out_specs[0] if one else out_specs,
+        scratch_shapes=list(scratch),
+        input_output_aliases=alias or {},
+        compiler_params=pltpu.CompilerParams(vmem_limit_bytes=vmem * 1024 * 1024),
+        cost_estimate=pl.CostEstimate(flops=flops, transcendentals=0, bytes_accessed=2**20),
+        name=name,
+    )(*args)
 
 
 def shape(dims, dtype=BF):
     return jax.ShapeDtypeStruct(dims, dtype)
 
 
-def tables():
-    o = np.arange(192)
-    regroup = (o % 48 // 12 * 48 + o // 48 * 12 + o % 12)[:, None] == np.arange(192)[None, :]
-    r = np.arange(CH)
-    lane = (r % SLOTS)[:, None] == np.arange(128)[None, :]
-    source = np.arange(16)[:, None] == (r // SLOTS)[None, :]
-    j = np.arange(256)
-    src, row = j // 32, j % 32
-    at = np.where(row < 24, row // 12 * 96 + src * 12 + row % 12, 200 + row - 25)
-    at = np.where(row == 24, 192 + src, at)
-    back = (at[:, None] == np.arange(208)[None, :]) & (row < 29)[:, None]
-    return tuple(jnp.asarray(a.astype(np.float32), BF) for a in (regroup, lane, source, back))
-
-
-def dispatch_body(rt, gt, tok, cot, out):
-    x = lax.axis_index("tp")
+def twelfths(n):
+    return (n * 171) >> 11
+
+
+def ones_where(hit):
+    return jnp.where(hit, 1.0, 0.0).astype(BF)
+
+
+def dispatch_body(rt_in, gt_in, tok_in, cot_in, out, rt, gt, tok, cot, sems):
+    cols = pl.ds(pl.multiple_of(lax.axis_index("tp") * H, H), H)
+    moves = [
+        pltpu.make_async_copy(src, dst, sems.at[n])
+        for n, (src, dst) in enumerate(
+            ((rt_in, rt), (gt_in, gt), (tok_in.at[:, cols], tok), (cot_in.at[:, cols], cot))
+        )
+    ]
+    for move in moves:
+        move.start()
+    for move in moves:
+        move.wait()
     r0, r1 = rt[0:1, :], rt[1:2, :]
     g0, g1 = gt[0:1, :].astype(F32), gt[1:2, :].astype(F32)
     e = iota((EXPERTS, T), 0)
@@ -85,7 +86,7 @@
         row = iota((192, T), 0) + i * 192
         total = jnp.zeros((192, 128), F32)
         for half in range(2):
-            cols = pl.ds(pl.multiple_of((x * 2 + half) * 128, 128), 128)
+            cols = slice(half * 128, (half + 1) * 128)
             for kind in range(2):
                 off = kind * 24 + half * 12
                 hit0, hit1 = row == base0 + off, row == base1 + off
@@ -101,9 +102,14 @@
     lax.fori_loop(0, 8, step, 0)
 
 
-def regroup_body(order, rows, out):
+def regroup_body(rows, out):
+    o, i = iota((192, 192), 0), iota((192, 192), 1)
+    k = (o >= 48).astype(jnp.int32) + (o >= 96).astype(jnp.int32) + (o >= 144).astype(jnp.int32)
+    rest = o - k * 48
+    src = twelfths(rest)
+    order = ones_where(i == src * 48 + k * 12 + rest - src * 12)
     for b in range(8):
-        moved = dot(order[...], rows[b * 192 : (b + 1) * 192, :]).astype(BF)
+        moved = dot(order, rows[b * 192 : (b + 1) * 192, :]).astype(BF)
         for k in range(4):
             out[k * ROWS + b * 48 : k * ROWS + (b + 1) * 48, :] = moved[k * 48 : (k + 1) * 48]
 
@@ -136,64 +142,87 @@
     return jnp.concatenate(cols, axis=1)
 
 
-def expert_rows(pieces, lane, source, pg, pu, pd, out, group, scaled_o, ggp_o, gup_o):
-    def step(i, carry):
-        first = pl.multiple_of(i * CH, CH)
-        kept = pl.ds(first, CH)
-        rows_x = rows_of(pieces, 0, first, CH)
-        rows_y = rows_of(pieces, 1, first, CH)
+def expert_rows(pieces, pg, pu, pd, out, hidden_out, group, buf, hidden, sems):
+    r = iota((CH, 128), 0)
+    lane = jnp.where(iota((CH, 128), 1) == r - twelfths(r) * 12, 1.0, 0.0)
+    source = ones_where(iota((16, CH), 0) == twelfths(iota((16, CH), 1)))
+    moves = []
+    for i in range(2):
+        kept = slice(i * CH, (i + 1) * CH)
+        rows_x = rows_of(pieces, 0, i * CH, CH)
+        rows_y = rows_of(pieces, 1, i * CH, CH)
         pre_gate = dot(rows_x, pg[...])
         pre_up = dot(rows_x, pu[...])
         back = dot(rows_y, pd[...], NT)
         s = jax.nn.sigmoid(pre_gate)
         act = pre_gate * s
         prod = act * pre_up
-        scaled_o[kept, :] = prod.astype(BF)
         ggp = (back * pre_up * s * (1.0 + pre_gate * (1.0 - s))).astype(BF)
         gup = (back * act).astype(BF)
-        ggp_o[kept, :] = ggp
-        gup_o[kept, :] = gup
+        for n, value in enumerate((prod.astype(BF), ggp, gup)):
+            hidden[n, kept, :] = value
+            to = hidden_out.at[n, kept, :]
+            moves.append(pltpu.make_async_copy(hidden.at[n, kept, :], to, sems.at[len(moves)]))
+            moves[-1].start()
         part = jnp.sum(back * prod, axis=1, keepdims=True)
-        spread = (part * lane[...].astype(F32)).astype(BF)
-        gates = dot(source[...], spread).astype(BF)
+        gates = dot(source, (part * lane).astype(BF)).astype(BF)
         grad = (dot(ggp, pg[...], NT) + dot(gup, pu[...], NT)).astype(BF)
         for t, x in enumerate(blocks()):
             for b in range(2):
                 cols = slice((t * 2 + b) * 128, (t * 2 + b + 1) * 128)
-                out[group * 4 + x, pl.ds(b * ROWS + first, CH), :] = grad[:, cols]
-            out[group * 4 + x, pl.ds(pl.multiple_of(ALL + i * 16, 16), 16), :] = gates
-        return carry
-
-    lax.fori_loop(0, ROWS // CH, step, 0)
-
-
-def first_body(lane, source, *refs):
-    pieces, (pg, pu, pd), (out, *hidden) = refs[:4], refs[4:7], refs[7:]
-    expert_rows(pieces, lane, source, pg, pu, pd, out, 0, *hidden)
-
-
-def second_body(lane, source, early, *refs):
-    pieces, (pg, pu, pd), (out, *hidden) = refs[:4], refs[4:7], refs[7:]
+                buf[i, t, b * CH : (b + 1) * CH, :] = grad[:, cols]
+            buf[i, t, 2 * CH : PART, :] = gates
+            to = out.at[group * 4 + x, i * PART : (i + 1) * PART, :]
+            moves.append(pltpu.make_async_copy(buf.at[i, t], to, sems.at[len(moves)]))
+            moves[-1].start()
+    for move in moves:
+        move.wait()
+
+
+EXPERT_SCRATCH = (
+    pltpu.VMEM((2, 4, 400, 128), BF), pltpu.VMEM((3, 384, 512), BF), pltpu.SemaphoreType.DMA((14,)),
+)
+
+
+def first_body(*refs):
+    pieces, (pg, pu, pd), (out, hidden_out) = refs[:4], refs[4:7], refs[7:9]
     half = lax.axis_index("yp")
-    for x in range(4):
-        out[half * 4 + x] = early[x]
-    expert_rows(pieces, lane, source, pg, pu, pd, out, 1 - half, *hidden)
+    expert_rows(pieces, pg, pu, pd, out, hidden_out, half, *refs[9:])
+
+
+def second_body(early, *refs):
+    pieces, (pg, pu, pd), (out, hidden_out) = refs[:4], refs[4:7], refs[7:9]
+    half = lax.axis_index("yp")
+    expert_rows(pieces, pg, pu, pd, out, hidden_out, 1 - half, *refs[9:])
 
 
 def weights_body(*refs):
-    pieces = refs[:4], refs[4:8]
-    hidden = refs[8:11], refs[11:14]
-    g_own, u_own, d_own, far = refs[14:18]
+    given, (g_own, u_own, d_own, far), local, sems = refs[:10], refs[10:14], refs[14:24], refs[24]
+    moves = [pltpu.make_async_copy(a, b, sems.at[n]) for n, (a, b) in enumerate(zip(given, local))]
+    for n in (8, 9, 0, 4, 1, 5, 2, 6, 3, 7):
+        moves[n].start()
+    pieces, hidden = (local[:4], local[4:8]), local[8:10]
+    moves[8].wait()
+    moves[9].wait()
     for t, here in enumerate(places()):
+        moves[t].wait()
+        moves[4 + t].wait()
         rows_x = [rows_of((p[t],), 0, 0, ROWS) for p in pieces]
         rows_y = [rows_of((p[t],), 1, 0, ROWS) for p in pieces]
         for n, own in ((0, g_own), (1, u_own)):
-            grad = sum(dot(rows_x[k], hidden[k][1 + n][...], TN) for k in range(2))
+            grad = sum(dot(rows_x[k], hidden[k][1 + n], TN) for k in range(2))
             own[here, :] = grad[:, :H]
             far[n, here, :] = grad[:, H:].astype(BF)
-        down = sum(dot(hidden[k][0][...], rows_y[k], TN) for k in range(2))
+        down = sum(dot(hidden[k][0], rows_y[k], TN) for k in range(2))
         d_own[:, here] = down[:H]
         far[2, here, :] = down[H:].astype(BF)
+
+
+WEIGHTS_SCRATCH = (
+    *[pltpu.VMEM((1536, 128), BF) for _ in range(8)],
+    *[pltpu.VMEM((3, 384, 512), BF) for _ in range(2)],
+    pltpu.SemaphoreType.DMA((10,)),
+)
 
 
 def sums_body(g_own, u_own, d_own, far, g_out, u_out, d_out, in_sq, hid_sq):
@@ -216,8 +245,13 @@
     hid_sq[...] = total[0:1]
 
 
-def back_body(order, parts, squares, out):
+def back_body(parts, squares, out):
     norms = jnp.sum(squares[...], axis=0)
+    o, i = iota((256, 208), 0), iota((256, 208), 1)
+    src, row = o >> 5, o & 31
+    late = (row >= 12).astype(jnp.int32)
+    at = jnp.where(row < 24, late * 84 + src * 12 + row, jnp.where(row == 24, 192 + src, 175 + row))
+    order = ones_where((i == at) & (row < 29))
 
     def total(first, count):
         rows = slice(first, first + count)
@@ -226,11 +260,14 @@
             added += parts[k, rows, :].astype(F32)
         return added
 
-    gates = total(ALL, SRC)
-    for b in range(4):
-        filled = [total(b * 96, 96), total(ROWS + b * 96, 96), gates[b * 8 : (b + 1) * 8], norms]
-        filled = jnp.concatenate(filled, axis=0).astype(BF)
-        out[b * 256 : (b + 1) * 256, :] = dot(order[...], filled).astype(BF)
+    for n in range(2):
+        gates = total(n * PART + 2 * CH, 16)
+        for b in range(2):
+            first = n * PART + b * 96
+            filled = [total(first, 96), total(first + CH, 96), gates[b * 8 : (b + 1) * 8], norms]
+            filled = jnp.concatenate(filled, axis=0).astype(BF)
+            at = (n * 2 + b) * 256
+            out[at : at + 256, :] = dot(order, filled).astype(BF)
 
 
 def combine_body(rt, gt, got, out, gate):
@@ -287,63 +324,64 @@
 
 
 def body(tokens, cotangent, routing, gates, gate_proj, up_proj, down_proj):
-    regroup, lane, source, back = tables()
+    vm, hbm = pltpu.VMEM, pltpu.HBM
     weights = (gate_proj[0], up_proj[0], down_proj[0])
-    sent = call(
-        kernel_of(dispatch_body, "dispatch"), shape((1536, 128)),
-        routing.T, gates.T, tokens, cotangent,
+    sent = kernel(
+        dispatch_body, "dispatch", shape((1536, 128)),
+        *(pltpu.with_memory_space_constraint(a, hbm) for a in (routing.T, gates.T, tokens, cotangent)),
+        spaces=[pltpu.HBM] * 4,
+        scratch=(
+            pltpu.VMEM((2, T), jnp.int32), pltpu.VMEM((2, T), BF), pltpu.VMEM((T, H), BF),
+            pltpu.VMEM((T, H), BF), pltpu.SemaphoreType.DMA((4,)),
+        ),
     )
     others = [lax.ppermute(w, "c", SWAP) for w in weights]
     moved = lax.all_to_all(sent.reshape(SRC, 48, 128), HOMES, 0, 0, tiled=True)
-    mine = call(
-        kernel_of(regroup_body, "regroup"), shape((1536, 128)), regroup, moved.reshape(1536, 128)
-    )
+    mine = kernel(regroup_body, "regroup", shape((1536, 128)), moved.reshape(1536, 128))
     mine2 = turned(mine, 2)
     near = lax.ppermute(mine, "yp", SWAP)
     mine1, mine3 = turned(mine, 1), turned(mine, -1)
     near2 = lax.ppermute(mine2, "yp", SWAP)
     near1, near3 = turned(near, 1), turned(near, -1)
     pieces, nears = (mine, mine1, mine3, mine2), (near, near1, near3, near2)
-    ordered = call(
-        kernel_of(prepare_body, "prepare"),
-        (shape((D, 2 * H)), shape((D, 2 * H)), shape((2 * H, D))),
+    ordered = kernel(
+        prepare_body, "prepare", (shape((D, 2 * H)), shape((D, 2 * H)), shape((2 * H, D))),
         *(w for pair in zip(weights, others) for w in pair),
     )
-    hidden = shape((ROWS, 2 * H))
-    early, *hidden1 = call(
-        kernel_of(first_body, "first", flops=2**31, vmem=VM[0]),
-        (shape((4, SENT, 128)), hidden, hidden, hidden), lane, source, *pieces, *ordered,
-    )
-    rows, *hidden2 = call(
-        kernel_of(second_body, "second", flops=2**31, vmem=VM[0]),
-        (shape((8, SENT, 128)), hidden, hidden, hidden), lane, source, early, *nears, *ordered,
+    halves = (hbm((8, 2 * PART, 128), BF), hbm((3, ROWS, 2 * H), BF))
+    options = dict(flops=2**31, vmem=8, out_spaces=[hbm, hbm], scratch=EXPERT_SCRATCH)
+    early, hidden1 = kernel(first_body, "first", halves, *pieces, *ordered, **options)
+    rows, hidden2 = kernel(
+        second_body, "second", halves, early, *nears, *ordered,
+        spaces=[hbm] + [vm] * 7, alias={0: 0}, **options,
     )
     parts = lax.all_to_all(rows, GROUP, 0, 0, tiled=True)
-    g_own, u_own, d_own, far = call(
-        kernel_of(weights_body, "weights", flops=2**31, vmem=VM[1]),
+    given = [pltpu.with_memory_space_constraint(a, hbm) for a in (*pieces, *nears, hidden1, hidden2)]
+    g_own, u_own, d_own, far = kernel(
+        weights_body, "weights",
         (shape((D, H), F32), shape((D, H), F32), shape((H, D), F32), shape((3, D, H))),
-        *pieces, *nears, *hidden1, *hidden2,
+        *given, flops=2**31, vmem=16, spaces=[hbm] * 10, scratch=WEIGHTS_SCRATCH,
     )
     far = lax.ppermute(far, "c", SWAP)
-    gate_grad, up_grad, down_grad, squares, hid_sq = call(
-        kernel_of(sums_body, "sums", flops=2**29, vmem=VM[2]),
+    gate_grad, up_grad, down_grad, squares, hid_sq = kernel(
+        sums_body, "sums",
         (
             shape((D, H)), shape((D, H)), shape((H, D)),
             shape((16, 8, 128), F32), shape((1, H), F32),
         ),
-        g_own, u_own, d_own, far,
+        g_own, u_own, d_own, far, flops=2**29, vmem=8,
     )
     squares, parts = lax.optimization_barrier((squares, parts))
     squares = lax.all_to_all(squares, ("c",) + GROUP, 0, 0, tiled=True)
-    answer = call(kernel_of(back_body, "back"), shape((1024, 128)), back, parts, squares)
+    answer = kernel(back_body, "back", shape((1024, 128)), parts, squares)
     got = lax.all_to_all(answer.reshape(SRC, 32, 128), HOMES, 0, 0, tiled=True)
-    own, gate = call(
-        kernel_of(combine_body, "combine"), (shape((4, 384, 128)), shape((2, T), F32)),
+    own, gate = kernel(
+        combine_body, "combine", (shape((4, 384, 128)), shape((2, T), F32)),
         routing.T, gates.T, got.reshape(1024, 128),
     )
     every = lax.all_to_all(own, "tp", 0, 0, tiled=True)
-    token, norms = call(
-        kernel_of(final_body, "final"), (shape((T, D)), shape((EXPERTS, 2, D), F32)), every
+    token, norms = kernel(
+        final_body, "final", (shape((T, D)), shape((EXPERTS, 2, D), F32)), every
     )
     return (
         token,

time: 152 us -> 144 us (0.947)
  local copies, waits for them, and re-layouts: 18.8 us -> 0.06 us
  waiting for transfers between devices: 18.5 us -> 25.5 us
  Pallas kernels: 19.3 us -> 23 us
  starting transfers between devices: 52.6 us -> 54.5 us
    unnamed x82 -> x26, local copies, waits for them, and re-layouts: 18.8 us -> 0.06 us
    all_to_all x1, waiting for transfers between devices: 0.97 us -> 8.51 us  [body(): parts = lax.all_to_all(rows, GROUP, 0, 0, tiled=True)]
    pallas_call x10, Pallas kernels: 19.3 us -> 23 us  [kernel(): pl.pallas_call(body, out_shape=outs, in_specs=[pl.BlockSpec(memory_space=...]
    ppermute x5, starting transfers between devices: 17 us -> 19 us  [turned(): return lax.ppermute(x, 'tp', [(i, (i + by) % 4) for i in range(4)])]
  transfers between devices with their start and end apart: 13 -> 13, of which waited for: 5 -> 6; matrix products, arithmetic and copies ran while one was open for 0% -> 0% of each run, Pallas kernels for 6% -> 9%
where the time goes in v2:
time: 144 us; the launch traced here: 143 us
  starting transfers between devices  54.5 us (38%)
  blocking collectives  39.3 us (27%)
  waiting for transfers between devices  25.5 us (18%)
  Pallas kernels  23 us (16%)
    pallas_call x10, Pallas kernels, kernel(): pl.pallas_call(body, out_shape=outs, in_specs=[pl.BlockSpec(memory_space=...  23 us
    all_to_all x1, blocking collectives, body(): got = lax.all_to_all(answer.reshape(SRC, 32, 128), HOMES, 0, 0, tiled=True)  19.1 us
    ppermute x5, starting transfers between devices, turned(): return lax.ppermute(x, 'tp', [(i, (i + by) % 4) for i in range(4)])  19 us
    all_to_all x1, starting transfers between devices, body(): moved = lax.all_to_all(sent.reshape(SRC, 48, 128), HOMES, 0, 0, tiled=True)  16.1 us
    all_to_all x1, blocking collectives, body(): every = lax.all_to_all(own, 'tp', 0, 0, tiled=True)  10.5 us
    all_to_all x1, waiting for transfers between devices, body(): moved = lax.all_to_all(sent.reshape(SRC, 48, 128), HOMES, 0, 0, tiled=True)  10.5 us
    all_to_all x1, blocking collectives, body(): squares = lax.all_to_all(squares, ('c',) + GROUP, 0, 0, tiled=True)  9.69 us
    all_to_all x1, waiting for transfers between devices, body(): parts = lax.all_to_all(rows, GROUP, 0, 0, tiled=True)  8.51 us
  transfers between devices with their start and end apart: 13, of which 6 were waited for; matrix products, arithmetic and copies ran while one was open for 0% of the time, Pallas kernels for 9%

profile of v2, /device:TPU:16, one launch (start us, length us, event | category | flops | bytes accessed | tf_op | source)
XLA Modules:
  0.0 143.3 jit_solution(1498064176205643059)
XLA Ops:
  0.6 0.0 copy-start
  0.6 0.0 copy-start.1
  0.7 0.0 copy-start.2
  0.7 3.6 %dispatch.1 = bf16[1536,128]{1,0:T(8,128)(2,1)} custom-call(s32[2,128]{1,0:T(2,128)} %bitcast.22, bf16[2,128]{1,0:T(2,128)(2,1)} %bitcast.24, bf16[128,1024]{1,0:T(8,128)(2,1)} %tok_in.1, bf16[128,1024]{1,0:T(8,128)(2,1)} %cot_in.1), custom_call_target="tpu_custom_call" | custom-call | flops 134217728 | bytes 1048576 | tf_op jit(solution)/shard_map/dispatch/pallas_call | solution.py:39
  4.2 16.1 %all-to-all-start = ((bf16[32,48,128]{2,1,0:T(8,128)(2,1)}), bf16[32,48,128]{2,1,0:T(8,128)(2,1)S(1)}, u32[]{:S(2)}, u32[]{:S(2)}) async-start(bf16[32,48,128]{2,1,0:T(8,128)(2,1)} %bitcast.2), calls=%async_computation | async-start | bytes 786432 | tf_op jit(solution)/shard_map/all_to_all | solution.py:339
  20.3 1.9 %collective-permute-start.7 = (bf16[1024,256]{1,0:T(8,128)(2,1)S(1)}, bf16[1024,256]{1,0:T(8,128)(2,1)S(1)}, u32[]{:S(2)}, u32[]{:S(2)}) collective-permute-start(bf16[1024,256]{1,0:T(8,128)(2,1)S(1)} %bitcast.15), channel_id=1, source_target_pairs={{0,4},{4,0},{1,5},{5,1},{2,6},{6,2},{3,7},{7,3},{8,12},{12,8},{9,1... | collective-permute-start | bytes 1572872 | tf_op jit(solution)/shard_map/ppermute | solution.py:338
  22.3 2.4 %collective-permute-start.8 = (bf16[1024,256]{1,0:T(8,128)(2,1)S(1)}, bf16[1024,256]{1,0:T(8,128)(2,1)S(1)}, u32[]{:S(2)}, u32[]{:S(2)}) collective-permute-start(bf16[1024,256]{1,0:T(8,128)(2,1)S(1)} %bitcast.17), channel_id=1, source_target_pairs={{0,4},{4,0},{1,5},{5,1},{2,6},{6,2},{3,7},{7,3},{8,12},{12,8},{9,1... | collective-permute-start | bytes 1572872 | tf_op jit(solution)/shard_map/ppermute | solution.py:338
  24.7 1.9 %collective-permute-start.9 = (bf16[256,1024]{1,0:T(8,128)(2,1)S(1)}, bf16[256,1024]{1,0:T(8,128)(2,1)S(1)}, u32[]{:S(2)}, u32[]{:S(2)}) collective-permute-start(bf16[256,1024]{1,0:T(8,128)(2,1)S(1)} %bitcast.19), channel_id=1, source_target_pairs={{0,4},{4,0},{1,5},{5,1},{2,6},{6,2},{3,7},{7,3},{8,12},{12,8},{9,1... | collective-permute-start | bytes 1572872 | tf_op jit(solution)/shard_map/ppermute | solution.py:338
  26.6 10.5 %all-to-all-done = bf16[32,48,128]{2,1,0:T(8,128)(2,1)S(1)} async-done(((bf16[32,48,128]{2,1,0:T(8,128)(2,1)}), bf16[32,48,128]{2,1,0:T(8,128)(2,1)S(1)}, u32[]{:S(2)}, u32[]{:S(2)}) %all-to-all-start) | async-done | bytes 393248 | tf_op jit(solution)/shard_map/all_to_all | solution.py:339
  37.1 0.4 regroup.1.refs_0_
  37.4 0.0 copy-start.3
  37.5 1.9 %collective-permute-start.3 = (bf16[1536,128]{1,0:T(8,128)(2,1)S(1)}, bf16[1536,128]{1,0:T(8,128)(2,1)S(1)}, u32[]{:S(2)}, u32[]{:S(2)}) collective-permute-start(bf16[1536,128]{1,0:T(8,128)(2,1)S(1)} %regroup.1.refs_0_), channel_id=1, source_target_pairs={{0,8},{8,0},{1,9},{9,1},{2,10},{10,2},{3,11},{11,3},{4,12},{12,4},... | collective-permute-start | bytes 1179656 | tf_op jit(solution)/shard_map/ppermute | solution.py:342
  39.4 4.9 %collective-permute-start.2 = (bf16[1536,128]{1,0:T(8,128)(2,1)S(1)}, bf16[1536,128]{1,0:T(8,128)(2,1)S(1)}, u32[]{:S(2)}, u32[]{:S(2)}) collective-permute-start(bf16[1536,128]{1,0:T(8,128)(2,1)S(1)} %regroup.1.refs_0_), channel_id=1, source_target_pairs={{0,2},{1,3},{2,0},{3,1},{4,6},{5,7},{6,4},{7,5},{8,10},{9,11},{10,... | collective-permute-start | bytes 1179656 | tf_op jit(solution)/shard_map/ppermute | solution.py:323
  44.3 0.0 collective-permute-done.7.wgo
  44.3 2.5 %collective-permute-start = (bf16[1536,128]{1,0:T(8,128)(2,1)S(1)}, bf16[1536,128]{1,0:T(8,128)(2,1)S(1)}, u32[]{:S(2)}, u32[]{:S(2)}) collective-permute-start(bf16[1536,128]{1,0:T(8,128)(2,1)S(1)} %regroup.1.refs_0_), channel_id=1, source_target_pairs={{0,1},{1,2},{2,3},{3,0},{4,5},{5,6},{6,7},{7,4},{8,9},{9,10},{10,1... | collective-permute-start | bytes 1179656 | tf_op jit(solution)/shard_map/ppermute | solution.py:323
  46.8 0.0 collective-permute-done.8.wuo
  46.9 4.6 %collective-permute-start.1 = (bf16[1536,128]{1,0:T(8,128)(2,1)S(1)}, bf16[1536,128]{1,0:T(8,128)(2,1)S(1)}, u32[]{:S(2)}, u32[]{:S(2)}) collective-permute-start(bf16[1536,128]{1,0:T(8,128)(2,1)S(1)} %regroup.1.refs_0_), channel_id=1, source_target_pairs={{0,3},{1,0},{2,1},{3,2},{4,7},{5,4},{6,5},{7,6},{8,11},{9,8},{10,9... | collective-permute-start | bytes 1179656 | tf_op jit(solution)/shard_map/ppermute | solution.py:323
  51.4 0.0 collective-permute-done.3.refs_0_.refs_4_
  51.4 1.9 %collective-permute-start.4 = (bf16[1536,128]{1,0:T(8,128)(2,1)S(1)}, bf16[1536,128]{1,0:T(8,128)(2,1)S(1)}, u32[]{:S(2)}, u32[]{:S(2)}) collective-permute-start(bf16[1536,128]{1,0:T(8,128)(2,1)S(1)} %collective-permute-done.3.refs_0_.refs_4_), channel_id=1, source_target_pairs={{0,1},{1,2},{2,3},{3,0},{4,5},{5,6},{6,7},{7,4},{8,9},{9,10},{10,1... | collective-permute-start | bytes 1179656 | tf_op jit(solution)/shard_map/ppermute | solution.py:323
  53.4 0.0 collective-permute-done.9.wdo
  53.4 5.1 %collective-permute-start.5 = (bf16[1536,128]{1,0:T(8,128)(2,1)S(1)}, bf16[1536,128]{1,0:T(8,128)(2,1)S(1)}, u32[]{:S(2)}, u32[]{:S(2)}) collective-permute-start(bf16[1536,128]{1,0:T(8,128)(2,1)S(1)} %collective-permute-done.3.refs_0_.refs_4_), channel_id=1, source_target_pairs={{0,3},{1,0},{2,1},{3,2},{4,7},{5,4},{6,5},{7,6},{8,11},{9,8},{10,9... | collective-permute-start | bytes 1179656 | tf_op jit(solution)/shard_map/ppermute | solution.py:323
  58.5 0.0 collective-permute-done.2.refs_3_
  58.5 3.9 %collective-permute-start.6 = (bf16[1536,128]{1,0:T(8,128)(2,1)S(1)}, bf16[1536,128]{1,0:T(8,128)(2,1)S(1)}, u32[]{:S(2)}, u32[]{:S(2)}) collective-permute-start(bf16[1536,128]{1,0:T(8,128)(2,1)S(1)} %collective-permute-done.2.refs_3_), channel_id=1, source_target_pairs={{0,8},{8,0},{1,9},{9,1},{2,10},{10,2},{3,11},{11,3},{4,12},{12,4},... | collective-permute-start | bytes 1179656 | tf_op jit(solution)/shard_map/ppermute | solution.py:344
  62.5 0.3 prepare.1
  62.8 0.0 collective-permute-done.refs_1_
  62.8 0.0 copy-start.8
  62.8 0.5 collective-permute-done.1.refs_2_
  63.3 4.2 %first.1 = (bf16[8,800,128]{2,1,0:T(8,128)(2,1)}, bf16[3,384,512]{2,1,0:T(8,128)(2,1)}) custom-call(bf16[1536,128]{1,0:T(8,128)(2,1)S(1)} %regroup.1.refs_0_, bf16[1536,128]{1,0:T(8,128)(2,1)S(1)} %collective-permute-done.refs_1_, bf16[1536,128]{1,0:T(8,128)(2,1)S(1)} %collective-permute-done.1.refs_2_, ...), custom_call_target="tpu_custom_call" | custom-call | flops 2147483648 | bytes 1048576 | tf_op jit(solution)/shard_map/first/pallas_call | solution.py:39
  67.5 0.0 copy-done.8
  67.5 0.0 copy-done.9
  67.6 2.5 %collective-permute-done.4.refs_1_.refs_5_ = bf16[1536,128]{1,0:T(8,128)(2,1)S(1)} collective-permute-done((bf16[1536,128]{1,0:T(8,128)(2,1)S(1)}, bf16[1536,128]{1,0:T(8,128)(2,1)S(1)}, u32[]{:S(2)}, u32[]{:S(2)}) %collective-permute-start.4) | collective-permute-done | bytes 393248 | tf_op jit(solution)/shard_map/ppermute | solution.py:323
  70.1 0.1 collective-permute-done.5.refs_2_.refs_6_
  70.2 0.0 collective-permute-done.6.refs_3_.refs_7_
  70.2 0.0 copy-done.6
  70.2 4.2 %second.1 = (bf16[8,800,128]{2,1,0:T(8,128)(2,1)}, bf16[3,384,512]{2,1,0:T(8,128)(2,1)}) custom-call(bf16[8,800,128]{2,1,0:T(8,128)(2,1)} %get-tuple-element.33.early, bf16[1536,128]{1,0:T(8,128)(2,1)S(1)} %collective-permute-done.3.refs_0_.refs_4_, bf16[1536,128]{1,0:T(8,128)(2,1)S(1)} %collective-permute-done.4.refs_1_.refs_5_, ...), custom_call_target="tpu_custom_call", output_to_operand_aliasing={{0}: (0, {})} | custom-call | flops 2147483648 | bytes 1048576 | tf_op jit(solution)/shard_map/second/pallas_call | solution.py:39
  74.5 5.4 %all-to-all-start.1 = ((bf16[8,800,128]{2,1,0:T(8,128)(2,1)}), bf16[8,800,128]{2,1,0:T(8,128)(2,1)S(1)}, u32[]{:S(2)}, u32[]{:S(2)}) async-start(bf16[8,800,128]{2,1,0:T(8,128)(2,1)} %get-tuple-element.40), calls=%async_computation.1 | async-start | bytes 3276800 | tf_op jit(solution)/shard_map/all_to_all | solution.py:358
  79.9 5.9 %weights.1 = (f32[1024,256]{1,0:T(8,128)S(1)}, f32[1024,256]{1,0:T(8,128)S(1)}, f32[256,1024]{1,0:T(8,128)S(1)}, bf16[3,1024,256]{2,1,0:T(8,128)(2,1)S(1)}) custom-call(bf16[1536,128]{1,0:T(8,128)(2,1)} %copy-done.3, bf16[1536,128]{1,0:T(8,128)(2,1)} %copy-done.8, bf16[1536,128]{1,0:T(8,128)(2,1)} %copy-done.9, bf16[1536,128]{1,0:T(8,128)(2,1)} %copy-done.7, ...), custom_call_target="tpu_custom_call" | custom-call | flops 2147483648 | bytes 1048576 | tf_op jit(solution)/shard_map/weights/pallas_call | solution.py:39
  85.8 1.9 %collective-permute-start.10 = (bf16[3,1024,256]{2,1,0:T(8,128)(2,1)S(1)}, bf16[3,1024,256]{2,1,0:T(8,128)(2,1)S(1)}, u32[]{:S(2)}, u32[]{:S(2)}) collective-permute-start(bf16[3,1024,256]{2,1,0:T(8,128)(2,1)S(1)} %get-tuple-element.38), channel_id=1, source_target_pairs={{0,4},{4,0},{1,5},{5,1},{2,6},{6,2},{3,7},{7,3},{8,12},{12,8},{9,1... | collective-permute-start | bytes 4718600 | tf_op jit(solution)/shard_map/ppermute | solution.py:365
  87.7 3.4 %collective-permute-done.10.far = bf16[3,1024,256]{2,1,0:T(8,128)(2,1)S(1)} collective-permute-done((bf16[3,1024,256]{2,1,0:T(8,128)(2,1)S(1)}, bf16[3,1024,256]{2,1,0:T(8,128)(2,1)S(1)}, u32[]{:S(2)}, u32[]{:S(2)}) %collective-permute-start.10) | collective-permute-done | bytes 1572896 | tf_op jit(solution)/shard_map/ppermute | solution.py:365
  91.1 1.5 %sums.1 = (bf16[1024,256]{1,0:T(8,128)(2,1)}, bf16[1024,256]{1,0:T(8,128)(2,1)}, bf16[256,1024]{1,0:T(8,128)(2,1)}, f32[16,8,128]{2,1,0:T(8,128)S(1)}, f32[1,256]{1,0:T(1,128)}) custom-call(f32[1024,256]{1,0:T(8,128)S(1)} %get-tuple-element.35.g_own, f32[1024,256]{1,0:T(8,128)S(1)} %get-tuple-element.36.u_own, f32[256,1024]{1,0:T(8,128)S(1)} %get-tuple-element.37.d_own, ...), custom_call_target="tpu_custom_call" | custom-call | flops 536870912 | bytes 1048576 | tf_op jit(solution)/shard_map/sums/pallas_call | solution.py:39
  92.6 8.5 %all-to-all-done.1.parts = bf16[8,800,128]{2,1,0:T(8,128)(2,1)S(1)} async-done(((bf16[8,800,128]{2,1,0:T(8,128)(2,1)}), bf16[8,800,128]{2,1,0:T(8,128)(2,1)S(1)}, u32[]{:S(2)}, u32[]{:S(2)}) %all-to-all-start.1) | async-done | bytes 1638432 | tf_op jit(solution)/shard_map/all_to_all | solution.py:358
  101.2 9.7 %all_to_all.25.squares = f32[16,8,128]{2,1,0:T(8,128)S(1)} all-to-all(f32[16,8,128]{2,1,0:T(8,128)S(1)} %get-tuple-element.42), channel_id=1, replica_groups=mesh['z'=8,'yh'=4,'yp'=2,'c'=2,'tp'=4] {'c','yp','tp'}, dimensions={0} | all-to-all | bytes 131072 | tf_op jit(solution)/shard_map/all_to_all | solution.py:375
  110.8 0.5 back.1
  111.3 19.1 %all_to_all.26 = bf16[32,32,128]{2,1,0:T(8,128)(2,1)S(1)} all-to-all(bf16[32,32,128]{2,1,0:T(8,128)(2,1)S(1)} %bitcast.14), channel_id=1, replica_groups=mesh['z'=8,'yh'=4,'yp'=2,'c'=2,'tp'=4] {'z','yh'}, dimensions={0} | all-to-all | bytes 524288 | tf_op jit(solution)/shard_map/all_to_all | solution.py:377
  130.4 0.0 copy-done.5
  130.4 1.5 %combine.1 = (bf16[4,384,128]{2,1,0:T(8,128)(2,1)S(1)}, f32[2,128]{1,0:T(2,128)}) custom-call(s32[2,128]{1,0:T(2,128)S(1)} %bitcast.23, bf16[2,128]{1,0:T(2,128)(2,1)S(1)} %bitcast.25, bf16[1024,128]{1,0:T(8,128)(2,1)S(1)} %bitcast.21), custom_call_target="tpu_custom_call" | custom-call | flops 134217728 | bytes 1048576 | tf_op jit(solution)/shard_map/combine/pallas_call | solution.py:39
  131.9 10.5 %all_to_all.27.got = bf16[4,384,128]{2,1,0:T(8,128)(2,1)S(1)} all-to-all(bf16[4,384,128]{2,1,0:T(8,128)(2,1)S(1)} %get-tuple-element.43), channel_id=1, replica_groups=mesh['z'=8,'yh'=4,'yp'=2,'c'=2,'tp'=4] {'tp'}, dimensions={0} | all-to-all | bytes 786432 | tf_op jit(solution)/shard_map/all_to_all | solution.py:382
  142.4 0.9 final.1
  (17 shorter events, 0.0 us)
Async XLA Ops:
  0.6 19.7 %copy-start = (bf16[1,1024,256]{2,1,0:T(8,128)(2,1)S(1)}, bf16[1,1024,256]{2,1,0:T(8,128)(2,1)}, u32[]{:S(2)}) copy-start(bf16[1,1024,256]{2,1,0:T(8,128)(2,1)} %param.11) | copy-start | bytes 1572868
  0.6 21.6 %copy-start.1 = (bf16[1,1024,256]{2,1,0:T(8,128)(2,1)S(1)}, bf16[1,1024,256]{2,1,0:T(8,128)(2,1)}, u32[]{:S(2)}) copy-start(bf16[1,1024,256]{2,1,0:T(8,128)(2,1)} %param.12) | copy-start | bytes 1572868
  0.7 24.0 %copy-start.2 = (bf16[1,256,1024]{2,1,0:T(8,128)(2,1)S(1)}, bf16[1,256,1024]{2,1,0:T(8,128)(2,1)}, u32[]{:S(2)}) copy-start(bf16[1,256,1024]{2,1,0:T(8,128)(2,1)} %param.13) | copy-start | bytes 1572868
  4.2 32.9 %all-to-all-start = ((bf16[32,48,128]{2,1,0:T(8,128)(2,1)}), bf16[32,48,128]{2,1,0:T(8,128)(2,1)S(1)}, u32[]{:S(2)}, u32[]{:S(2)}) async-start(bf16[32,48,128]{2,1,0:T(8,128)(2,1)} %bitcast.2), calls=%async_computation | async-start | bytes 786432 | tf_op jit(solution)/shard_map/all_to_all | solution.py:339
  20.3 24.0 %collective-permute-start.7 = (bf16[1024,256]{1,0:T(8,128)(2,1)S(1)}, bf16[1024,256]{1,0:T(8,128)(2,1)S(1)}, u32[]{:S(2)}, u32[]{:S(2)}) collective-permute-start(bf16[1024,256]{1,0:T(8,128)(2,1)S(1)} %bitcast.15), channel_id=1, source_target_pairs={{0,4},{4,0},{1,5},{5,1},{2,6},{6,2},{3,7},{7,3},{8,12},{12,8},{9,1... | collective-permute-start | bytes 1572872 | tf_op jit(solution)/shard_map/ppermute | solution.py:338
  22.3 24.6 %collective-permute-start.8 = (bf16[1024,256]{1,0:T(8,128)(2,1)S(1)}, bf16[1024,256]{1,0:T(8,128)(2,1)S(1)}, u32[]{:S(2)}, u32[]{:S(2)}) collective-permute-start(bf16[1024,256]{1,0:T(8,128)(2,1)S(1)} %bitcast.17), channel_id=1, source_target_pairs={{0,4},{4,0},{1,5},{5,1},{2,6},{6,2},{3,7},{7,3},{8,12},{12,8},{9,1... | collective-permute-start | bytes 1572872 | tf_op jit(solution)/shard_map/ppermute | solution.py:338
  24.7 28.7 %collective-permute-start.9 = (bf16[256,1024]{1,0:T(8,128)(2,1)S(1)}, bf16[256,1024]{1,0:T(8,128)(2,1)S(1)}, u32[]{:S(2)}, u32[]{:S(2)}) collective-permute-start(bf16[256,1024]{1,0:T(8,128)(2,1)S(1)} %bitcast.19), channel_id=1, source_target_pairs={{0,4},{4,0},{1,5},{5,1},{2,6},{6,2},{3,7},{7,3},{8,12},{12,8},{9,1... | collective-permute-start | bytes 1572872 | tf_op jit(solution)/shard_map/ppermute | solution.py:338
  37.4 25.8 %copy-start.3 = (bf16[1536,128]{1,0:T(8,128)(2,1)}, bf16[1536,128]{1,0:T(8,128)(2,1)S(1)}, u32[]{:S(2)}) copy-start(bf16[1536,128]{1,0:T(8,128)(2,1)S(1)} %regroup.1.refs_0_) | copy-start | bytes 1179652
  37.5 14.0 %collective-permute-start.3 = (bf16[1536,128]{1,0:T(8,128)(2,1)S(1)}, bf16[1536,128]{1,0:T(8,128)(2,1)S(1)}, u32[]{:S(2)}, u32[]{:S(2)}) collective-permute-start(bf16[1536,128]{1,0:T(8,128)(2,1)S(1)} %regroup.1.refs_0_), channel_id=1, source_target_pairs={{0,8},{8,0},{1,9},{9,1},{2,10},{10,2},{3,11},{11,3},{4,12},{12,4},... | collective-permute-start | bytes 1179656 | tf_op jit(solution)/shard_map/ppermute | solution.py:342
  39.4 19.1 %collective-permute-start.2 = (bf16[1536,128]{1,0:T(8,128)(2,1)S(1)}, bf16[1536,128]{1,0:T(8,128)(2,1)S(1)}, u32[]{:S(2)}, u32[]{:S(2)}) collective-permute-start(bf16[1536,128]{1,0:T(8,128)(2,1)S(1)} %regroup.1.refs_0_), channel_id=1, source_target_pairs={{0,2},{1,3},{2,0},{3,1},{4,6},{5,7},{6,4},{7,5},{8,10},{9,11},{10,... | collective-permute-start | bytes 1179656 | tf_op jit(solution)/shard_map/ppermute | solution.py:323
  44.3 18.4 %collective-permute-start = (bf16[1536,128]{1,0:T(8,128)(2,1)S(1)}, bf16[1536,128]{1,0:T(8,128)(2,1)S(1)}, u32[]{:S(2)}, u32[]{:S(2)}) collective-permute-start(bf16[1536,128]{1,0:T(8,128)(2,1)S(1)} %regroup.1.refs_0_), channel_id=1, source_target_pairs={{0,1},{1,2},{2,3},{3,0},{4,5},{5,6},{6,7},{7,4},{8,9},{9,10},{10,1... | collective-permute-start | bytes 1179656 | tf_op jit(solution)/shard_map/ppermute | solution.py:323
  46.9 16.4 %collective-permute-start.1 = (bf16[1536,128]{1,0:T(8,128)(2,1)S(1)}, bf16[1536,128]{1,0:T(8,128)(2,1)S(1)}, u32[]{:S(2)}, u32[]{:S(2)}) collective-permute-start(bf16[1536,128]{1,0:T(8,128)(2,1)S(1)} %regroup.1.refs_0_), channel_id=1, source_target_pairs={{0,3},{1,0},{2,1},{3,2},{4,7},{5,4},{6,5},{7,6},{8,11},{9,8},{10,9... | collective-permute-start | bytes 1179656 | tf_op jit(solution)/shard_map/ppermute | solution.py:323
  51.4 18.8 %copy-start.6 = (bf16[1536,128]{1,0:T(8,128)(2,1)}, bf16[1536,128]{1,0:T(8,128)(2,1)S(1)}, u32[]{:S(2)}) copy-start(bf16[1536,128]{1,0:T(8,128)(2,1)S(1)} %collective-permute-done.3.refs_0_.refs_4_) | copy-start | bytes 1179652
  51.4 18.6 %collective-permute-start.4 = (bf16[1536,128]{1,0:T(8,128)(2,1)S(1)}, bf16[1536,128]{1,0:T(8,128)(2,1)S(1)}, u32[]{:S(2)}, u32[]{:S(2)}) collective-permute-start(bf16[1536,128]{1,0:T(8,128)(2,1)S(1)} %collective-permute-done.3.refs_0_.refs_4_), channel_id=1, source_target_pairs={{0,1},{1,2},{2,3},{3,0},{4,5},{5,6},{6,7},{7,4},{8,9},{9,10},{10,1... | collective-permute-start | bytes 1179656 | tf_op jit(solution)/shard_map/ppermute | solution.py:323
  53.4 16.8 %collective-permute-start.5 = (bf16[1536,128]{1,0:T(8,128)(2,1)S(1)}, bf16[1536,128]{1,0:T(8,128)(2,1)S(1)}, u32[]{:S(2)}, u32[]{:S(2)}) collective-permute-start(bf16[1536,128]{1,0:T(8,128)(2,1)S(1)} %collective-permute-done.3.refs_0_.refs_4_), channel_id=1, source_target_pairs={{0,3},{1,0},{2,1},{3,2},{4,7},{5,4},{6,5},{7,6},{8,11},{9,8},{10,9... | collective-permute-start | bytes 1179656 | tf_op jit(solution)/shard_map/ppermute | solution.py:323
  58.5 4.8 %copy-start.7 = (bf16[1536,128]{1,0:T(8,128)(2,1)}, bf16[1536,128]{1,0:T(8,128)(2,1)S(1)}, u32[]{:S(2)}) copy-start(bf16[1536,128]{1,0:T(8,128)(2,1)S(1)} %collective-permute-done.2.refs_3_) | copy-start | bytes 1179652
  58.5 11.6 %collective-permute-start.6 = (bf16[1536,128]{1,0:T(8,128)(2,1)S(1)}, bf16[1536,128]{1,0:T(8,128)(2,1)S(1)}, u32[]{:S(2)}, u32[]{:S(2)}) collective-permute-start(bf16[1536,128]{1,0:T(8,128)(2,1)S(1)} %collective-permute-done.2.refs_3_), channel_id=1, source_target_pairs={{0,8},{8,0},{1,9},{9,1},{2,10},{10,2},{3,11},{11,3},{4,12},{12,4},... | collective-permute-start | bytes 1179656 | tf_op jit(solution)/shard_map/ppermute | solution.py:344
  62.8 4.8 %copy-start.8 = (bf16[1536,128]{1,0:T(8,128)(2,1)}, bf16[1536,128]{1,0:T(8,128)(2,1)S(1)}, u32[]{:S(2)}) copy-start(bf16[1536,128]{1,0:T(8,128)(2,1)S(1)} %collective-permute-done.refs_1_) | copy-start | bytes 1179652
  63.3 4.3 %copy-start.9 = (bf16[1536,128]{1,0:T(8,128)(2,1)}, bf16[1536,128]{1,0:T(8,128)(2,1)S(1)}, u32[]{:S(2)}) copy-start(bf16[1536,128]{1,0:T(8,128)(2,1)S(1)} %collective-permute-done.1.refs_2_) | copy-start | bytes 1179652
  70.1 4.3 %copy-start.10 = (bf16[1536,128]{1,0:T(8,128)(2,1)}, bf16[1536,128]{1,0:T(8,128)(2,1)S(1)}, u32[]{:S(2)}) copy-start(bf16[1536,128]{1,0:T(8,128)(2,1)S(1)} %collective-permute-done.4.refs_1_.refs_5_) | copy-start | bytes 1179652
  70.2 4.3 %copy-start.11 = (bf16[1536,128]{1,0:T(8,128)(2,1)}, bf16[1536,128]{1,0:T(8,128)(2,1)S(1)}, u32[]{:S(2)}) copy-start(bf16[1536,128]{1,0:T(8,128)(2,1)S(1)} %collective-permute-done.5.refs_2_.refs_6_) | copy-start | bytes 1179652
  70.2 4.3 %copy-start.12 = (bf16[1536,128]{1,0:T(8,128)(2,1)}, bf16[1536,128]{1,0:T(8,128)(2,1)S(1)}, u32[]{:S(2)}) copy-start(bf16[1536,128]{1,0:T(8,128)(2,1)S(1)} %collective-permute-done.6.refs_3_.refs_7_) | copy-start | bytes 1179652
  74.5 26.7 %all-to-all-start.1 = ((bf16[8,800,128]{2,1,0:T(8,128)(2,1)}), bf16[8,800,128]{2,1,0:T(8,128)(2,1)S(1)}, u32[]{:S(2)}, u32[]{:S(2)}) async-start(bf16[8,800,128]{2,1,0:T(8,128)(2,1)} %get-tuple-element.40), calls=%async_computation.1 | async-start | bytes 3276800 | tf_op jit(solution)/shard_map/all_to_all | solution.py:358
  85.8 5.3 %collective-permute-start.10 = (bf16[3,1024,256]{2,1,0:T(8,128)(2,1)S(1)}, bf16[3,1024,256]{2,1,0:T(8,128)(2,1)S(1)}, u32[]{:S(2)}, u32[]{:S(2)}) collective-permute-start(bf16[3,1024,256]{2,1,0:T(8,128)(2,1)S(1)} %get-tuple-element.38), channel_id=1, source_target_pairs={{0,4},{4,0},{1,5},{5,1},{2,6},{6,2},{3,7},{7,3},{8,12},{12,8},{9,1... | collective-permute-start | bytes 4718600 | tf_op jit(solution)/shard_map/ppermute | solution.py:365
  92.6 37.8 %copy-start.4 = (s32[128,2]{0,1:T(2,128)S(1)}, s32[128,2]{0,1:T(2,128)}, u32[]{:S(2)}) copy-start(s32[128,2]{0,1:T(2,128)} %param.9) | copy-start | bytes 3076
  92.6 37.8 %copy-start.5 = (bf16[128,2]{0,1:T(2,128)(2,1)S(1)}, bf16[128,2]{0,1:T(2,128)(2,1)}, u32[]{:S(2)}) copy-start(bf16[128,2]{0,1:T(2,128)(2,1)} %param.10) | copy-start | bytes 1540

commit v3 on v2

--- a/solution.py
+++ b/solution.py
@@ -1,11 +1,11 @@
 import jax
 import jax.numpy as jnp
-import numpy as np
 from jax import lax
 from jax.experimental import pallas as pl
 from jax.experimental.pallas import tpu as pltpu
 from jax.sharding import Mesh
 from jax.sharding import PartitionSpec as P
+
 
 EP = ("z", "yh", "yp", "c")
 HOMES = ("z", "yh")
@@ -15,8 +15,7 @@
 T, D, H = 128, 1024, 256
 EXPERTS, SLOTS, SRC = 32, 12, 32
 ROWS = SRC * SLOTS
-CH = 192
-PART = 2 * CH + 16
+PART = 2 * ROWS + SRC
 TURNS = (0, 3, 1, 2)
 NN = (((1,), (0,)), ((), ()))
 NT = (((1,), (1,)), ((), ()))
@@ -31,7 +30,7 @@
     return lax.broadcasted_iota(jnp.int32, shape, dim)
 
 
-def kernel(body, name, outs, *args, flops=2**27, vmem=4, spaces=None, out_spaces=None, scratch=(), alias=None):
+def kernel(body, outs, *args, flops=2**27, vmem=4, spaces=None, out_spaces=None, scratch=(), alias=None):
     vm = pltpu.VMEM
     one = not isinstance(outs, tuple)
     out_spaces = out_spaces or [vm] * (1 if one else len(outs))
@@ -45,7 +44,6 @@
         input_output_aliases=alias or {},
         compiler_params=pltpu.CompilerParams(vmem_limit_bytes=vmem * 1024 * 1024),
         cost_estimate=pl.CostEstimate(flops=flops, transcendentals=0, bytes_accessed=2**20),
-        name=name,
     )(*args)
 
 
@@ -61,7 +59,7 @@
     return jnp.where(hit, 1.0, 0.0).astype(BF)
 
 
-def dispatch_body(rt_in, gt_in, tok_in, cot_in, out, rt, gt, tok, cot, sems):
+def dispatch_body(rt_in, gt_in, tok_in, cot_in, out, rt, gt, tok, cot, buf, sems, out_sems):
     cols = pl.ds(pl.multiple_of(lax.axis_index("tp") * H, H), H)
     moves = [
         pltpu.make_async_copy(src, dst, sems.at[n])
@@ -71,8 +69,8 @@
     ]
     for move in moves:
         move.start()
-    for move in moves:
-        move.wait()
+    moves[0].wait()
+    moves[1].wait()
     r0, r1 = rt[0:1, :], rt[1:2, :]
     g0, g1 = gt[0:1, :].astype(F32), gt[1:2, :].astype(F32)
     e = iota((EXPERTS, T), 0)
@@ -82,24 +80,26 @@
     base0 = r0 * 48 + jnp.sum(m0 * before, axis=0, keepdims=True).astype(jnp.int32)
     base1 = r1 * 48 + jnp.sum(m1 * before, axis=0, keepdims=True).astype(jnp.int32)
 
-    def step(i, carry):
-        row = iota((192, T), 0) + i * 192
-        total = jnp.zeros((192, 128), F32)
+    moves[2].wait()
+    moves[3].wait()
+
+    sends = []
+    for i in range(4):
+        row = iota((384, T), 0) + i * 384
+        total = jnp.zeros((384, 128), F32)
         for half in range(2):
             cols = slice(half * 128, (half + 1) * 128)
-            for kind in range(2):
-                off = kind * 24 + half * 12
-                hit0, hit1 = row == base0 + off, row == base1 + off
-                if kind == 0:
-                    pick = jnp.where(hit0 | hit1, 1.0, 0.0)
-                    total += dot(pick.astype(BF), tok[:, cols])
-                else:
-                    pick = jnp.where(hit0, g0, jnp.where(hit1, g1, 0.0))
-                    total += dot(pick.astype(BF), cot[:, cols])
-        out[pl.ds(pl.multiple_of(i * 192, 192), 192), :] = total.astype(BF)
-        return carry
-
-    lax.fori_loop(0, 8, step, 0)
+            hit0, hit1 = row == base0 + half * 12, row == base1 + half * 12
+            total += dot(ones_where(hit0 | hit1), tok[:, cols])
+            hit0, hit1 = row == base0 + (24 + half * 12), row == base1 + (24 + half * 12)
+            pick = jnp.where(hit0, g0, jnp.where(hit1, g1, 0.0))
+            total += dot(pick.astype(BF), cot[:, cols])
+        part = slice(i * 384, (i + 1) * 384)
+        buf[part, :] = total.astype(BF)
+        sends.append(pltpu.make_async_copy(buf.at[part], out.at[part], out_sems.at[i]))
+        sends[-1].start()
+    for send in sends:
+        send.wait()
 
 
 def regroup_body(rows, out):
@@ -133,54 +133,46 @@
         pd[H:, there] = wdo[:, here]
 
 
-def rows_of(pieces, kind, first, count):
-    cols = []
-    for piece in pieces:
-        for half in range(2):
-            start = (kind * 2 + half) * ROWS + first
-            cols.append(piece[pl.ds(start, count), :])
-    return jnp.concatenate(cols, axis=1)
+def rows_of(pieces, kind):
+    starts = [(kind * 2 + half) * ROWS for half in range(2)]
+    return jnp.concatenate([p[s : s + ROWS, :] for p in pieces for s in starts], axis=1)
 
 
 def expert_rows(pieces, pg, pu, pd, out, hidden_out, group, buf, hidden, sems):
-    r = iota((CH, 128), 0)
-    lane = jnp.where(iota((CH, 128), 1) == r - twelfths(r) * 12, 1.0, 0.0)
-    source = ones_where(iota((16, CH), 0) == twelfths(iota((16, CH), 1)))
+    r = iota((ROWS, 128), 0)
+    lane = jnp.where(iota((ROWS, 128), 1) == r - twelfths(r) * 12, 1.0, 0.0)
+    source = ones_where(iota((SRC, ROWS), 0) == twelfths(iota((SRC, ROWS), 1)))
     moves = []
-    for i in range(2):
-        kept = slice(i * CH, (i + 1) * CH)
-        rows_x = rows_of(pieces, 0, i * CH, CH)
-        rows_y = rows_of(pieces, 1, i * CH, CH)
-        pre_gate = dot(rows_x, pg[...])
-        pre_up = dot(rows_x, pu[...])
-        back = dot(rows_y, pd[...], NT)
-        s = jax.nn.sigmoid(pre_gate)
-        act = pre_gate * s
-        prod = act * pre_up
-        ggp = (back * pre_up * s * (1.0 + pre_gate * (1.0 - s))).astype(BF)
-        gup = (back * act).astype(BF)
-        for n, value in enumerate((prod.astype(BF), ggp, gup)):
-            hidden[n, kept, :] = value
-            to = hidden_out.at[n, kept, :]
-            moves.append(pltpu.make_async_copy(hidden.at[n, kept, :], to, sems.at[len(moves)]))
-            moves[-1].start()
-        part = jnp.sum(back * prod, axis=1, keepdims=True)
-        gates = dot(source, (part * lane).astype(BF)).astype(BF)
-        grad = (dot(ggp, pg[...], NT) + dot(gup, pu[...], NT)).astype(BF)
-        for t, x in enumerate(blocks()):
-            for b in range(2):
-                cols = slice((t * 2 + b) * 128, (t * 2 + b + 1) * 128)
-                buf[i, t, b * CH : (b + 1) * CH, :] = grad[:, cols]
-            buf[i, t, 2 * CH : PART, :] = gates
-            to = out.at[group * 4 + x, i * PART : (i + 1) * PART, :]
-            moves.append(pltpu.make_async_copy(buf.at[i, t], to, sems.at[len(moves)]))
-            moves[-1].start()
+    rows_x = rows_of(pieces, 0)
+    rows_y = rows_of(pieces, 1)
+    pre_gate = dot(rows_x, pg[...])
+    pre_up = dot(rows_x, pu[...])
+    back = dot(rows_y, pd[...], NT)
+    s = jax.nn.sigmoid(pre_gate)
+    act = pre_gate * s
+    prod = act * pre_up
+    ggp = (back * pre_up * s * (1.0 + pre_gate * (1.0 - s))).astype(BF)
+    gup = (back * act).astype(BF)
+    for n, value in enumerate((prod.astype(BF), ggp, gup)):
+        hidden[n] = value
+        moves.append(pltpu.make_async_copy(hidden.at[n], hidden_out.at[n], sems.at[n]))
+        moves[-1].start()
+    part = jnp.sum(back * prod, axis=1, keepdims=True)
+    gates = dot(source, (part * lane).astype(BF)).astype(BF)
+    for t, x in enumerate(blocks()):
+        there = slice(t * H, (t + 1) * H)
+        grad = (dot(ggp, pg[there, :], NT) + dot(gup, pu[there, :], NT)).astype(BF)
+        buf[t, :ROWS, :] = grad[:, :128]
+        buf[t, ROWS : 2 * ROWS, :] = grad[:, 128:]
+        buf[t, 2 * ROWS :, :] = gates
+        moves.append(pltpu.make_async_copy(buf.at[t], out.at[group * 4 + x], sems.at[3 + t]))
+        moves[-1].start()
     for move in moves:
         move.wait()
 
 
 EXPERT_SCRATCH = (
-    pltpu.VMEM((2, 4, 400, 128), BF), pltpu.VMEM((3, 384, 512), BF), pltpu.SemaphoreType.DMA((14,)),
+    pltpu.VMEM((4, 800, 128), BF), pltpu.VMEM((3, 384, 512), BF), pltpu.SemaphoreType.DMA((7,)),
 )
 
 
@@ -207,8 +199,8 @@
     for t, here in enumerate(places()):
         moves[t].wait()
         moves[4 + t].wait()
-        rows_x = [rows_of((p[t],), 0, 0, ROWS) for p in pieces]
-        rows_y = [rows_of((p[t],), 1, 0, ROWS) for p in pieces]
+        rows_x = [rows_of((p[t],), 0) for p in pieces]
+        rows_y = [rows_of((p[t],), 1) for p in pieces]
         for n, own in ((0, g_own), (1, u_own)):
             grad = sum(dot(rows_x[k], hidden[k][1 + n], TN) for k in range(2))
             own[here, :] = grad[:, :H]
@@ -260,14 +252,11 @@
             added += parts[k, rows, :].astype(F32)
         return added
 
-    for n in range(2):
-        gates = total(n * PART + 2 * CH, 16)
-        for b in range(2):
-            first = n * PART + b * 96
-            filled = [total(first, 96), total(first + CH, 96), gates[b * 8 : (b + 1) * 8], norms]
-            filled = jnp.concatenate(filled, axis=0).astype(BF)
-            at = (n * 2 + b) * 256
-            out[at : at + 256, :] = dot(order, filled).astype(BF)
+    gates = total(2 * ROWS, SRC)
+    for b in range(4):
+        filled = [total(b * 96, 96), total(ROWS + b * 96, 96), gates[b * 8 : (b + 1) * 8], norms]
+        filled = jnp.concatenate(filled, axis=0).astype(BF)
+        out[b * 256 : (b + 1) * 256, :] = dot(order, filled).astype(BF)
 
 
 def combine_body(rt, gt, got, out, gate):
@@ -327,44 +316,47 @@
     vm, hbm = pltpu.VMEM, pltpu.HBM
     weights = (gate_proj[0], up_proj[0], down_proj[0])
     sent = kernel(
-        dispatch_body, "dispatch", shape((1536, 128)),
+        dispatch_body, hbm((1536, 128), BF),
         *(pltpu.with_memory_space_constraint(a, hbm) for a in (routing.T, gates.T, tokens, cotangent)),
-        spaces=[pltpu.HBM] * 4,
+        spaces=[hbm] * 4, out_spaces=[hbm],
         scratch=(
             pltpu.VMEM((2, T), jnp.int32), pltpu.VMEM((2, T), BF), pltpu.VMEM((T, H), BF),
-            pltpu.VMEM((T, H), BF), pltpu.SemaphoreType.DMA((4,)),
+            pltpu.VMEM((T, H), BF), pltpu.VMEM((1536, 128), BF), pltpu.SemaphoreType.DMA((4,)),
+            pltpu.SemaphoreType.DMA((4,)),
         ),
     )
     others = [lax.ppermute(w, "c", SWAP) for w in weights]
     moved = lax.all_to_all(sent.reshape(SRC, 48, 128), HOMES, 0, 0, tiled=True)
-    mine = kernel(regroup_body, "regroup", shape((1536, 128)), moved.reshape(1536, 128))
+    mine = kernel(regroup_body, shape((1536, 128)), moved.reshape(1536, 128))
     mine2 = turned(mine, 2)
     near = lax.ppermute(mine, "yp", SWAP)
-    mine1, mine3 = turned(mine, 1), turned(mine, -1)
+    mine1 = turned(mine, 1)
+    mine3 = turned(mine, -1)
     near2 = lax.ppermute(mine2, "yp", SWAP)
-    near1, near3 = turned(near, 1), turned(near, -1)
+    near1 = turned(near, 1)
+    near3 = turned(near, -1)
     pieces, nears = (mine, mine1, mine3, mine2), (near, near1, near3, near2)
     ordered = kernel(
-        prepare_body, "prepare", (shape((D, 2 * H)), shape((D, 2 * H)), shape((2 * H, D))),
+        prepare_body, (shape((D, 2 * H)), shape((D, 2 * H)), shape((2 * H, D))),
         *(w for pair in zip(weights, others) for w in pair),
     )
-    halves = (hbm((8, 2 * PART, 128), BF), hbm((3, ROWS, 2 * H), BF))
+    halves = (hbm((8, PART, 128), BF), hbm((3, ROWS, 2 * H), BF))
     options = dict(flops=2**31, vmem=8, out_spaces=[hbm, hbm], scratch=EXPERT_SCRATCH)
-    early, hidden1 = kernel(first_body, "first", halves, *pieces, *ordered, **options)
+    early, hidden1 = kernel(first_body, halves, *pieces, *ordered, **options)
     rows, hidden2 = kernel(
-        second_body, "second", halves, early, *nears, *ordered,
+        second_body, halves, early, *nears, *ordered,
         spaces=[hbm] + [vm] * 7, alias={0: 0}, **options,
     )
     parts = lax.all_to_all(rows, GROUP, 0, 0, tiled=True)
     given = [pltpu.with_memory_space_constraint(a, hbm) for a in (*pieces, *nears, hidden1, hidden2)]
     g_own, u_own, d_own, far = kernel(
-        weights_body, "weights",
+        weights_body,
         (shape((D, H), F32), shape((D, H), F32), shape((H, D), F32), shape((3, D, H))),
         *given, flops=2**31, vmem=16, spaces=[hbm] * 10, scratch=WEIGHTS_SCRATCH,
     )
     far = lax.ppermute(far, "c", SWAP)
     gate_grad, up_grad, down_grad, squares, hid_sq = kernel(
-        sums_body, "sums",
+        sums_body,
         (
             shape((D, H)), shape((D, H)), shape((H, D)),
             shape((16, 8, 128), F32), shape((1, H), F32),
@@ -373,16 +365,14 @@
     )
     squares, parts = lax.optimization_barrier((squares, parts))
     squares = lax.all_to_all(squares, ("c",) + GROUP, 0, 0, tiled=True)
-    answer = kernel(back_body, "back", shape((1024, 128)), parts, squares)
+    answer = kernel(back_body, shape((1024, 128)), parts, squares)
     got = lax.all_to_all(answer.reshape(SRC, 32, 128), HOMES, 0, 0, tiled=True)
     own, gate = kernel(
-        combine_body, "combine", (shape((4, 384, 128)), shape((2, T), F32)),
+        combine_body, (shape((4, 384, 128)), shape((2, T), F32)),
         routing.T, gates.T, got.reshape(1024, 128),
     )
     every = lax.all_to_all(own, "tp", 0, 0, tiled=True)
-    token, norms = kernel(
-        final_body, "final", (shape((T, D)), shape((EXPERTS, 2, D), F32)), every
-    )
+    token, norms = kernel(final_body, (shape((T, D)), shape((EXPERTS, 2, D), F32)), every)
     return (
         token,
         gate.T,

time: 144 us -> 142 us (0.986)
  Pallas kernels: 23 us -> 20.5 us
    pallas_call x10, Pallas kernels: 23 us -> 20.5 us  [kernel(): pl.pallas_call(body, out_shape=outs, in_specs=[pl.BlockSpec(memory_space=...]
  transfers between devices with their start and end apart: 13 -> 13, of which waited for: 6 -> 6; matrix products, arithmetic and copies ran while one was open for 0% -> 0% of each run, Pallas kernels for 9% -> 8%
where the time goes in v3:
time: 142 us
  starting transfers between devices  54.5 us (38%)
  blocking collectives  39.3 us (28%)
  waiting for transfers between devices  26.2 us (18%)
  Pallas kernels  20.5 us (14%)
    pallas_call x10, Pallas kernels, kernel(): pl.pallas_call(body, out_shape=outs, in_specs=[pl.BlockSpec(memory_space=...  20.5 us
    all_to_all x1, blocking collectives, body(): got = lax.all_to_all(answer.reshape(SRC, 32, 128), HOMES, 0, 0, tiled=True)  19.1 us
    ppermute x5, starting transfers between devices, turned(): return lax.ppermute(x, 'tp', [(i, (i + by) % 4) for i in range(4)])  19 us
    all_to_all x1, starting transfers between devices, body(): moved = lax.all_to_all(sent.reshape(SRC, 48, 128), HOMES, 0, 0, tiled=True)  16.1 us
    all_to_all x1, blocking collectives, body(): every = lax.all_to_all(own, 'tp', 0, 0, tiled=True)  10.5 us
    all_to_all x1, waiting for transfers between devices, body(): moved = lax.all_to_all(sent.reshape(SRC, 48, 128), HOMES, 0, 0, tiled=True)  10.5 us
    all_to_all x1, blocking collectives, body(): squares = lax.all_to_all(squares, ('c',) + GROUP, 0, 0, tiled=True)  9.69 us
    all_to_all x1, waiting for transfers between devices, body(): parts = lax.all_to_all(rows, GROUP, 0, 0, tiled=True)  8.51 us
  transfers between devices with their start and end apart: 13, of which 6 were waited for; matrix products, arithmetic and copies ran while one was open for 0% of the time, Pallas kernels for 8%

profile of v3, /device:TPU:16, one launch (start us, length us, event | category | flops | bytes accessed | tf_op | source)
XLA Modules:
  0.0 141.5 jit_solution(898866607066363444)
XLA Ops:
  0.6 0.0 copy-start
  0.6 0.0 copy-start.1
  0.7 0.0 copy-start.2
  0.7 2.5 %shard_map.126 = bf16[1536,128]{1,0:T(8,128)(2,1)} custom-call(s32[2,128]{1,0:T(2,128)} %bitcast.22, bf16[2,128]{1,0:T(2,128)(2,1)} %bitcast.24, bf16[128,1024]{1,0:T(8,128)(2,1)} %tok_in.1, bf16[128,1024]{1,0:T(8,128)(2,1)} %cot_in.1), custom_call_target="tpu_custom_call" | custom-call | flops 134217728 | bytes 1048576 | tf_op jit(solution)/shard_map/pallas_call | solution.py:38
  3.1 16.1 %all-to-all-start = ((bf16[32,48,128]{2,1,0:T(8,128)(2,1)}), bf16[32,48,128]{2,1,0:T(8,128)(2,1)S(1)}, u32[]{:S(2)}, u32[]{:S(2)}) async-start(bf16[32,48,128]{2,1,0:T(8,128)(2,1)} %bitcast.26), calls=%async_computation | async-start | bytes 786432 | tf_op jit(solution)/shard_map/all_to_all | solution.py:329
  19.2 0.0 copy-done
  19.2 1.9 %collective-permute-start.7 = (bf16[1024,256]{1,0:T(8,128)(2,1)S(1)}, bf16[1024,256]{1,0:T(8,128)(2,1)S(1)}, u32[]{:S(2)}, u32[]{:S(2)}) collective-permute-start(bf16[1024,256]{1,0:T(8,128)(2,1)S(1)} %bitcast.15), channel_id=1, source_target_pairs={{0,4},{4,0},{1,5},{5,1},{2,6},{6,2},{3,7},{7,3},{8,12},{12,8},{9,1... | collective-permute-start | bytes 1572872 | tf_op jit(solution)/shard_map/ppermute | solution.py:328
  21.2 0.0 copy-done.1
  21.2 2.4 %collective-permute-start.8 = (bf16[1024,256]{1,0:T(8,128)(2,1)S(1)}, bf16[1024,256]{1,0:T(8,128)(2,1)S(1)}, u32[]{:S(2)}, u32[]{:S(2)}) collective-permute-start(bf16[1024,256]{1,0:T(8,128)(2,1)S(1)} %bitcast.17), channel_id=1, source_target_pairs={{0,4},{4,0},{1,5},{5,1},{2,6},{6,2},{3,7},{7,3},{8,12},{12,8},{9,1... | collective-permute-start | bytes 1572872 | tf_op jit(solution)/shard_map/ppermute | solution.py:328
  23.6 1.9 %collective-permute-start.9 = (bf16[256,1024]{1,0:T(8,128)(2,1)S(1)}, bf16[256,1024]{1,0:T(8,128)(2,1)S(1)}, u32[]{:S(2)}, u32[]{:S(2)}) collective-permute-start(bf16[256,1024]{1,0:T(8,128)(2,1)S(1)} %bitcast.19), channel_id=1, source_target_pairs={{0,4},{4,0},{1,5},{5,1},{2,6},{6,2},{3,7},{7,3},{8,12},{12,8},{9,1... | collective-permute-start | bytes 1572872 | tf_op jit(solution)/shard_map/ppermute | solution.py:328
  25.5 10.5 %all-to-all-done = bf16[32,48,128]{2,1,0:T(8,128)(2,1)S(1)} async-done(((bf16[32,48,128]{2,1,0:T(8,128)(2,1)}), bf16[32,48,128]{2,1,0:T(8,128)(2,1)S(1)}, u32[]{:S(2)}, u32[]{:S(2)}) %all-to-all-start) | async-done | bytes 393248 | tf_op jit(solution)/shard_map/all_to_all | solution.py:329
  36.0 0.4 shard_map.127.refs_0_
  36.4 0.0 copy-start.3
  36.4 1.9 %collective-permute-start.3 = (bf16[1536,128]{1,0:T(8,128)(2,1)S(1)}, bf16[1536,128]{1,0:T(8,128)(2,1)S(1)}, u32[]{:S(2)}, u32[]{:S(2)}) collective-permute-start(bf16[1536,128]{1,0:T(8,128)(2,1)S(1)} %shard_map.127.refs_0_), channel_id=1, source_target_pairs={{0,8},{8,0},{1,9},{9,1},{2,10},{10,2},{3,11},{11,3},{4,12},{12,4},... | collective-permute-start | bytes 1179656 | tf_op jit(solution)/shard_map/ppermute | solution.py:332
  38.3 4.9 %collective-permute-start.2 = (bf16[1536,128]{1,0:T(8,128)(2,1)S(1)}, bf16[1536,128]{1,0:T(8,128)(2,1)S(1)}, u32[]{:S(2)}, u32[]{:S(2)}) collective-permute-start(bf16[1536,128]{1,0:T(8,128)(2,1)S(1)} %shard_map.127.refs_0_), channel_id=1, source_target_pairs={{0,2},{1,3},{2,0},{3,1},{4,6},{5,7},{6,4},{7,5},{8,10},{9,11},{10,... | collective-permute-start | bytes 1179656 | tf_op jit(solution)/shard_map/ppermute | solution.py:312
  43.2 0.0 collective-permute-done.7.wgo
  43.2 2.5 %collective-permute-start = (bf16[1536,128]{1,0:T(8,128)(2,1)S(1)}, bf16[1536,128]{1,0:T(8,128)(2,1)S(1)}, u32[]{:S(2)}, u32[]{:S(2)}) collective-permute-start(bf16[1536,128]{1,0:T(8,128)(2,1)S(1)} %shard_map.127.refs_0_), channel_id=1, source_target_pairs={{0,1},{1,2},{2,3},{3,0},{4,5},{5,6},{6,7},{7,4},{8,9},{9,10},{10,1... | collective-permute-start | bytes 1179656 | tf_op jit(solution)/shard_map/ppermute | solution.py:312
  45.8 0.0 collective-permute-done.8.wuo
  45.8 4.5 %collective-permute-start.1 = (bf16[1536,128]{1,0:T(8,128)(2,1)S(1)}, bf16[1536,128]{1,0:T(8,128)(2,1)S(1)}, u32[]{:S(2)}, u32[]{:S(2)}) collective-permute-start(bf16[1536,128]{1,0:T(8,128)(2,1)S(1)} %shard_map.127.refs_0_), channel_id=1, source_target_pairs={{0,3},{1,0},{2,1},{3,2},{4,7},{5,4},{6,5},{7,6},{8,11},{9,8},{10,9... | collective-permute-start | bytes 1179656 | tf_op jit(solution)/shard_map/ppermute | solution.py:312
  50.3 0.0 collective-permute-done.3.refs_0_.refs_4_
  50.3 1.9 %collective-permute-start.4 = (bf16[1536,128]{1,0:T(8,128)(2,1)S(1)}, bf16[1536,128]{1,0:T(8,128)(2,1)S(1)}, u32[]{:S(2)}, u32[]{:S(2)}) collective-permute-start(bf16[1536,128]{1,0:T(8,128)(2,1)S(1)} %collective-permute-done.3.refs_0_.refs_4_), channel_id=1, source_target_pairs={{0,1},{1,2},{2,3},{3,0},{4,5},{5,6},{6,7},{7,4},{8,9},{9,10},{10,1... | collective-permute-start | bytes 1179656 | tf_op jit(solution)/shard_map/ppermute | solution.py:312
  52.3 0.0 collective-permute-done.9.wdo
  52.3 5.1 %collective-permute-start.5 = (bf16[1536,128]{1,0:T(8,128)(2,1)S(1)}, bf16[1536,128]{1,0:T(8,128)(2,1)S(1)}, u32[]{:S(2)}, u32[]{:S(2)}) collective-permute-start(bf16[1536,128]{1,0:T(8,128)(2,1)S(1)} %collective-permute-done.3.refs_0_.refs_4_), channel_id=1, source_target_pairs={{0,3},{1,0},{2,1},{3,2},{4,7},{5,4},{6,5},{7,6},{8,11},{9,8},{10,9... | collective-permute-start | bytes 1179656 | tf_op jit(solution)/shard_map/ppermute | solution.py:312
  57.4 0.0 collective-permute-done.2.refs_3_
  57.4 3.9 %collective-permute-start.6 = (bf16[1536,128]{1,0:T(8,128)(2,1)S(1)}, bf16[1536,128]{1,0:T(8,128)(2,1)S(1)}, u32[]{:S(2)}, u32[]{:S(2)}) collective-permute-start(bf16[1536,128]{1,0:T(8,128)(2,1)S(1)} %collective-permute-done.2.refs_3_), channel_id=1, source_target_pairs={{0,8},{8,0},{1,9},{9,1},{2,10},{10,2},{3,11},{11,3},{4,12},{12,4},... | collective-permute-start | bytes 1179656 | tf_op jit(solution)/shard_map/ppermute | solution.py:335
  61.4 0.3 shard_map.128
  61.7 0.0 collective-permute-done.refs_1_
  61.7 0.0 copy-start.8
  61.7 0.5 collective-permute-done.1.refs_2_
  62.2 3.5 %shard_map.129 = (bf16[8,800,128]{2,1,0:T(8,128)(2,1)}, bf16[3,384,512]{2,1,0:T(8,128)(2,1)}) custom-call(bf16[1536,128]{1,0:T(8,128)(2,1)S(1)} %shard_map.127.refs_0_, bf16[1536,128]{1,0:T(8,128)(2,1)S(1)} %collective-permute-done.refs_1_, bf16[1536,128]{1,0:T(8,128)(2,1)S(1)} %collective-permute-done.1.refs_2_, ...), custom_call_target="tpu_custom_call" | custom-call | flops 2147483648 | bytes 1048576 | tf_op jit(solution)/shard_map/pallas_call | solution.py:38
  65.8 3.2 %collective-permute-done.4.refs_1_.refs_5_ = bf16[1536,128]{1,0:T(8,128)(2,1)S(1)} collective-permute-done((bf16[1536,128]{1,0:T(8,128)(2,1)S(1)}, bf16[1536,128]{1,0:T(8,128)(2,1)S(1)}, u32[]{:S(2)}, u32[]{:S(2)}) %collective-permute-start.4) | collective-permute-done | bytes 393248 | tf_op jit(solution)/shard_map/ppermute | solution.py:312
  69.0 0.1 collective-permute-done.5.refs_2_.refs_6_
  69.1 0.0 collective-permute-done.6.refs_3_.refs_7_
  69.1 0.0 copy-done.6
  69.1 3.5 %shard_map.130 = (bf16[8,800,128]{2,1,0:T(8,128)(2,1)}, bf16[3,384,512]{2,1,0:T(8,128)(2,1)}) custom-call(bf16[8,800,128]{2,1,0:T(8,128)(2,1)} %get-tuple-element.33.early, bf16[1536,128]{1,0:T(8,128)(2,1)S(1)} %collective-permute-done.3.refs_0_.refs_4_, ...), custom_call_target="tpu_custom_call", output_to_operand_aliasing={{0}: (0, {})} | custom-call | flops 2147483648 | bytes 1048576 | tf_op jit(solution)/shard_map/pallas_call | solution.py:38
  72.7 5.4 %all-to-all-start.1 = ((bf16[8,800,128]{2,1,0:T(8,128)(2,1)}), bf16[8,800,128]{2,1,0:T(8,128)(2,1)S(1)}, u32[]{:S(2)}, u32[]{:S(2)}) async-start(bf16[8,800,128]{2,1,0:T(8,128)(2,1)} %get-tuple-element.40), calls=%async_computation.1 | async-start | bytes 3276800 | tf_op jit(solution)/shard_map/all_to_all | solution.py:350
  78.1 5.9 %shard_map.131 = (f32[1024,256]{1,0:T(8,128)S(1)}, f32[1024,256]{1,0:T(8,128)S(1)}, f32[256,1024]{1,0:T(8,128)S(1)}, bf16[3,1024,256]{2,1,0:T(8,128)(2,1)S(1)}) custom-call(bf16[1536,128]{1,0:T(8,128)(2,1)} %copy-done.3, bf16[1536,128]{1,0:T(8,128)(2,1)} %copy-done.8, bf16[1536,128]{1,0:T(8,128)(2,1)} %copy-done.9, bf16[1536,128]{1,0:T(8,128)(2,1)} %copy-done.7, ...), custom_call_target="tpu_custom_call" | custom-call | flops 2147483648 | bytes 1048576 | tf_op jit(solution)/shard_map/pallas_call | solution.py:38
  84.0 1.9 %collective-permute-start.10 = (bf16[3,1024,256]{2,1,0:T(8,128)(2,1)S(1)}, bf16[3,1024,256]{2,1,0:T(8,128)(2,1)S(1)}, u32[]{:S(2)}, u32[]{:S(2)}) collective-permute-start(bf16[3,1024,256]{2,1,0:T(8,128)(2,1)S(1)} %get-tuple-element.38), channel_id=1, source_target_pairs={{0,4},{4,0},{1,5},{5,1},{2,6},{6,2},{3,7},{7,3},{8,12},{12,8},{9,1... | collective-permute-start | bytes 4718600 | tf_op jit(solution)/shard_map/ppermute | solution.py:357
  85.9 3.4 %collective-permute-done.10.far = bf16[3,1024,256]{2,1,0:T(8,128)(2,1)S(1)} collective-permute-done((bf16[3,1024,256]{2,1,0:T(8,128)(2,1)S(1)}, bf16[3,1024,256]{2,1,0:T(8,128)(2,1)S(1)}, u32[]{:S(2)}, u32[]{:S(2)}) %collective-permute-start.10) | collective-permute-done | bytes 1572896 | tf_op jit(solution)/shard_map/ppermute | solution.py:357
  89.3 1.5 %shard_map.132 = (bf16[1024,256]{1,0:T(8,128)(2,1)}, bf16[1024,256]{1,0:T(8,128)(2,1)}, bf16[256,1024]{1,0:T(8,128)(2,1)}, f32[16,8,128]{2,1,0:T(8,128)S(1)}, f32[1,256]{1,0:T(1,128)}) custom-call(f32[1024,256]{1,0:T(8,128)S(1)} %get-tuple-element.35.g_own, f32[1024,256]{1,0:T(8,128)S(1)} %get-tuple-element.36.u_own, ...), custom_call_target="tpu_custom_call" | custom-call | flops 536870912 | bytes 1048576 | tf_op jit(solution)/shard_map/pallas_call | solution.py:38
  90.9 8.5 %all-to-all-done.1.parts = bf16[8,800,128]{2,1,0:T(8,128)(2,1)S(1)} async-done(((bf16[8,800,128]{2,1,0:T(8,128)(2,1)}), bf16[8,800,128]{2,1,0:T(8,128)(2,1)S(1)}, u32[]{:S(2)}, u32[]{:S(2)}) %all-to-all-start.1) | async-done | bytes 1638432 | tf_op jit(solution)/shard_map/all_to_all | solution.py:350
  99.4 9.7 %all_to_all.25.squares = f32[16,8,128]{2,1,0:T(8,128)S(1)} all-to-all(f32[16,8,128]{2,1,0:T(8,128)S(1)} %get-tuple-element.42), channel_id=1, replica_groups=mesh['z'=8,'yh'=4,'yp'=2,'c'=2,'tp'=4] {'c','yp','tp'}, dimensions={0} | all-to-all | bytes 131072 | tf_op jit(solution)/shard_map/all_to_all | solution.py:367
  109.1 0.5 shard_map.133
  109.5 19.1 %all_to_all.26 = bf16[32,32,128]{2,1,0:T(8,128)(2,1)S(1)} all-to-all(bf16[32,32,128]{2,1,0:T(8,128)(2,1)S(1)} %bitcast.14), channel_id=1, replica_groups=mesh['z'=8,'yh'=4,'yp'=2,'c'=2,'tp'=4] {'z','yh'}, dimensions={0} | all-to-all | bytes 524288 | tf_op jit(solution)/shard_map/all_to_all | solution.py:369
  128.6 0.0 copy-done.5
  128.6 1.5 %shard_map.134 = (bf16[4,384,128]{2,1,0:T(8,128)(2,1)S(1)}, f32[2,128]{1,0:T(2,128)}) custom-call(s32[2,128]{1,0:T(2,128)S(1)} %bitcast.23, bf16[2,128]{1,0:T(2,128)(2,1)S(1)} %bitcast.25, bf16[1024,128]{1,0:T(8,128)(2,1)S(1)} %bitcast.21), custom_call_target="tpu_custom_call" | custom-call | flops 134217728 | bytes 1048576 | tf_op jit(solution)/shard_map/pallas_call | solution.py:38
  130.1 10.5 %all_to_all.27.got = bf16[4,384,128]{2,1,0:T(8,128)(2,1)S(1)} all-to-all(bf16[4,384,128]{2,1,0:T(8,128)(2,1)S(1)} %get-tuple-element.43), channel_id=1, replica_groups=mesh['z'=8,'yh'=4,'yp'=2,'c'=2,'tp'=4] {'tp'}, dimensions={0} | all-to-all | bytes 786432 | tf_op jit(solution)/shard_map/all_to_all | solution.py:374
  140.6 0.9 shard_map.135
  (17 shorter events, 0.0 us)
Async XLA Ops:
  0.6 18.6 %copy-start = (bf16[1,1024,256]{2,1,0:T(8,128)(2,1)S(1)}, bf16[1,1024,256]{2,1,0:T(8,128)(2,1)}, u32[]{:S(2)}) copy-start(bf16[1,1024,256]{2,1,0:T(8,128)(2,1)} %param.11) | copy-start | bytes 1572868
  0.6 20.5 %copy-start.1 = (bf16[1,1024,256]{2,1,0:T(8,128)(2,1)S(1)}, bf16[1,1024,256]{2,1,0:T(8,128)(2,1)}, u32[]{:S(2)}) copy-start(bf16[1,1024,256]{2,1,0:T(8,128)(2,1)} %param.12) | copy-start | bytes 1572868
  0.7 22.9 %copy-start.2 = (bf16[1,256,1024]{2,1,0:T(8,128)(2,1)S(1)}, bf16[1,256,1024]{2,1,0:T(8,128)(2,1)}, u32[]{:S(2)}) copy-start(bf16[1,256,1024]{2,1,0:T(8,128)(2,1)} %param.13) | copy-start | bytes 1572868
  3.1 32.9 %all-to-all-start = ((bf16[32,48,128]{2,1,0:T(8,128)(2,1)}), bf16[32,48,128]{2,1,0:T(8,128)(2,1)S(1)}, u32[]{:S(2)}, u32[]{:S(2)}) async-start(bf16[32,48,128]{2,1,0:T(8,128)(2,1)} %bitcast.26), calls=%async_computation | async-start | bytes 786432 | tf_op jit(solution)/shard_map/all_to_all | solution.py:329
  19.2 24.0 %collective-permute-start.7 = (bf16[1024,256]{1,0:T(8,128)(2,1)S(1)}, bf16[1024,256]{1,0:T(8,128)(2,1)S(1)}, u32[]{:S(2)}, u32[]{:S(2)}) collective-permute-start(bf16[1024,256]{1,0:T(8,128)(2,1)S(1)} %bitcast.15), channel_id=1, source_target_pairs={{0,4},{4,0},{1,5},{5,1},{2,6},{6,2},{3,7},{7,3},{8,12},{12,8},{9,1... | collective-permute-start | bytes 1572872 | tf_op jit(solution)/shard_map/ppermute | solution.py:328
  21.2 24.6 %collective-permute-start.8 = (bf16[1024,256]{1,0:T(8,128)(2,1)S(1)}, bf16[1024,256]{1,0:T(8,128)(2,1)S(1)}, u32[]{:S(2)}, u32[]{:S(2)}) collective-permute-start(bf16[1024,256]{1,0:T(8,128)(2,1)S(1)} %bitcast.17), channel_id=1, source_target_pairs={{0,4},{4,0},{1,5},{5,1},{2,6},{6,2},{3,7},{7,3},{8,12},{12,8},{9,1... | collective-permute-start | bytes 1572872 | tf_op jit(solution)/shard_map/ppermute | solution.py:328
  23.6 28.7 %collective-permute-start.9 = (bf16[256,1024]{1,0:T(8,128)(2,1)S(1)}, bf16[256,1024]{1,0:T(8,128)(2,1)S(1)}, u32[]{:S(2)}, u32[]{:S(2)}) collective-permute-start(bf16[256,1024]{1,0:T(8,128)(2,1)S(1)} %bitcast.19), channel_id=1, source_target_pairs={{0,4},{4,0},{1,5},{5,1},{2,6},{6,2},{3,7},{7,3},{8,12},{12,8},{9,1... | collective-permute-start | bytes 1572872 | tf_op jit(solution)/shard_map/ppermute | solution.py:328
  36.4 25.8 %copy-start.3 = (bf16[1536,128]{1,0:T(8,128)(2,1)}, bf16[1536,128]{1,0:T(8,128)(2,1)S(1)}, u32[]{:S(2)}) copy-start(bf16[1536,128]{1,0:T(8,128)(2,1)S(1)} %shard_map.127.refs_0_) | copy-start | bytes 1179652
  36.4 14.0 %collective-permute-start.3 = (bf16[1536,128]{1,0:T(8,128)(2,1)S(1)}, bf16[1536,128]{1,0:T(8,128)(2,1)S(1)}, u32[]{:S(2)}, u32[]{:S(2)}) collective-permute-start(bf16[1536,128]{1,0:T(8,128)(2,1)S(1)} %shard_map.127.refs_0_), channel_id=1, source_target_pairs={{0,8},{8,0},{1,9},{9,1},{2,10},{10,2},{3,11},{11,3},{4,12},{12,4},... | collective-permute-start | bytes 1179656 | tf_op jit(solution)/shard_map/ppermute | solution.py:332
  38.3 19.1 %collective-permute-start.2 = (bf16[1536,128]{1,0:T(8,128)(2,1)S(1)}, bf16[1536,128]{1,0:T(8,128)(2,1)S(1)}, u32[]{:S(2)}, u32[]{:S(2)}) collective-permute-start(bf16[1536,128]{1,0:T(8,128)(2,1)S(1)} %shard_map.127.refs_0_), channel_id=1, source_target_pairs={{0,2},{1,3},{2,0},{3,1},{4,6},{5,7},{6,4},{7,5},{8,10},{9,11},{10,... | collective-permute-start | bytes 1179656 | tf_op jit(solution)/shard_map/ppermute | solution.py:312
  43.2 18.4 %collective-permute-start = (bf16[1536,128]{1,0:T(8,128)(2,1)S(1)}, bf16[1536,128]{1,0:T(8,128)(2,1)S(1)}, u32[]{:S(2)}, u32[]{:S(2)}) collective-permute-start(bf16[1536,128]{1,0:T(8,128)(2,1)S(1)} %shard_map.127.refs_0_), channel_id=1, source_target_pairs={{0,1},{1,2},{2,3},{3,0},{4,5},{5,6},{6,7},{7,4},{8,9},{9,10},{10,1... | collective-permute-start | bytes 1179656 | tf_op jit(solution)/shard_map/ppermute | solution.py:312
  45.8 16.4 %collective-permute-start.1 = (bf16[1536,128]{1,0:T(8,128)(2,1)S(1)}, bf16[1536,128]{1,0:T(8,128)(2,1)S(1)}, u32[]{:S(2)}, u32[]{:S(2)}) collective-permute-start(bf16[1536,128]{1,0:T(8,128)(2,1)S(1)} %shard_map.127.refs_0_), channel_id=1, source_target_pairs={{0,3},{1,0},{2,1},{3,2},{4,7},{5,4},{6,5},{7,6},{8,11},{9,8},{10,9... | collective-permute-start | bytes 1179656 | tf_op jit(solution)/shard_map/ppermute | solution.py:312
  50.3 18.8 %copy-start.6 = (bf16[1536,128]{1,0:T(8,128)(2,1)}, bf16[1536,128]{1,0:T(8,128)(2,1)S(1)}, u32[]{:S(2)}) copy-start(bf16[1536,128]{1,0:T(8,128)(2,1)S(1)} %collective-permute-done.3.refs_0_.refs_4_) | copy-start | bytes 1179652
  50.3 18.6 %collective-permute-start.4 = (bf16[1536,128]{1,0:T(8,128)(2,1)S(1)}, bf16[1536,128]{1,0:T(8,128)(2,1)S(1)}, u32[]{:S(2)}, u32[]{:S(2)}) collective-permute-start(bf16[1536,128]{1,0:T(8,128)(2,1)S(1)} %collective-permute-done.3.refs_0_.refs_4_), channel_id=1, source_target_pairs={{0,1},{1,2},{2,3},{3,0},{4,5},{5,6},{6,7},{7,4},{8,9},{9,10},{10,1... | collective-permute-start | bytes 1179656 | tf_op jit(solution)/shard_map/ppermute | solution.py:312
  52.3 16.8 %collective-permute-start.5 = (bf16[1536,128]{1,0:T(8,128)(2,1)S(1)}, bf16[1536,128]{1,0:T(8,128)(2,1)S(1)}, u32[]{:S(2)}, u32[]{:S(2)}) collective-permute-start(bf16[1536,128]{1,0:T(8,128)(2,1)S(1)} %collective-permute-done.3.refs_0_.refs_4_), channel_id=1, source_target_pairs={{0,3},{1,0},{2,1},{3,2},{4,7},{5,4},{6,5},{7,6},{8,11},{9,8},{10,9... | collective-permute-start | bytes 1179656 | tf_op jit(solution)/shard_map/ppermute | solution.py:312
  57.4 4.8 %copy-start.7 = (bf16[1536,128]{1,0:T(8,128)(2,1)}, bf16[1536,128]{1,0:T(8,128)(2,1)S(1)}, u32[]{:S(2)}) copy-start(bf16[1536,128]{1,0:T(8,128)(2,1)S(1)} %collective-permute-done.2.refs_3_) | copy-start | bytes 1179652
  57.4 11.6 %collective-permute-start.6 = (bf16[1536,128]{1,0:T(8,128)(2,1)S(1)}, bf16[1536,128]{1,0:T(8,128)(2,1)S(1)}, u32[]{:S(2)}, u32[]{:S(2)}) collective-permute-start(bf16[1536,128]{1,0:T(8,128)(2,1)S(1)} %collective-permute-done.2.refs_3_), channel_id=1, source_target_pairs={{0,8},{8,0},{1,9},{9,1},{2,10},{10,2},{3,11},{11,3},{4,12},{12,4},... | collective-permute-start | bytes 1179656 | tf_op jit(solution)/shard_map/ppermute | solution.py:335
  61.7 4.1 %copy-start.8 = (bf16[1536,128]{1,0:T(8,128)(2,1)}, bf16[1536,128]{1,0:T(8,128)(2,1)S(1)}, u32[]{:S(2)}) copy-start(bf16[1536,128]{1,0:T(8,128)(2,1)S(1)} %collective-permute-done.refs_1_) | copy-start | bytes 1179652
  62.2 3.5 %copy-start.9 = (bf16[1536,128]{1,0:T(8,128)(2,1)}, bf16[1536,128]{1,0:T(8,128)(2,1)S(1)}, u32[]{:S(2)}) copy-start(bf16[1536,128]{1,0:T(8,128)(2,1)S(1)} %collective-permute-done.1.refs_2_) | copy-start | bytes 1179652
  69.0 3.7 %copy-start.10 = (bf16[1536,128]{1,0:T(8,128)(2,1)}, bf16[1536,128]{1,0:T(8,128)(2,1)S(1)}, u32[]{:S(2)}) copy-start(bf16[1536,128]{1,0:T(8,128)(2,1)S(1)} %collective-permute-done.4.refs_1_.refs_5_) | copy-start | bytes 1179652
  69.1 3.6 %copy-start.11 = (bf16[1536,128]{1,0:T(8,128)(2,1)}, bf16[1536,128]{1,0:T(8,128)(2,1)S(1)}, u32[]{:S(2)}) copy-start(bf16[1536,128]{1,0:T(8,128)(2,1)S(1)} %collective-permute-done.5.refs_2_.refs_6_) | copy-start | bytes 1179652
  69.1 3.6 %copy-start.12 = (bf16[1536,128]{1,0:T(8,128)(2,1)}, bf16[1536,128]{1,0:T(8,128)(2,1)S(1)}, u32[]{:S(2)}) copy-start(bf16[1536,128]{1,0:T(8,128)(2,1)S(1)} %collective-permute-done.6.refs_3_.refs_7_) | copy-start | bytes 1179652
  72.7 26.7 %all-to-all-start.1 = ((bf16[8,800,128]{2,1,0:T(8,128)(2,1)}), bf16[8,800,128]{2,1,0:T(8,128)(2,1)S(1)}, u32[]{:S(2)}, u32[]{:S(2)}) async-start(bf16[8,800,128]{2,1,0:T(8,128)(2,1)} %get-tuple-element.40), calls=%async_computation.1 | async-start | bytes 3276800 | tf_op jit(solution)/shard_map/all_to_all | solution.py:350
  84.0 5.3 %collective-permute-start.10 = (bf16[3,1024,256]{2,1,0:T(8,128)(2,1)S(1)}, bf16[3,1024,256]{2,1,0:T(8,128)(2,1)S(1)}, u32[]{:S(2)}, u32[]{:S(2)}) collective-permute-start(bf16[3,1024,256]{2,1,0:T(8,128)(2,1)S(1)} %get-tuple-element.38), channel_id=1, source_target_pairs={{0,4},{4,0},{1,5},{5,1},{2,6},{6,2},{3,7},{7,3},{8,12},{12,8},{9,1... | collective-permute-start | bytes 4718600 | tf_op jit(solution)/shard_map/ppermute | solution.py:357
  90.9 37.8 %copy-start.4 = (s32[128,2]{0,1:T(2,128)S(1)}, s32[128,2]{0,1:T(2,128)}, u32[]{:S(2)}) copy-start(s32[128,2]{0,1:T(2,128)} %param.9) | copy-start | bytes 3076
  90.9 37.8 %copy-start.5 = (bf16[128,2]{0,1:T(2,128)(2,1)S(1)}, bf16[128,2]{0,1:T(2,128)(2,1)}, u32[]{:S(2)}) copy-start(bf16[128,2]{0,1:T(2,128)(2,1)} %param.10) | copy-start | bytes 1540

commit v4 on v3

--- a/solution.py
+++ b/solution.py
@@ -165,7 +165,8 @@
         buf[t, :ROWS, :] = grad[:, :128]
         buf[t, ROWS : 2 * ROWS, :] = grad[:, 128:]
         buf[t, 2 * ROWS :, :] = gates
-        moves.append(pltpu.make_async_copy(buf.at[t], out.at[group * 4 + x], sems.at[3 + t]))
+        to = out.at[x, group * PART : (group + 1) * PART]
+        moves.append(pltpu.make_async_copy(buf.at[t], to, sems.at[3 + t]))
         moves[-1].start()
     for move in moves:
         move.wait()
@@ -177,15 +178,11 @@
 
 
 def first_body(*refs):
-    pieces, (pg, pu, pd), (out, hidden_out) = refs[:4], refs[4:7], refs[7:9]
-    half = lax.axis_index("yp")
-    expert_rows(pieces, pg, pu, pd, out, hidden_out, half, *refs[9:])
+    expert_rows(refs[:4], *refs[4:9], 0, *refs[9:])
 
 
 def second_body(early, *refs):
-    pieces, (pg, pu, pd), (out, hidden_out) = refs[:4], refs[4:7], refs[7:9]
-    half = lax.axis_index("yp")
-    expert_rows(pieces, pg, pu, pd, out, hidden_out, 1 - half, *refs[9:])
+    expert_rows(refs[:4], *refs[4:9], 1, *refs[9:])
 
 
 def weights_body(*refs):
@@ -237,7 +234,11 @@
     hid_sq[...] = total[0:1]
 
 
-def back_body(parts, squares, out):
+def partner_body(parts, out):
+    out[...] = sum(parts[k, PART:, :].astype(F32) for k in range(4)).astype(BF)
+
+
+def back_body(parts, near, squares, out):
     norms = jnp.sum(squares[...], axis=0)
     o, i = iota((256, 208), 0), iota((256, 208), 1)
     src, row = o >> 5, o & 31
@@ -247,10 +248,7 @@
 
     def total(first, count):
         rows = slice(first, first + count)
-        added = parts[0, rows, :].astype(F32)
-        for k in range(1, 8):
-            added += parts[k, rows, :].astype(F32)
-        return added
+        return sum((parts[k, rows, :].astype(F32) for k in range(4)), near[rows, :].astype(F32))
 
     gates = total(2 * ROWS, SRC)
     for b in range(4):
@@ -340,14 +338,14 @@
         prepare_body, (shape((D, 2 * H)), shape((D, 2 * H)), shape((2 * H, D))),
         *(w for pair in zip(weights, others) for w in pair),
     )
-    halves = (hbm((8, PART, 128), BF), hbm((3, ROWS, 2 * H), BF))
+    halves = (hbm((4, 2 * PART, 128), BF), hbm((3, ROWS, 2 * H), BF))
     options = dict(flops=2**31, vmem=8, out_spaces=[hbm, hbm], scratch=EXPERT_SCRATCH)
     early, hidden1 = kernel(first_body, halves, *pieces, *ordered, **options)
     rows, hidden2 = kernel(
         second_body, halves, early, *nears, *ordered,
         spaces=[hbm] + [vm] * 7, alias={0: 0}, **options,
     )
-    parts = lax.all_to_all(rows, GROUP, 0, 0, tiled=True)
+    parts = lax.all_to_all(rows, "tp", 0, 0, tiled=True)
     given = [pltpu.with_memory_space_constraint(a, hbm) for a in (*pieces, *nears, hidden1, hidden2)]
     g_own, u_own, d_own, far = kernel(
         weights_body,
@@ -365,7 +363,9 @@
     )
     squares, parts = lax.optimization_barrier((squares, parts))
     squares = lax.all_to_all(squares, ("c",) + GROUP, 0, 0, tiled=True)
-    answer = kernel(back_body, shape((1024, 128)), parts, squares)
+    near_sums = kernel(partner_body, shape((PART, 128)), parts)
+    near_sums = lax.ppermute(near_sums, "yp", SWAP)
+    answer = kernel(back_body, shape((1024, 128)), parts, near_sums, squares)
     got = lax.all_to_all(answer.reshape(SRC, 32, 128), HOMES, 0, 0, tiled=True)
     own, gate = kernel(
         combine_body, (shape((4, 384, 128)), shape((2, T), F32)),

time: 142 us -> 157 us (1.11)
  local copies, waits for them, and re-layouts: 0.06 us -> 6.69 us
  waiting for transfers between devices: 26.2 us -> 31.2 us
  starting transfers between devices: 54.5 us -> 57 us
    all_to_all x1, waiting for transfers between devices: 8.51 us -> 16.8 us  [body(): parts = lax.all_to_all(rows, 'tp', 0, 0, tiled=True)]
    unnamed x26 -> x38, local copies, waits for them, and re-layouts: 0.06 us -> 6.69 us
    ppermute x0 -> x1, starting transfers between devices: none -> 3.64 us  [body(): near_sums = lax.ppermute(near_sums, 'yp', SWAP)]
    ppermute x1, waiting for transfers between devices: 3.38 us -> 0.01 us  [body(): far = lax.ppermute(far, 'c', SWAP)]
    pallas_call x10 -> x11, Pallas kernels: 20.5 us -> 21.7 us  [kernel(): pl.pallas_call(body, out_shape=outs, in_specs=[pl.BlockSpec(memory_space=...]
  transfers between devices with their start and end apart: 13 -> 14, of which waited for: 6 -> 5; matrix products, arithmetic and copies ran while one was open for 0% -> 0% of each run, Pallas kernels for 8% -> 4%
where the time goes in v4:
time: 157 us; the launch traced here: 156 us
  starting transfers between devices  57 us (36%)
  blocking collectives  38.3 us (24%)
  waiting for transfers between devices  31.2 us (20%)
  Pallas kernels  21.7 us (14%)
  local copies, waits for them, and re-layouts  6.69 us (4%)
    pallas_call x11, Pallas kernels, kernel(): pl.pallas_call(body, out_shape=outs, in_specs=[pl.BlockSpec(memory_space=...  21.7 us
    all_to_all x1, blocking collectives, body(): got = lax.all_to_all(answer.reshape(SRC, 32, 128), HOMES, 0, 0, tiled=True)  19.1 us
    ppermute x5, starting transfers between devices, turned(): return lax.ppermute(x, 'tp', [(i, (i + by) % 4) for i in range(4)])  19 us
    all_to_all x1, waiting for transfers between devices, body(): parts = lax.all_to_all(rows, 'tp', 0, 0, tiled=True)  16.8 us
    all_to_all x1, starting transfers between devices, body(): moved = lax.all_to_all(sent.reshape(SRC, 48, 128), HOMES, 0, 0, tiled=True)  16.1 us
    all_to_all x1, blocking collectives, body(): every = lax.all_to_all(own, 'tp', 0, 0, tiled=True)  10.5 us
    all_to_all x1, waiting for transfers between devices, body(): moved = lax.all_to_all(sent.reshape(SRC, 48, 128), HOMES, 0, 0, tiled=True)  10.5 us
    all_to_all x1, blocking collectives, body(): squares = lax.all_to_all(squares, ('c',) + GROUP, 0, 0, tiled=True)  8.69 us
  transfers between devices with their start and end apart: 14, of which 5 were waited for; matrix products, arithmetic and copies ran while one was open for 0% of the time, Pallas kernels for 4%

profile of v4, /device:TPU:16, one launch (start us, length us, event | category | flops | bytes accessed | tf_op | source)
XLA Modules:
  0.0 155.9 jit_solution(12550448271771114540)
XLA Ops:
  0.7 2.5 %shard_map.126 = bf16[1536,128]{1,0:T(8,128)(2,1)} custom-call(s32[2,128]{1,0:T(2,128)} %bitcast.22, bf16[2,128]{1,0:T(2,128)(2,1)} %bitcast.24, bf16[128,1024]{1,0:T(8,128)(2,1)} %tok_in.1, bf16[128,1024]{1,0:T(8,128)(2,1)} %cot_in.1), custom_call_target="tpu_custom_call" | custom-call | flops 134217728 | bytes 1048576 | tf_op jit(solution)/shard_map/pallas_call | solution.py:38
  3.1 16.1 %all-to-all-start = ((bf16[32,48,128]{2,1,0:T(8,128)(2,1)}), bf16[32,48,128]{2,1,0:T(8,128)(2,1)S(1)}, u32[]{:S(2)}, u32[]{:S(2)}) async-start(bf16[32,48,128]{2,1,0:T(8,128)(2,1)} %bitcast.26), calls=%async_computation | async-start | bytes 786432 | tf_op jit(solution)/shard_map/all_to_all | solution.py:327
  19.2 1.9 %collective-permute-start.7 = (bf16[1024,256]{1,0:T(8,128)(2,1)S(1)}, bf16[1024,256]{1,0:T(8,128)(2,1)S(1)}, u32[]{:S(2)}, u32[]{:S(2)}) collective-permute-start(bf16[1024,256]{1,0:T(8,128)(2,1)S(1)} %bitcast.15), channel_id=1, source_target_pairs={{0,4},{4,0},{1,5},{5,1},{2,6},{6,2},{3,7},{7,3},{8,12},{12,8},{9,1... | collective-permute-start | bytes 1572872 | tf_op jit(solution)/shard_map/ppermute | solution.py:326
  21.2 2.4 %collective-permute-start.8 = (bf16[1024,256]{1,0:T(8,128)(2,1)S(1)}, bf16[1024,256]{1,0:T(8,128)(2,1)S(1)}, u32[]{:S(2)}, u32[]{:S(2)}) collective-permute-start(bf16[1024,256]{1,0:T(8,128)(2,1)S(1)} %bitcast.17), channel_id=1, source_target_pairs={{0,4},{4,0},{1,5},{5,1},{2,6},{6,2},{3,7},{7,3},{8,12},{12,8},{9,1... | collective-permute-start | bytes 1572872 | tf_op jit(solution)/shard_map/ppermute | solution.py:326
  23.6 1.9 %collective-permute-start.9 = (bf16[256,1024]{1,0:T(8,128)(2,1)S(1)}, bf16[256,1024]{1,0:T(8,128)(2,1)S(1)}, u32[]{:S(2)}, u32[]{:S(2)}) collective-permute-start(bf16[256,1024]{1,0:T(8,128)(2,1)S(1)} %bitcast.19), channel_id=1, source_target_pairs={{0,4},{4,0},{1,5},{5,1},{2,6},{6,2},{3,7},{7,3},{8,12},{12,8},{9,1... | collective-permute-start | bytes 1572872 | tf_op jit(solution)/shard_map/ppermute | solution.py:326
  25.5 10.5 %all-to-all-done = bf16[32,48,128]{2,1,0:T(8,128)(2,1)S(1)} async-done(((bf16[32,48,128]{2,1,0:T(8,128)(2,1)}), bf16[32,48,128]{2,1,0:T(8,128)(2,1)S(1)}, u32[]{:S(2)}, u32[]{:S(2)}) %all-to-all-start) | async-done | bytes 393248 | tf_op jit(solution)/shard_map/all_to_all | solution.py:327
  36.0 0.4 shard_map.127.refs_0_
  36.4 0.0 copy-start.9
  36.4 1.9 %collective-permute-start.3 = (bf16[1536,128]{1,0:T(8,128)(2,1)S(1)}, bf16[1536,128]{1,0:T(8,128)(2,1)S(1)}, u32[]{:S(2)}, u32[]{:S(2)}) collective-permute-start(bf16[1536,128]{1,0:T(8,128)(2,1)S(1)} %shard_map.127.refs_0_), channel_id=1, source_target_pairs={{0,8},{8,0},{1,9},{9,1},{2,10},{10,2},{3,11},{11,3},{4,12},{12,4},... | collective-permute-start | bytes 1179656 | tf_op jit(solution)/shard_map/ppermute | solution.py:330
  38.3 4.9 %collective-permute-start.2 = (bf16[1536,128]{1,0:T(8,128)(2,1)S(1)}, bf16[1536,128]{1,0:T(8,128)(2,1)S(1)}, u32[]{:S(2)}, u32[]{:S(2)}) collective-permute-start(bf16[1536,128]{1,0:T(8,128)(2,1)S(1)} %shard_map.127.refs_0_), channel_id=1, source_target_pairs={{0,2},{1,3},{2,0},{3,1},{4,6},{5,7},{6,4},{7,5},{8,10},{9,11},{10,... | collective-permute-start | bytes 1179656 | tf_op jit(solution)/shard_map/ppermute | solution.py:310
  43.2 2.5 %collective-permute-start = (bf16[1536,128]{1,0:T(8,128)(2,1)S(1)}, bf16[1536,128]{1,0:T(8,128)(2,1)S(1)}, u32[]{:S(2)}, u32[]{:S(2)}) collective-permute-start(bf16[1536,128]{1,0:T(8,128)(2,1)S(1)} %shard_map.127.refs_0_), channel_id=1, source_target_pairs={{0,1},{1,2},{2,3},{3,0},{4,5},{5,6},{6,7},{7,4},{8,9},{9,10},{10,1... | collective-permute-start | bytes 1179656 | tf_op jit(solution)/shard_map/ppermute | solution.py:310
  45.8 0.0 collective-permute-done.8.wuo
  45.8 4.5 %collective-permute-start.1 = (bf16[1536,128]{1,0:T(8,128)(2,1)S(1)}, bf16[1536,128]{1,0:T(8,128)(2,1)S(1)}, u32[]{:S(2)}, u32[]{:S(2)}) collective-permute-start(bf16[1536,128]{1,0:T(8,128)(2,1)S(1)} %shard_map.127.refs_0_), channel_id=1, source_target_pairs={{0,3},{1,0},{2,1},{3,2},{4,7},{5,4},{6,5},{7,6},{8,11},{9,8},{10,9... | collective-permute-start | bytes 1179656 | tf_op jit(solution)/shard_map/ppermute | solution.py:310
  50.3 1.9 %collective-permute-start.4 = (bf16[1536,128]{1,0:T(8,128)(2,1)S(1)}, bf16[1536,128]{1,0:T(8,128)(2,1)S(1)}, u32[]{:S(2)}, u32[]{:S(2)}) collective-permute-start(bf16[1536,128]{1,0:T(8,128)(2,1)S(1)} %collective-permute-done.3.refs_0_.refs_4_), channel_id=1, source_target_pairs={{0,1},{1,2},{2,3},{3,0},{4,5},{5,6},{6,7},{7,4},{8,9},{9,10},{10,1... | collective-permute-start | bytes 1179656 | tf_op jit(solution)/shard_map/ppermute | solution.py:310
  52.3 0.0 collective-permute-done.9.wdo
  52.3 5.1 %collective-permute-start.5 = (bf16[1536,128]{1,0:T(8,128)(2,1)S(1)}, bf16[1536,128]{1,0:T(8,128)(2,1)S(1)}, u32[]{:S(2)}, u32[]{:S(2)}) collective-permute-start(bf16[1536,128]{1,0:T(8,128)(2,1)S(1)} %collective-permute-done.3.refs_0_.refs_4_), channel_id=1, source_target_pairs={{0,3},{1,0},{2,1},{3,2},{4,7},{5,4},{6,5},{7,6},{8,11},{9,8},{10,9... | collective-permute-start | bytes 1179656 | tf_op jit(solution)/shard_map/ppermute | solution.py:310
  57.4 3.9 %collective-permute-start.6 = (bf16[1536,128]{1,0:T(8,128)(2,1)S(1)}, bf16[1536,128]{1,0:T(8,128)(2,1)S(1)}, u32[]{:S(2)}, u32[]{:S(2)}) collective-permute-start(bf16[1536,128]{1,0:T(8,128)(2,1)S(1)} %collective-permute-done.2.refs_3_), channel_id=1, source_target_pairs={{0,8},{8,0},{1,9},{9,1},{2,10},{10,2},{3,11},{11,3},{4,12},{12,4},... | collective-permute-start | bytes 1179656 | tf_op jit(solution)/shard_map/ppermute | solution.py:333
  61.4 0.3 shard_map.128
  61.7 0.0 collective-permute-done.refs_1_
  61.7 0.0 copy-start.14
  61.7 0.5 collective-permute-done.1.refs_2_
  62.2 3.5 %shard_map.129 = (bf16[4,1600,128]{2,1,0:T(8,128)(2,1)}, bf16[3,384,512]{2,1,0:T(8,128)(2,1)}) custom-call(bf16[1536,128]{1,0:T(8,128)(2,1)S(1)} %shard_map.127.refs_0_, bf16[1536,128]{1,0:T(8,128)(2,1)S(1)} %collective-permute-done.refs_1_, bf16[1536,128]{1,0:T(8,128)(2,1)S(1)} %collective-permute-done.1.refs_2_, ...), custom_call_target="tpu_custom_call" | custom-call | flops 2147483648 | bytes 1048576 | tf_op jit(solution)/shard_map/pallas_call | solution.py:38
  65.8 3.2 %collective-permute-done.4.refs_1_.refs_5_ = bf16[1536,128]{1,0:T(8,128)(2,1)S(1)} collective-permute-done((bf16[1536,128]{1,0:T(8,128)(2,1)S(1)}, bf16[1536,128]{1,0:T(8,128)(2,1)S(1)}, u32[]{:S(2)}, u32[]{:S(2)}) %collective-permute-start.4) | collective-permute-done | bytes 393248 | tf_op jit(solution)/shard_map/ppermute | solution.py:310
  69.0 0.1 collective-permute-done.5.refs_2_.refs_6_
  69.1 0.0 collective-permute-done.6.refs_3_.refs_7_
  69.1 3.6 %shard_map.130 = (bf16[4,1600,128]{2,1,0:T(8,128)(2,1)}, bf16[3,384,512]{2,1,0:T(8,128)(2,1)}) custom-call(bf16[4,1600,128]{2,1,0:T(8,128)(2,1)} %get-tuple-element.33.early, bf16[1536,128]{1,0:T(8,128)(2,1)S(1)} %collective-permute-done.3.refs_0_.refs_4_, ...), custom_call_target="tpu_custom_call", output_to_operand_aliasing={{0}: (0, {})} | custom-call | flops 2147483648 | bytes 1048576 | tf_op jit(solution)/shard_map/pallas_call | solution.py:38
  72.7 7.1 %shard_map.131 = (f32[1024,256]{1,0:T(8,128)S(1)}, f32[1024,256]{1,0:T(8,128)S(1)}, f32[256,1024]{1,0:T(8,128)S(1)}, bf16[3,1024,256]{2,1,0:T(8,128)(2,1)}) custom-call(bf16[1536,128]{1,0:T(8,128)(2,1)} %copy-done.9, bf16[1536,128]{1,0:T(8,128)(2,1)} %copy-done.14, bf16[1536,128]{1,0:T(8,128)(2,1)} %copy-done.15, bf16[1536,128]{1,0:T(8,128)(2,1)} %copy-done.13, ...), custom_call_target="tpu_custom_call" | custom-call | flops 2147483648 | bytes 1048576 | tf_op jit(solution)/shard_map/pallas_call | solution.py:38
  79.8 1.0 copy-done
  80.8 1.0 copy-done.2
  81.8 1.0 copy-done.4
  82.8 1.9 %collective-permute-start.10 = (bf16[3,1024,256]{2,1,0:T(8,128)(2,1)}, bf16[3,1024,256]{2,1,0:T(8,128)(2,1)S(1)}, u32[]{:S(2)}, u32[]{:S(2)}) collective-permute-start(bf16[3,1024,256]{2,1,0:T(8,128)(2,1)} %get-tuple-element.38), channel_id=1, source_target_pairs={{0,4},{4,0},{1,5},{5,1},{2,6},{6,2},{3,7},{7,3},{8,12},{12,8},{9,1... | collective-permute-start | bytes 4718600 | tf_op jit(solution)/shard_map/ppermute | solution.py:355
  84.7 4.2 %all-to-all-start.1 = ((bf16[4,1600,128]{2,1,0:T(8,128)(2,1)}), bf16[4,1600,128]{2,1,0:T(8,128)(2,1)S(1)}, u32[]{:S(2)}, u32[]{:S(2)}) async-start(bf16[4,1600,128]{2,1,0:T(8,128)(2,1)} %get-tuple-element.40), calls=%async_computation.1 | async-start | bytes 3276800 | tf_op jit(solution)/shard_map/all_to_all | solution.py:348
  88.9 1.2 copy-done.1
  90.1 1.2 copy-done.3
  91.4 1.2 copy-done.5
  92.6 1.5 shard_map.132
  94.1 16.8 %all-to-all-done.1.parts = bf16[4,1600,128]{2,1,0:T(8,128)(2,1)S(1)} async-done(((bf16[4,1600,128]{2,1,0:T(8,128)(2,1)}), bf16[4,1600,128]{2,1,0:T(8,128)(2,1)S(1)}, u32[]{:S(2)}, u32[]{:S(2)}) %all-to-all-start.1) | async-done | bytes 1638432 | tf_op jit(solution)/shard_map/all_to_all | solution.py:348
  111.0 0.1 shard_map.133
  111.1 0.0 copy-start.10
  111.1 0.0 copy-start.11
  111.1 3.6 %collective-permute-start.11 = (bf16[800,128]{1,0:T(8,128)(2,1)S(1)}, bf16[800,128]{1,0:T(8,128)(2,1)S(1)}, u32[]{:S(2)}, u32[]{:S(2)}) collective-permute-start(bf16[800,128]{1,0:T(8,128)(2,1)S(1)} %shard_map.133), channel_id=1, source_target_pairs={{0,8},{8,0},{1,9},{9,1},{2,10},{10,2},{3,11},{11,3},{4,12},{12,4},... | collective-permute-start | bytes 614408 | tf_op jit(solution)/shard_map/ppermute | solution.py:367
  114.8 8.7 %all_to_all.25.squares = f32[16,8,128]{2,1,0:T(8,128)S(1)} all-to-all(f32[16,8,128]{2,1,0:T(8,128)S(1)} %get-tuple-element.42), channel_id=1, replica_groups=mesh['z'=8,'yh'=4,'yp'=2,'c'=2,'tp'=4] {'c','yp','tp'}, dimensions={0} | all-to-all | bytes 131072 | tf_op jit(solution)/shard_map/all_to_all | solution.py:365
  123.5 0.0 collective-permute-done.11.near
  123.5 0.4 shard_map.134
  123.9 19.1 %all_to_all.26 = bf16[32,32,128]{2,1,0:T(8,128)(2,1)S(1)} all-to-all(bf16[32,32,128]{2,1,0:T(8,128)(2,1)S(1)} %bitcast.14), channel_id=1, replica_groups=mesh['z'=8,'yh'=4,'yp'=2,'c'=2,'tp'=4] {'z','yh'}, dimensions={0} | all-to-all | bytes 524288 | tf_op jit(solution)/shard_map/all_to_all | solution.py:369
  143.0 1.5 shard_map.135
  144.5 10.5 %all_to_all.27.got = bf16[4,384,128]{2,1,0:T(8,128)(2,1)S(1)} all-to-all(bf16[4,384,128]{2,1,0:T(8,128)(2,1)S(1)} %get-tuple-element.43), channel_id=1, replica_groups=mesh['z'=8,'yh'=4,'yp'=2,'c'=2,'tp'=4] {'tp'}, dimensions={0} | all-to-all | bytes 786432 | tf_op jit(solution)/shard_map/all_to_all | solution.py:374
  155.0 0.9 shard_map.136
  (32 shorter events, 0.1 us)
Async XLA Ops:
  0.6 18.6 %copy-start.6 = (bf16[1,1024,256]{2,1,0:T(8,128)(2,1)S(1)}, bf16[1,1024,256]{2,1,0:T(8,128)(2,1)}, u32[]{:S(2)}) copy-start(bf16[1,1024,256]{2,1,0:T(8,128)(2,1)} %param.11) | copy-start | bytes 1572868
  0.6 20.5 %copy-start.7 = (bf16[1,1024,256]{2,1,0:T(8,128)(2,1)S(1)}, bf16[1,1024,256]{2,1,0:T(8,128)(2,1)}, u32[]{:S(2)}) copy-start(bf16[1,1024,256]{2,1,0:T(8,128)(2,1)} %param.12) | copy-start | bytes 1572868
  0.7 22.9 %copy-start.8 = (bf16[1,256,1024]{2,1,0:T(8,128)(2,1)S(1)}, bf16[1,256,1024]{2,1,0:T(8,128)(2,1)}, u32[]{:S(2)}) copy-start(bf16[1,256,1024]{2,1,0:T(8,128)(2,1)} %param.13) | copy-start | bytes 1572868
  3.1 32.9 %all-to-all-start = ((bf16[32,48,128]{2,1,0:T(8,128)(2,1)}), bf16[32,48,128]{2,1,0:T(8,128)(2,1)S(1)}, u32[]{:S(2)}, u32[]{:S(2)}) async-start(bf16[32,48,128]{2,1,0:T(8,128)(2,1)} %bitcast.26), calls=%async_computation | async-start | bytes 786432 | tf_op jit(solution)/shard_map/all_to_all | solution.py:327
  19.2 24.0 %collective-permute-start.7 = (bf16[1024,256]{1,0:T(8,128)(2,1)S(1)}, bf16[1024,256]{1,0:T(8,128)(2,1)S(1)}, u32[]{:S(2)}, u32[]{:S(2)}) collective-permute-start(bf16[1024,256]{1,0:T(8,128)(2,1)S(1)} %bitcast.15), channel_id=1, source_target_pairs={{0,4},{4,0},{1,5},{5,1},{2,6},{6,2},{3,7},{7,3},{8,12},{12,8},{9,1... | collective-permute-start | bytes 1572872 | tf_op jit(solution)/shard_map/ppermute | solution.py:326
  21.2 24.6 %collective-permute-start.8 = (bf16[1024,256]{1,0:T(8,128)(2,1)S(1)}, bf16[1024,256]{1,0:T(8,128)(2,1)S(1)}, u32[]{:S(2)}, u32[]{:S(2)}) collective-permute-start(bf16[1024,256]{1,0:T(8,128)(2,1)S(1)} %bitcast.17), channel_id=1, source_target_pairs={{0,4},{4,0},{1,5},{5,1},{2,6},{6,2},{3,7},{7,3},{8,12},{12,8},{9,1... | collective-permute-start | bytes 1572872 | tf_op jit(solution)/shard_map/ppermute | solution.py:326
  23.6 28.7 %collective-permute-start.9 = (bf16[256,1024]{1,0:T(8,128)(2,1)S(1)}, bf16[256,1024]{1,0:T(8,128)(2,1)S(1)}, u32[]{:S(2)}, u32[]{:S(2)}) collective-permute-start(bf16[256,1024]{1,0:T(8,128)(2,1)S(1)} %bitcast.19), channel_id=1, source_target_pairs={{0,4},{4,0},{1,5},{5,1},{2,6},{6,2},{3,7},{7,3},{8,12},{12,8},{9,1... | collective-permute-start | bytes 1572872 | tf_op jit(solution)/shard_map/ppermute | solution.py:326
  36.4 25.8 %copy-start.9 = (bf16[1536,128]{1,0:T(8,128)(2,1)}, bf16[1536,128]{1,0:T(8,128)(2,1)S(1)}, u32[]{:S(2)}) copy-start(bf16[1536,128]{1,0:T(8,128)(2,1)S(1)} %shard_map.127.refs_0_) | copy-start | bytes 1179652
  36.4 14.0 %collective-permute-start.3 = (bf16[1536,128]{1,0:T(8,128)(2,1)S(1)}, bf16[1536,128]{1,0:T(8,128)(2,1)S(1)}, u32[]{:S(2)}, u32[]{:S(2)}) collective-permute-start(bf16[1536,128]{1,0:T(8,128)(2,1)S(1)} %shard_map.127.refs_0_), channel_id=1, source_target_pairs={{0,8},{8,0},{1,9},{9,1},{2,10},{10,2},{3,11},{11,3},{4,12},{12,4},... | collective-permute-start | bytes 1179656 | tf_op jit(solution)/shard_map/ppermute | solution.py:330
  38.3 19.1 %collective-permute-start.2 = (bf16[1536,128]{1,0:T(8,128)(2,1)S(1)}, bf16[1536,128]{1,0:T(8,128)(2,1)S(1)}, u32[]{:S(2)}, u32[]{:S(2)}) collective-permute-start(bf16[1536,128]{1,0:T(8,128)(2,1)S(1)} %shard_map.127.refs_0_), channel_id=1, source_target_pairs={{0,2},{1,3},{2,0},{3,1},{4,6},{5,7},{6,4},{7,5},{8,10},{9,11},{10,... | collective-permute-start | bytes 1179656 | tf_op jit(solution)/shard_map/ppermute | solution.py:310
  43.2 18.4 %collective-permute-start = (bf16[1536,128]{1,0:T(8,128)(2,1)S(1)}, bf16[1536,128]{1,0:T(8,128)(2,1)S(1)}, u32[]{:S(2)}, u32[]{:S(2)}) collective-permute-start(bf16[1536,128]{1,0:T(8,128)(2,1)S(1)} %shard_map.127.refs_0_), channel_id=1, source_target_pairs={{0,1},{1,2},{2,3},{3,0},{4,5},{5,6},{6,7},{7,4},{8,9},{9,10},{10,1... | collective-permute-start | bytes 1179656 | tf_op jit(solution)/shard_map/ppermute | solution.py:310
  45.8 16.4 %collective-permute-start.1 = (bf16[1536,128]{1,0:T(8,128)(2,1)S(1)}, bf16[1536,128]{1,0:T(8,128)(2,1)S(1)}, u32[]{:S(2)}, u32[]{:S(2)}) collective-permute-start(bf16[1536,128]{1,0:T(8,128)(2,1)S(1)} %shard_map.127.refs_0_), channel_id=1, source_target_pairs={{0,3},{1,0},{2,1},{3,2},{4,7},{5,4},{6,5},{7,6},{8,11},{9,8},{10,9... | collective-permute-start | bytes 1179656 | tf_op jit(solution)/shard_map/ppermute | solution.py:310
  50.3 18.8 %copy-start.12 = (bf16[1536,128]{1,0:T(8,128)(2,1)}, bf16[1536,128]{1,0:T(8,128)(2,1)S(1)}, u32[]{:S(2)}) copy-start(bf16[1536,128]{1,0:T(8,128)(2,1)S(1)} %collective-permute-done.3.refs_0_.refs_4_) | copy-start | bytes 1179652
  50.3 18.6 %collective-permute-start.4 = (bf16[1536,128]{1,0:T(8,128)(2,1)S(1)}, bf16[1536,128]{1,0:T(8,128)(2,1)S(1)}, u32[]{:S(2)}, u32[]{:S(2)}) collective-permute-start(bf16[1536,128]{1,0:T(8,128)(2,1)S(1)} %collective-permute-done.3.refs_0_.refs_4_), channel_id=1, source_target_pairs={{0,1},{1,2},{2,3},{3,0},{4,5},{5,6},{6,7},{7,4},{8,9},{9,10},{10,1... | collective-permute-start | bytes 1179656 | tf_op jit(solution)/shard_map/ppermute | solution.py:310
  52.3 16.8 %collective-permute-start.5 = (bf16[1536,128]{1,0:T(8,128)(2,1)S(1)}, bf16[1536,128]{1,0:T(8,128)(2,1)S(1)}, u32[]{:S(2)}, u32[]{:S(2)}) collective-permute-start(bf16[1536,128]{1,0:T(8,128)(2,1)S(1)} %collective-permute-done.3.refs_0_.refs_4_), channel_id=1, source_target_pairs={{0,3},{1,0},{2,1},{3,2},{4,7},{5,4},{6,5},{7,6},{8,11},{9,8},{10,9... | collective-permute-start | bytes 1179656 | tf_op jit(solution)/shard_map/ppermute | solution.py:310
  57.4 4.8 %copy-start.13 = (bf16[1536,128]{1,0:T(8,128)(2,1)}, bf16[1536,128]{1,0:T(8,128)(2,1)S(1)}, u32[]{:S(2)}) copy-start(bf16[1536,128]{1,0:T(8,128)(2,1)S(1)} %collective-permute-done.2.refs_3_) | copy-start | bytes 1179652
  57.4 11.6 %collective-permute-start.6 = (bf16[1536,128]{1,0:T(8,128)(2,1)S(1)}, bf16[1536,128]{1,0:T(8,128)(2,1)S(1)}, u32[]{:S(2)}, u32[]{:S(2)}) collective-permute-start(bf16[1536,128]{1,0:T(8,128)(2,1)S(1)} %collective-permute-done.2.refs_3_), channel_id=1, source_target_pairs={{0,8},{8,0},{1,9},{9,1},{2,10},{10,2},{3,11},{11,3},{4,12},{12,4},... | collective-permute-start | bytes 1179656 | tf_op jit(solution)/shard_map/ppermute | solution.py:333
  61.7 4.1 %copy-start.14 = (bf16[1536,128]{1,0:T(8,128)(2,1)}, bf16[1536,128]{1,0:T(8,128)(2,1)S(1)}, u32[]{:S(2)}) copy-start(bf16[1536,128]{1,0:T(8,128)(2,1)S(1)} %collective-permute-done.refs_1_) | copy-start | bytes 1179652
  62.2 3.5 %copy-start.15 = (bf16[1536,128]{1,0:T(8,128)(2,1)}, bf16[1536,128]{1,0:T(8,128)(2,1)S(1)}, u32[]{:S(2)}) copy-start(bf16[1536,128]{1,0:T(8,128)(2,1)S(1)} %collective-permute-done.1.refs_2_) | copy-start | bytes 1179652
  69.0 3.7 %copy-start.16 = (bf16[1536,128]{1,0:T(8,128)(2,1)}, bf16[1536,128]{1,0:T(8,128)(2,1)S(1)}, u32[]{:S(2)}) copy-start(bf16[1536,128]{1,0:T(8,128)(2,1)S(1)} %collective-permute-done.4.refs_1_.refs_5_) | copy-start | bytes 1179652
  69.1 3.6 %copy-start.17 = (bf16[1536,128]{1,0:T(8,128)(2,1)}, bf16[1536,128]{1,0:T(8,128)(2,1)S(1)}, u32[]{:S(2)}) copy-start(bf16[1536,128]{1,0:T(8,128)(2,1)S(1)} %collective-permute-done.5.refs_2_.refs_6_) | copy-start | bytes 1179652
  69.1 3.6 %copy-start.18 = (bf16[1536,128]{1,0:T(8,128)(2,1)}, bf16[1536,128]{1,0:T(8,128)(2,1)S(1)}, u32[]{:S(2)}) copy-start(bf16[1536,128]{1,0:T(8,128)(2,1)S(1)} %collective-permute-done.6.refs_3_.refs_7_) | copy-start | bytes 1179652
  79.8 1.0 copy-start
  80.8 1.0 copy-start.2
  81.8 1.0 copy-start.4
  82.8 6.1 %collective-permute-start.10 = (bf16[3,1024,256]{2,1,0:T(8,128)(2,1)}, bf16[3,1024,256]{2,1,0:T(8,128)(2,1)S(1)}, u32[]{:S(2)}, u32[]{:S(2)}) collective-permute-start(bf16[3,1024,256]{2,1,0:T(8,128)(2,1)} %get-tuple-element.38), channel_id=1, source_target_pairs={{0,4},{4,0},{1,5},{5,1},{2,6},{6,2},{3,7},{7,3},{8,12},{12,8},{9,1... | collective-permute-start | bytes 4718600 | tf_op jit(solution)/shard_map/ppermute | solution.py:355
  84.7 26.3 %all-to-all-start.1 = ((bf16[4,1600,128]{2,1,0:T(8,128)(2,1)}), bf16[4,1600,128]{2,1,0:T(8,128)(2,1)S(1)}, u32[]{:S(2)}, u32[]{:S(2)}) async-start(bf16[4,1600,128]{2,1,0:T(8,128)(2,1)} %get-tuple-element.40), calls=%async_computation.1 | async-start | bytes 3276800 | tf_op jit(solution)/shard_map/all_to_all | solution.py:348
  88.9 1.2 copy-start.1
  90.1 1.2 copy-start.3
  91.4 1.2 copy-start.5
  111.1 31.9 %copy-start.10 = (s32[128,2]{0,1:T(2,128)S(1)}, s32[128,2]{0,1:T(2,128)}, u32[]{:S(2)}) copy-start(s32[128,2]{0,1:T(2,128)} %param.9) | copy-start | bytes 3076
  111.1 31.9 %copy-start.11 = (bf16[128,2]{0,1:T(2,128)(2,1)S(1)}, bf16[128,2]{0,1:T(2,128)(2,1)}, u32[]{:S(2)}) copy-start(bf16[128,2]{0,1:T(2,128)(2,1)} %param.10) | copy-start | bytes 1540
  111.1 12.3 %collective-permute-start.11 = (bf16[800,128]{1,0:T(8,128)(2,1)S(1)}, bf16[800,128]{1,0:T(8,128)(2,1)S(1)}, u32[]{:S(2)}, u32[]{:S(2)}) collective-permute-start(bf16[800,128]{1,0:T(8,128)(2,1)S(1)} %shard_map.133), channel_id=1, source_target_pairs={{0,8},{8,0},{1,9},{9,1},{2,10},{10,2},{3,11},{11,3},{4,12},{12,4},... | collective-permute-start | bytes 614408 | tf_op jit(solution)/shard_map/ppermute | solution.py:367

commit v5 on v3

--- a/solution.py
+++ b/solution.py
@@ -219,14 +219,14 @@
 
 def sums_body(g_own, u_own, d_own, far, g_out, u_out, d_out, in_sq, hid_sq):
     ones = jnp.ones((8, H), BF)
-    in_sq[...] = jnp.zeros((16, 8, 128), F32)
+    in_sq[...] = jnp.zeros((8, 8, 128), F32)
     for k, (own, out) in enumerate(((g_own, g_out), (u_own, u_out))):
         grad = own[...] + far[k].astype(F32)
         out[...] = grad.astype(BF)
         squares = dot(ones, (grad * grad).astype(BF), NT)
         for b in range(8):
             row = k * 2 + b % 2
-            for copy in range(4):
+            for copy in range(2):
                 in_sq[copy * 4 + b // 2, row : row + 1, :] = squares[0:1, b * 128 : (b + 1) * 128]
     total = jnp.zeros((8, H), F32)
     for b in range(4):
@@ -261,10 +261,6 @@
 
 def combine_body(rt, gt, got, out, gate):
     diagonal = iota((T, T), 0) == iota((T, T), 1)
-
-    def put(where, value):
-        for x in range(4):
-            out[x, where, :] = value.astype(BF)
 
     def column(row):
         return jnp.sum(jnp.where(diagonal, row, 0.0), axis=1, keepdims=True)
@@ -278,20 +274,22 @@
     rank0 = jnp.sum(m0 * before, axis=1, keepdims=True).astype(jnp.int32)
     rank1 = jnp.sum(m1 * before, axis=1, keepdims=True).astype(jnp.int32)
     row = iota((T, 1024), 1)
-    rows = got[...]
+    picks = []
     for half in range(2):
         hit0 = row == r0 * 32 + rank0 + half * 12
         hit1 = row == r1 * 32 + rank1 + half * 12
-        pick = jnp.where(hit0 | hit1, 1.0, 0.0).astype(BF)
-        put(slice(half * T, (half + 1) * T), dot(pick, rows))
-    for k, (r, rank) in enumerate(((r0, rank0), (r1, rank1))):
-        both = dot(jnp.where(row == r * 32 + 24, 1.0, 0.0).astype(BF), rows)
+        picks.append(ones_where(hit0 | hit1))
+    n = iota((T, 1024), 0)
+    picks.append(ones_where(row == (n & 31) * 32 + 25 + ((n >> 5) & 1) * 2 + (n >> 6)))
+    picks += [ones_where(row == r * 32 + 24) for r in (r0, r1)]
+    picked = dot(jnp.concatenate(picks, axis=0), got[...])
+    for x in range(4):
+        out[x] = picked[: 3 * T].astype(BF)
+    for k, rank in enumerate((rank0, rank1)):
+        both = picked[(3 + k) * T : (4 + k) * T]
         total = jnp.sum(jnp.where(e == rank, both, 0.0), axis=1, keepdims=True)
         share = jnp.where(diagonal, total / gates[k], 0.0)
         gate[k : k + 1, :] = jnp.sum(share, axis=0, keepdims=True)
-    n = iota((T, 1024), 0)
-    hit = row == (n & 31) * 32 + 25 + ((n >> 5) & 1) * 2 + (n >> 6)
-    put(slice(2 * T, 3 * T), dot(jnp.where(hit, 1.0, 0.0).astype(BF), rows))
 
 
 def final_body(got, token, norms):
@@ -359,12 +357,13 @@
         sums_body,
         (
             shape((D, H)), shape((D, H)), shape((H, D)),
-            shape((16, 8, 128), F32), shape((1, H), F32),
+            shape((8, 8, 128), F32), shape((1, H), F32),
         ),
         g_own, u_own, d_own, far, flops=2**29, vmem=8,
     )
+    squares = squares + lax.ppermute(squares, "c", SWAP)
     squares, parts = lax.optimization_barrier((squares, parts))
-    squares = lax.all_to_all(squares, ("c",) + GROUP, 0, 0, tiled=True)
+    squares = lax.all_to_all(squares, GROUP, 0, 0, tiled=True)
     answer = kernel(back_body, shape((1024, 128)), parts, squares)
     got = lax.all_to_all(answer.reshape(SRC, 32, 128), HOMES, 0, 0, tiled=True)
     own, gate = kernel(

time: 142 us -> 140 us (0.986)
  the two profiles are of different devices: /device:TPU:16 before, /device:TPU:8 now
where the time goes in v5:
time: 140 us; the launch traced here: 139 us
  starting transfers between devices  56.5 us (40%)
  blocking collectives  38.3 us (27%)
  waiting for transfers between devices  22.8 us (16%)
  Pallas kernels  20.4 us (15%)
    pallas_call x10, Pallas kernels, kernel(): pl.pallas_call(body, out_shape=outs, in_specs=[pl.BlockSpec(memory_space=...  20.4 us
    all_to_all x1, blocking collectives, body(): got = lax.all_to_all(answer.reshape(SRC, 32, 128), HOMES, 0, 0, tiled=True)  19.7 us
    ppermute x5, starting transfers between devices, turned(): return lax.ppermute(x, 'tp', [(i, (i + by) % 4) for i in range(4)])  19 us
    all_to_all x1, starting transfers between devices, body(): moved = lax.all_to_all(sent.reshape(SRC, 48, 128), HOMES, 0, 0, tiled=True)  15.1 us
    all_to_all x1, blocking collectives, body(): every = lax.all_to_all(own, 'tp', 0, 0, tiled=True)  9.76 us
    all_to_all x1, waiting for transfers between devices, body(): moved = lax.all_to_all(sent.reshape(SRC, 48, 128), HOMES, 0, 0, tiled=True)  9.53 us
    all_to_all x1, blocking collectives, body(): squares = lax.all_to_all(squares, GROUP, 0, 0, tiled=True)  8.82 us
    ppermute x3, starting transfers between devices, body(): others = [lax.ppermute(w, 'c', SWAP) for w in weights]  6.25 us
  transfers between devices with their start and end apart: 14, of which 8 were waited for; matrix products, arithmetic and copies ran while one was open for 0% of the time, Pallas kernels for 8%

profile of v5, /device:TPU:8, one launch (start us, length us, event | category | flops | bytes accessed | tf_op | source)
XLA Modules:
  0.0 139.1 jit_solution(14829191372872646742)
XLA Ops:
  0.6 0.0 copy-start
  0.6 0.0 copy-start.1
  0.7 0.0 copy-start.2
  0.7 2.5 %shard_map.126 = bf16[1536,128]{1,0:T(8,128)(2,1)} custom-call(s32[2,128]{1,0:T(2,128)} %bitcast.22, bf16[2,128]{1,0:T(2,128)(2,1)} %bitcast.24, bf16[128,1024]{1,0:T(8,128)(2,1)} %tok_in.1, bf16[128,1024]{1,0:T(8,128)(2,1)} %cot_in.1), custom_call_target="tpu_custom_call" | custom-call | flops 134217728 | bytes 1048576 | tf_op jit(solution)/shard_map/pallas_call | solution.py:38
  3.1 15.1 %all-to-all-start = ((bf16[32,48,128]{2,1,0:T(8,128)(2,1)}), bf16[32,48,128]{2,1,0:T(8,128)(2,1)S(1)}, u32[]{:S(2)}, u32[]{:S(2)}) async-start(bf16[32,48,128]{2,1,0:T(8,128)(2,1)} %bitcast.26), calls=%async_computation | async-start | bytes 786432 | tf_op jit(solution)/shard_map/all_to_all | solution.py:327
  18.2 0.0 copy-done
  18.2 1.9 %collective-permute-start.7 = (bf16[1024,256]{1,0:T(8,128)(2,1)S(1)}, bf16[1024,256]{1,0:T(8,128)(2,1)S(1)}, u32[]{:S(2)}, u32[]{:S(2)}) collective-permute-start(bf16[1024,256]{1,0:T(8,128)(2,1)S(1)} %bitcast.15), channel_id=1, source_target_pairs={{0,4},{4,0},{1,5},{5,1},{2,6},{6,2},{3,7},{7,3},{8,12},{12,8},{9,1... | collective-permute-start | bytes 1572872 | tf_op jit(solution)/shard_map/ppermute | solution.py:326
  20.2 0.0 copy-done.1
  20.2 2.4 %collective-permute-start.8 = (bf16[1024,256]{1,0:T(8,128)(2,1)S(1)}, bf16[1024,256]{1,0:T(8,128)(2,1)S(1)}, u32[]{:S(2)}, u32[]{:S(2)}) collective-permute-start(bf16[1024,256]{1,0:T(8,128)(2,1)S(1)} %bitcast.17), channel_id=1, source_target_pairs={{0,4},{4,0},{1,5},{5,1},{2,6},{6,2},{3,7},{7,3},{8,12},{12,8},{9,1... | collective-permute-start | bytes 1572872 | tf_op jit(solution)/shard_map/ppermute | solution.py:326
  22.6 1.9 %collective-permute-start.9 = (bf16[256,1024]{1,0:T(8,128)(2,1)S(1)}, bf16[256,1024]{1,0:T(8,128)(2,1)S(1)}, u32[]{:S(2)}, u32[]{:S(2)}) collective-permute-start(bf16[256,1024]{1,0:T(8,128)(2,1)S(1)} %bitcast.19), channel_id=1, source_target_pairs={{0,4},{4,0},{1,5},{5,1},{2,6},{6,2},{3,7},{7,3},{8,12},{12,8},{9,1... | collective-permute-start | bytes 1572872 | tf_op jit(solution)/shard_map/ppermute | solution.py:326
  24.5 9.5 %all-to-all-done = bf16[32,48,128]{2,1,0:T(8,128)(2,1)S(1)} async-done(((bf16[32,48,128]{2,1,0:T(8,128)(2,1)}), bf16[32,48,128]{2,1,0:T(8,128)(2,1)S(1)}, u32[]{:S(2)}, u32[]{:S(2)}) %all-to-all-start) | async-done | bytes 393248 | tf_op jit(solution)/shard_map/all_to_all | solution.py:327
  34.1 0.4 shard_map.127.refs_0_
  34.4 0.0 copy-start.3
  34.4 4.1 %collective-permute-start.3 = (bf16[1536,128]{1,0:T(8,128)(2,1)S(1)}, bf16[1536,128]{1,0:T(8,128)(2,1)S(1)}, u32[]{:S(2)}, u32[]{:S(2)}) collective-permute-start(bf16[1536,128]{1,0:T(8,128)(2,1)S(1)} %shard_map.127.refs_0_), channel_id=1, source_target_pairs={{0,8},{8,0},{1,9},{9,1},{2,10},{10,2},{3,11},{11,3},{4,12},{12,4},... | collective-permute-start | bytes 1179656 | tf_op jit(solution)/shard_map/ppermute | solution.py:330
  38.6 4.9 %collective-permute-start.2 = (bf16[1536,128]{1,0:T(8,128)(2,1)S(1)}, bf16[1536,128]{1,0:T(8,128)(2,1)S(1)}, u32[]{:S(2)}, u32[]{:S(2)}) collective-permute-start(bf16[1536,128]{1,0:T(8,128)(2,1)S(1)} %shard_map.127.refs_0_), channel_id=1, source_target_pairs={{0,2},{1,3},{2,0},{3,1},{4,6},{5,7},{6,4},{7,5},{8,10},{9,11},{10,... | collective-permute-start | bytes 1179656 | tf_op jit(solution)/shard_map/ppermute | solution.py:310
  43.5 0.0 collective-permute-done.7.wgo
  43.5 2.5 %collective-permute-start = (bf16[1536,128]{1,0:T(8,128)(2,1)S(1)}, bf16[1536,128]{1,0:T(8,128)(2,1)S(1)}, u32[]{:S(2)}, u32[]{:S(2)}) collective-permute-start(bf16[1536,128]{1,0:T(8,128)(2,1)S(1)} %shard_map.127.refs_0_), channel_id=1, source_target_pairs={{0,1},{1,2},{2,3},{3,0},{4,5},{5,6},{6,7},{7,4},{8,9},{9,10},{10,1... | collective-permute-start | bytes 1179656 | tf_op jit(solution)/shard_map/ppermute | solution.py:310
  46.0 0.0 collective-permute-done.8.wuo
  46.0 4.6 %collective-permute-start.1 = (bf16[1536,128]{1,0:T(8,128)(2,1)S(1)}, bf16[1536,128]{1,0:T(8,128)(2,1)S(1)}, u32[]{:S(2)}, u32[]{:S(2)}) collective-permute-start(bf16[1536,128]{1,0:T(8,128)(2,1)S(1)} %shard_map.127.refs_0_), channel_id=1, source_target_pairs={{0,3},{1,0},{2,1},{3,2},{4,7},{5,4},{6,5},{7,6},{8,11},{9,8},{10,9... | collective-permute-start | bytes 1179656 | tf_op jit(solution)/shard_map/ppermute | solution.py:310
  50.6 0.0 collective-permute-done.3.refs_0_.refs_4_
  50.6 0.0 copy-start.6
  50.6 1.9 %collective-permute-start.4 = (bf16[1536,128]{1,0:T(8,128)(2,1)S(1)}, bf16[1536,128]{1,0:T(8,128)(2,1)S(1)}, u32[]{:S(2)}, u32[]{:S(2)}) collective-permute-start(bf16[1536,128]{1,0:T(8,128)(2,1)S(1)} %collective-permute-done.3.refs_0_.refs_4_), channel_id=1, source_target_pairs={{0,1},{1,2},{2,3},{3,0},{4,5},{5,6},{6,7},{7,4},{8,9},{9,10},{10,1... | collective-permute-start | bytes 1179656 | tf_op jit(solution)/shard_map/ppermute | solution.py:310
  52.5 0.0 collective-permute-done.9.wdo
  52.6 5.1 %collective-permute-start.5 = (bf16[1536,128]{1,0:T(8,128)(2,1)S(1)}, bf16[1536,128]{1,0:T(8,128)(2,1)S(1)}, u32[]{:S(2)}, u32[]{:S(2)}) collective-permute-start(bf16[1536,128]{1,0:T(8,128)(2,1)S(1)} %collective-permute-done.3.refs_0_.refs_4_), channel_id=1, source_target_pairs={{0,3},{1,0},{2,1},{3,2},{4,7},{5,4},{6,5},{7,6},{8,11},{9,8},{10,9... | collective-permute-start | bytes 1179656 | tf_op jit(solution)/shard_map/ppermute | solution.py:310
  57.7 0.0 collective-permute-done.2.refs_3_
  57.7 1.9 %collective-permute-start.6 = (bf16[1536,128]{1,0:T(8,128)(2,1)S(1)}, bf16[1536,128]{1,0:T(8,128)(2,1)S(1)}, u32[]{:S(2)}, u32[]{:S(2)}) collective-permute-start(bf16[1536,128]{1,0:T(8,128)(2,1)S(1)} %collective-permute-done.2.refs_3_), channel_id=1, source_target_pairs={{0,8},{8,0},{1,9},{9,1},{2,10},{10,2},{3,11},{11,3},{4,12},{12,4},... | collective-permute-start | bytes 1179656 | tf_op jit(solution)/shard_map/ppermute | solution.py:333
  59.6 0.3 shard_map.128
  59.9 1.5 %collective-permute-done.refs_1_ = bf16[1536,128]{1,0:T(8,128)(2,1)S(1)} collective-permute-done((bf16[1536,128]{1,0:T(8,128)(2,1)S(1)}, bf16[1536,128]{1,0:T(8,128)(2,1)S(1)}, u32[]{:S(2)}, u32[]{:S(2)}) %collective-permute-start) | collective-permute-done | bytes 393248 | tf_op jit(solution)/shard_map/ppermute | solution.py:310
  61.4 1.0 collective-permute-done.1.refs_2_
  62.5 3.5 %shard_map.129 = (bf16[8,800,128]{2,1,0:T(8,128)(2,1)}, bf16[3,384,512]{2,1,0:T(8,128)(2,1)}) custom-call(bf16[1536,128]{1,0:T(8,128)(2,1)S(1)} %shard_map.127.refs_0_, bf16[1536,128]{1,0:T(8,128)(2,1)S(1)} %collective-permute-done.refs_1_, bf16[1536,128]{1,0:T(8,128)(2,1)S(1)} %collective-permute-done.1.refs_2_, ...), custom_call_target="tpu_custom_call" | custom-call | flops 2147483648 | bytes 1048576 | tf_op jit(solution)/shard_map/pallas_call | solution.py:38
  66.0 1.7 %collective-permute-done.4.refs_1_.refs_5_ = bf16[1536,128]{1,0:T(8,128)(2,1)S(1)} collective-permute-done((bf16[1536,128]{1,0:T(8,128)(2,1)S(1)}, bf16[1536,128]{1,0:T(8,128)(2,1)S(1)}, u32[]{:S(2)}, u32[]{:S(2)}) %collective-permute-start.4) | collective-permute-done | bytes 393248 | tf_op jit(solution)/shard_map/ppermute | solution.py:310
  67.7 0.1 collective-permute-done.5.refs_2_.refs_6_
  67.8 0.0 collective-permute-done.6.refs_3_.refs_7_
  67.8 3.5 %shard_map.130 = (bf16[8,800,128]{2,1,0:T(8,128)(2,1)}, bf16[3,384,512]{2,1,0:T(8,128)(2,1)}) custom-call(bf16[8,800,128]{2,1,0:T(8,128)(2,1)} %get-tuple-element.33.early, bf16[1536,128]{1,0:T(8,128)(2,1)S(1)} %collective-permute-done.3.refs_0_.refs_4_, ...), custom_call_target="tpu_custom_call", output_to_operand_aliasing={{0}: (0, {})} | custom-call | flops 2147483648 | bytes 1048576 | tf_op jit(solution)/shard_map/pallas_call | solution.py:38
  71.4 6.0 %all-to-all-start.1 = ((bf16[8,800,128]{2,1,0:T(8,128)(2,1)}), bf16[8,800,128]{2,1,0:T(8,128)(2,1)S(1)}, u32[]{:S(2)}, u32[]{:S(2)}) async-start(bf16[8,800,128]{2,1,0:T(8,128)(2,1)} %get-tuple-element.40), calls=%async_computation.1 | async-start | bytes 3276800 | tf_op jit(solution)/shard_map/all_to_all | solution.py:348
  77.4 5.9 %shard_map.131 = (f32[1024,256]{1,0:T(8,128)S(1)}, f32[1024,256]{1,0:T(8,128)S(1)}, f32[256,1024]{1,0:T(8,128)S(1)}, bf16[3,1024,256]{2,1,0:T(8,128)(2,1)S(1)}) custom-call(bf16[1536,128]{1,0:T(8,128)(2,1)} %copy-done.3, bf16[1536,128]{1,0:T(8,128)(2,1)} %copy-done.8, bf16[1536,128]{1,0:T(8,128)(2,1)} %copy-done.9, bf16[1536,128]{1,0:T(8,128)(2,1)} %copy-done.7, ...), custom_call_target="tpu_custom_call" | custom-call | flops 2147483648 | bytes 1048576 | tf_op jit(solution)/shard_map/pallas_call | solution.py:38
  83.3 1.9 %collective-permute-start.10 = (bf16[3,1024,256]{2,1,0:T(8,128)(2,1)S(1)}, bf16[3,1024,256]{2,1,0:T(8,128)(2,1)S(1)}, u32[]{:S(2)}, u32[]{:S(2)}) collective-permute-start(bf16[3,1024,256]{2,1,0:T(8,128)(2,1)S(1)} %get-tuple-element.38), channel_id=1, source_target_pairs={{0,4},{4,0},{1,5},{5,1},{2,6},{6,2},{3,7},{7,3},{8,12},{12,8},{9,1... | collective-permute-start | bytes 4718600 | tf_op jit(solution)/shard_map/ppermute | solution.py:355
  85.3 3.4 %collective-permute-done.10.far = bf16[3,1024,256]{2,1,0:T(8,128)(2,1)S(1)} collective-permute-done((bf16[3,1024,256]{2,1,0:T(8,128)(2,1)S(1)}, bf16[3,1024,256]{2,1,0:T(8,128)(2,1)S(1)}, u32[]{:S(2)}, u32[]{:S(2)}) %collective-permute-start.10) | collective-permute-done | bytes 1572896 | tf_op jit(solution)/shard_map/ppermute | solution.py:355
  88.6 1.4 %shard_map.132 = (bf16[1024,256]{1,0:T(8,128)(2,1)}, bf16[1024,256]{1,0:T(8,128)(2,1)}, bf16[256,1024]{1,0:T(8,128)(2,1)}, f32[8,8,128]{2,1,0:T(8,128)S(1)}, f32[1,256]{1,0:T(1,128)}) custom-call(f32[1024,256]{1,0:T(8,128)S(1)} %get-tuple-element.35.g_own, f32[1024,256]{1,0:T(8,128)S(1)} %get-tuple-element.36.u_own, ...), custom_call_target="tpu_custom_call" | custom-call | flops 536870912 | bytes 1048576 | tf_op jit(solution)/shard_map/pallas_call | solution.py:38
  90.1 2.2 %collective-permute-start.11 = (f32[8,8,128]{2,1,0:T(8,128)S(1)}, f32[8,8,128]{2,1,0:T(8,128)S(1)}, u32[]{:S(2)}, u32[]{:S(2)}) collective-permute-start(f32[8,8,128]{2,1,0:T(8,128)S(1)} %get-tuple-element.39), channel_id=1, source_target_pairs={{0,4},{4,0},{1,5},{5,1},{2,6},{6,2},{3,7},{7,3},{8,12},{12,8},{9,1... | collective-permute-start | bytes 98312 | tf_op jit(solution)/shard_map/ppermute | solution.py:364
  92.2 1.0 collective-permute-done.11
  93.3 4.6 %all-to-all-done.1.parts = bf16[8,800,128]{2,1,0:T(8,128)(2,1)S(1)} async-done(((bf16[8,800,128]{2,1,0:T(8,128)(2,1)}), bf16[8,800,128]{2,1,0:T(8,128)(2,1)S(1)}, u32[]{:S(2)}, u32[]{:S(2)}) %all-to-all-start.1) | async-done | bytes 1638432 | tf_op jit(solution)/shard_map/all_to_all | solution.py:348
  97.9 8.8 %all_to_all.25.squares = f32[8,8,128]{2,1,0:T(8,128)S(1)} all-to-all(f32[8,8,128]{2,1,0:T(8,128)S(1)} %add.3), channel_id=1, replica_groups=mesh['z'=8,'yh'=4,'yp'=2,'c'=2,'tp'=4] {'yp','tp'}, dimensions={0} | all-to-all | bytes 65536 | tf_op jit(solution)/shard_map/all_to_all | solution.py:366
  106.7 0.5 shard_map.133
  107.1 19.7 %all_to_all.26 = bf16[32,32,128]{2,1,0:T(8,128)(2,1)S(1)} all-to-all(bf16[32,32,128]{2,1,0:T(8,128)(2,1)S(1)} %bitcast.14), channel_id=1, replica_groups=mesh['z'=8,'yh'=4,'yp'=2,'c'=2,'tp'=4] {'z','yh'}, dimensions={0} | all-to-all | bytes 524288 | tf_op jit(solution)/shard_map/all_to_all | solution.py:368
  126.9 1.5 %shard_map.134 = (bf16[4,384,128]{2,1,0:T(8,128)(2,1)S(1)}, f32[2,128]{1,0:T(2,128)}) custom-call(s32[2,128]{1,0:T(2,128)S(1)} %bitcast.23, bf16[2,128]{1,0:T(2,128)(2,1)S(1)} %bitcast.25, bf16[1024,128]{1,0:T(8,128)(2,1)S(1)} %bitcast.21), custom_call_target="tpu_custom_call" | custom-call | flops 134217728 | bytes 1048576 | tf_op jit(solution)/shard_map/pallas_call | solution.py:38
  128.4 9.8 %all_to_all.27.got = bf16[4,384,128]{2,1,0:T(8,128)(2,1)S(1)} all-to-all(bf16[4,384,128]{2,1,0:T(8,128)(2,1)S(1)} %get-tuple-element.43), channel_id=1, replica_groups=mesh['z'=8,'yh'=4,'yp'=2,'c'=2,'tp'=4] {'tp'}, dimensions={0} | all-to-all | bytes 786432 | tf_op jit(solution)/shard_map/all_to_all | solution.py:373
  138.2 0.9 shard_map.135
  (20 shorter events, 0.0 us)
Async XLA Ops:
  0.6 17.6 %copy-start = (bf16[1,1024,256]{2,1,0:T(8,128)(2,1)S(1)}, bf16[1,1024,256]{2,1,0:T(8,128)(2,1)}, u32[]{:S(2)}) copy-start(bf16[1,1024,256]{2,1,0:T(8,128)(2,1)} %param.11) | copy-start | bytes 1572868
  0.6 19.5 %copy-start.1 = (bf16[1,1024,256]{2,1,0:T(8,128)(2,1)S(1)}, bf16[1,1024,256]{2,1,0:T(8,128)(2,1)}, u32[]{:S(2)}) copy-start(bf16[1,1024,256]{2,1,0:T(8,128)(2,1)} %param.12) | copy-start | bytes 1572868
  0.7 21.9 %copy-start.2 = (bf16[1,256,1024]{2,1,0:T(8,128)(2,1)S(1)}, bf16[1,256,1024]{2,1,0:T(8,128)(2,1)}, u32[]{:S(2)}) copy-start(bf16[1,256,1024]{2,1,0:T(8,128)(2,1)} %param.13) | copy-start | bytes 1572868
  3.1 30.9 %all-to-all-start = ((bf16[32,48,128]{2,1,0:T(8,128)(2,1)}), bf16[32,48,128]{2,1,0:T(8,128)(2,1)S(1)}, u32[]{:S(2)}, u32[]{:S(2)}) async-start(bf16[32,48,128]{2,1,0:T(8,128)(2,1)} %bitcast.26), calls=%async_computation | async-start | bytes 786432 | tf_op jit(solution)/shard_map/all_to_all | solution.py:327
  18.2 25.3 %collective-permute-start.7 = (bf16[1024,256]{1,0:T(8,128)(2,1)S(1)}, bf16[1024,256]{1,0:T(8,128)(2,1)S(1)}, u32[]{:S(2)}, u32[]{:S(2)}) collective-permute-start(bf16[1024,256]{1,0:T(8,128)(2,1)S(1)} %bitcast.15), channel_id=1, source_target_pairs={{0,4},{4,0},{1,5},{5,1},{2,6},{6,2},{3,7},{7,3},{8,12},{12,8},{9,1... | collective-permute-start | bytes 1572872 | tf_op jit(solution)/shard_map/ppermute | solution.py:326
  20.2 25.9 %collective-permute-start.8 = (bf16[1024,256]{1,0:T(8,128)(2,1)S(1)}, bf16[1024,256]{1,0:T(8,128)(2,1)S(1)}, u32[]{:S(2)}, u32[]{:S(2)}) collective-permute-start(bf16[1024,256]{1,0:T(8,128)(2,1)S(1)} %bitcast.17), channel_id=1, source_target_pairs={{0,4},{4,0},{1,5},{5,1},{2,6},{6,2},{3,7},{7,3},{8,12},{12,8},{9,1... | collective-permute-start | bytes 1572872 | tf_op jit(solution)/shard_map/ppermute | solution.py:326
  22.6 29.9 %collective-permute-start.9 = (bf16[256,1024]{1,0:T(8,128)(2,1)S(1)}, bf16[256,1024]{1,0:T(8,128)(2,1)S(1)}, u32[]{:S(2)}, u32[]{:S(2)}) collective-permute-start(bf16[256,1024]{1,0:T(8,128)(2,1)S(1)} %bitcast.19), channel_id=1, source_target_pairs={{0,4},{4,0},{1,5},{5,1},{2,6},{6,2},{3,7},{7,3},{8,12},{12,8},{9,1... | collective-permute-start | bytes 1572872 | tf_op jit(solution)/shard_map/ppermute | solution.py:326
  34.4 28.0 %copy-start.3 = (bf16[1536,128]{1,0:T(8,128)(2,1)}, bf16[1536,128]{1,0:T(8,128)(2,1)S(1)}, u32[]{:S(2)}) copy-start(bf16[1536,128]{1,0:T(8,128)(2,1)S(1)} %shard_map.127.refs_0_) | copy-start | bytes 1179652
  34.4 16.2 %collective-permute-start.3 = (bf16[1536,128]{1,0:T(8,128)(2,1)S(1)}, bf16[1536,128]{1,0:T(8,128)(2,1)S(1)}, u32[]{:S(2)}, u32[]{:S(2)}) collective-permute-start(bf16[1536,128]{1,0:T(8,128)(2,1)S(1)} %shard_map.127.refs_0_), channel_id=1, source_target_pairs={{0,8},{8,0},{1,9},{9,1},{2,10},{10,2},{3,11},{11,3},{4,12},{12,4},... | collective-permute-start | bytes 1179656 | tf_op jit(solution)/shard_map/ppermute | solution.py:330
  38.6 19.1 %collective-permute-start.2 = (bf16[1536,128]{1,0:T(8,128)(2,1)S(1)}, bf16[1536,128]{1,0:T(8,128)(2,1)S(1)}, u32[]{:S(2)}, u32[]{:S(2)}) collective-permute-start(bf16[1536,128]{1,0:T(8,128)(2,1)S(1)} %shard_map.127.refs_0_), channel_id=1, source_target_pairs={{0,2},{1,3},{2,0},{3,1},{4,6},{5,7},{6,4},{7,5},{8,10},{9,11},{10,... | collective-permute-start | bytes 1179656 | tf_op jit(solution)/shard_map/ppermute | solution.py:310
  43.5 17.9 %collective-permute-start = (bf16[1536,128]{1,0:T(8,128)(2,1)S(1)}, bf16[1536,128]{1,0:T(8,128)(2,1)S(1)}, u32[]{:S(2)}, u32[]{:S(2)}) collective-permute-start(bf16[1536,128]{1,0:T(8,128)(2,1)S(1)} %shard_map.127.refs_0_), channel_id=1, source_target_pairs={{0,1},{1,2},{2,3},{3,0},{4,5},{5,6},{6,7},{7,4},{8,9},{9,10},{10,1... | collective-permute-start | bytes 1179656 | tf_op jit(solution)/shard_map/ppermute | solution.py:310
  46.0 16.4 %collective-permute-start.1 = (bf16[1536,128]{1,0:T(8,128)(2,1)S(1)}, bf16[1536,128]{1,0:T(8,128)(2,1)S(1)}, u32[]{:S(2)}, u32[]{:S(2)}) collective-permute-start(bf16[1536,128]{1,0:T(8,128)(2,1)S(1)} %shard_map.127.refs_0_), channel_id=1, source_target_pairs={{0,3},{1,0},{2,1},{3,2},{4,7},{5,4},{6,5},{7,6},{8,11},{9,8},{10,9... | collective-permute-start | bytes 1179656 | tf_op jit(solution)/shard_map/ppermute | solution.py:310
  50.6 17.2 %copy-start.6 = (bf16[1536,128]{1,0:T(8,128)(2,1)}, bf16[1536,128]{1,0:T(8,128)(2,1)S(1)}, u32[]{:S(2)}) copy-start(bf16[1536,128]{1,0:T(8,128)(2,1)S(1)} %collective-permute-done.3.refs_0_.refs_4_) | copy-start | bytes 1179652
  50.6 17.1 %collective-permute-start.4 = (bf16[1536,128]{1,0:T(8,128)(2,1)S(1)}, bf16[1536,128]{1,0:T(8,128)(2,1)S(1)}, u32[]{:S(2)}, u32[]{:S(2)}) collective-permute-start(bf16[1536,128]{1,0:T(8,128)(2,1)S(1)} %collective-permute-done.3.refs_0_.refs_4_), channel_id=1, source_target_pairs={{0,1},{1,2},{2,3},{3,0},{4,5},{5,6},{6,7},{7,4},{8,9},{9,10},{10,1... | collective-permute-start | bytes 1179656 | tf_op jit(solution)/shard_map/ppermute | solution.py:310
  52.6 15.3 %collective-permute-start.5 = (bf16[1536,128]{1,0:T(8,128)(2,1)S(1)}, bf16[1536,128]{1,0:T(8,128)(2,1)S(1)}, u32[]{:S(2)}, u32[]{:S(2)}) collective-permute-start(bf16[1536,128]{1,0:T(8,128)(2,1)S(1)} %collective-permute-done.3.refs_0_.refs_4_), channel_id=1, source_target_pairs={{0,3},{1,0},{2,1},{3,2},{4,7},{5,4},{6,5},{7,6},{8,11},{9,8},{10,9... | collective-permute-start | bytes 1179656 | tf_op jit(solution)/shard_map/ppermute | solution.py:310
  57.7 4.8 %copy-start.7 = (bf16[1536,128]{1,0:T(8,128)(2,1)}, bf16[1536,128]{1,0:T(8,128)(2,1)S(1)}, u32[]{:S(2)}) copy-start(bf16[1536,128]{1,0:T(8,128)(2,1)S(1)} %collective-permute-done.2.refs_3_) | copy-start | bytes 1179652
  57.7 10.1 %collective-permute-start.6 = (bf16[1536,128]{1,0:T(8,128)(2,1)S(1)}, bf16[1536,128]{1,0:T(8,128)(2,1)S(1)}, u32[]{:S(2)}, u32[]{:S(2)}) collective-permute-start(bf16[1536,128]{1,0:T(8,128)(2,1)S(1)} %collective-permute-done.2.refs_3_), channel_id=1, source_target_pairs={{0,8},{8,0},{1,9},{9,1},{2,10},{10,2},{3,11},{11,3},{4,12},{12,4},... | collective-permute-start | bytes 1179656 | tf_op jit(solution)/shard_map/ppermute | solution.py:333
  61.4 4.6 %copy-start.8 = (bf16[1536,128]{1,0:T(8,128)(2,1)}, bf16[1536,128]{1,0:T(8,128)(2,1)S(1)}, u32[]{:S(2)}) copy-start(bf16[1536,128]{1,0:T(8,128)(2,1)S(1)} %collective-permute-done.refs_1_) | copy-start | bytes 1179652
  62.5 3.6 %copy-start.9 = (bf16[1536,128]{1,0:T(8,128)(2,1)}, bf16[1536,128]{1,0:T(8,128)(2,1)S(1)}, u32[]{:S(2)}) copy-start(bf16[1536,128]{1,0:T(8,128)(2,1)S(1)} %collective-permute-done.1.refs_2_) | copy-start | bytes 1179652
  67.7 3.6 %copy-start.10 = (bf16[1536,128]{1,0:T(8,128)(2,1)}, bf16[1536,128]{1,0:T(8,128)(2,1)S(1)}, u32[]{:S(2)}) copy-start(bf16[1536,128]{1,0:T(8,128)(2,1)S(1)} %collective-permute-done.4.refs_1_.refs_5_) | copy-start | bytes 1179652
  67.8 3.6 %copy-start.11 = (bf16[1536,128]{1,0:T(8,128)(2,1)}, bf16[1536,128]{1,0:T(8,128)(2,1)S(1)}, u32[]{:S(2)}) copy-start(bf16[1536,128]{1,0:T(8,128)(2,1)S(1)} %collective-permute-done.5.refs_2_.refs_6_) | copy-start | bytes 1179652
  67.8 3.6 %copy-start.12 = (bf16[1536,128]{1,0:T(8,128)(2,1)}, bf16[1536,128]{1,0:T(8,128)(2,1)S(1)}, u32[]{:S(2)}) copy-start(bf16[1536,128]{1,0:T(8,128)(2,1)S(1)} %collective-permute-done.6.refs_3_.refs_7_) | copy-start | bytes 1179652
  71.4 26.5 %all-to-all-start.1 = ((bf16[8,800,128]{2,1,0:T(8,128)(2,1)}), bf16[8,800,128]{2,1,0:T(8,128)(2,1)S(1)}, u32[]{:S(2)}, u32[]{:S(2)}) async-start(bf16[8,800,128]{2,1,0:T(8,128)(2,1)} %get-tuple-element.40), calls=%async_computation.1 | async-start | bytes 3276800 | tf_op jit(solution)/shard_map/all_to_all | solution.py:348
  83.3 5.3 %collective-permute-start.10 = (bf16[3,1024,256]{2,1,0:T(8,128)(2,1)S(1)}, bf16[3,1024,256]{2,1,0:T(8,128)(2,1)S(1)}, u32[]{:S(2)}, u32[]{:S(2)}) collective-permute-start(bf16[3,1024,256]{2,1,0:T(8,128)(2,1)S(1)} %get-tuple-element.38), channel_id=1, source_target_pairs={{0,4},{4,0},{1,5},{5,1},{2,6},{6,2},{3,7},{7,3},{8,12},{12,8},{9,1... | collective-permute-start | bytes 4718600 | tf_op jit(solution)/shard_map/ppermute | solution.py:355
  90.1 36.8 %copy-start.4 = (s32[128,2]{0,1:T(2,128)S(1)}, s32[128,2]{0,1:T(2,128)}, u32[]{:S(2)}) copy-start(s32[128,2]{0,1:T(2,128)} %param.9) | copy-start | bytes 3076
  90.1 36.8 %copy-start.5 = (bf16[128,2]{0,1:T(2,128)(2,1)S(1)}, bf16[128,2]{0,1:T(2,128)(2,1)}, u32[]{:S(2)}) copy-start(bf16[128,2]{0,1:T(2,128)(2,1)} %param.10) | copy-start | bytes 1540
  90.1 3.2 %collective-permute-start.11 = (f32[8,8,128]{2,1,0:T(8,128)S(1)}, f32[8,8,128]{2,1,0:T(8,128)S(1)}, u32[]{:S(2)}, u32[]{:S(2)}) collective-permute-start(f32[8,8,128]{2,1,0:T(8,128)S(1)} %get-tuple-element.39), channel_id=1, source_target_pairs={{0,4},{4,0},{1,5},{5,1},{2,6},{6,2},{3,7},{7,3},{8,12},{12,8},{9,1... | collective-permute-start | bytes 98312 | tf_op jit(solution)/shard_map/ppermute | solution.py:364
